TPU v7x, 512 devices: a whole 4x4x16 slice. The times are simulated.
512 devices in a mesh: sp: 16 (over z), fs: 4 (over y), tp: 8 (over x, core).
Axes of the slice: x: 4, y: 4, z: 16, core: 2. Of those that a mesh axis runs over, the one named last changes fastest.
Arguments:
- inputs: bfloat16 [4, 2048, 2048], P('fs', 'sp'), may hold values from -9 to 9
- norm_gain: float32 [2048], replicated, may hold values from 0.1 to 1.9
- hg_query_w: bfloat16 [2048, 1024], P(('sp', 'fs'), 'tp'), may hold values from -0.125 to 0.125
- hg_fwd_w: bfloat16 [2048, 1024], P(('sp', 'fs'), 'tp'), may hold values from -0.125 to 0.125
- hg_bwd_w: bfloat16 [2048, 1024], P(('sp', 'fs'), 'tp'), may hold values from -0.125 to 0.125
- hg_value_w: bfloat16 [2048, 1024], P(('sp', 'fs'), 'tp'), may hold values from -0.125 to 0.125
- floor_gap: float32 [2, 1024], P(None, 'tp'), may hold values from 0 to 0.1
- hg_norm_gain: float32 [64], replicated, may hold values from 0.1 to 1.9
- df_query_w: bfloat16 [2048, 512], P(('sp', 'fs'), 'tp'), may hold values from -0.176776695 to 0.176776695
- df_key_w: bfloat16 [2048, 512], P(('sp', 'fs'), 'tp'), may hold values from -4.4194174 to 4.4194174
- df_value_w: bfloat16 [2048, 512], P(('sp', 'fs'), 'tp'), may hold values from -0.125 to 0.125
- diff_lambda: float32 [8], P('tp'), may hold values from 0.3 to 0.8
- df_norm_gain: float32 [64], replicated, may hold values from 0.1 to 1.9
- out_hg_w: bfloat16 [1024, 2048], P('tp'), may hold values from -0.15625 to 0.15625
- out_df_w: bfloat16 [512, 2048], P('tp'), may hold values from -0.15625 to 0.15625
- post_gain: float32 [2048], replicated, may hold values from 0.1 to 1.9
Outputs:
- mixed: bfloat16 [4, 2048, 2048], P('fs', ('sp', 'tp'))
All inputs are finite; a program needn't handle non-finite values.
Results may differ from a plain program's by a relative error of at most 0.017.
Values may be sent and summed in bfloat16 or wider, within the bound.
No kernel may reach another device: no remote copies, remote signals or barrier semaphores. Data moves between devices by JAX's collectives and lax.ppermute only.
A program may use at most 64 MiB of HBM per device.

v0:
```python
import jax
import jax.numpy as jnp
from jax import lax
from jax.sharding import PartitionSpec as P

HEAD = 64
DQK = 32
BLOCK = 64
DFV = 64


epsilon = 1e-06
df_factor = 0.8


def in_one_piece(arrays, axis, dim, along):
    ends, at = ([], 0)
    for a in arrays[:-1]:
        at += a.shape[along]
        ends.append(at)
    both = jnp.concatenate(arrays, axis=along)
    return tuple(jnp.split(lax.all_gather(both, axis, axis=dim, tiled=True), ends, axis=along))


def from_everyone(array, axis):
    devices = lax.axis_size(axis)
    return lax.all_to_all(
        jnp.broadcast_to(array[None], (devices, *array.shape)), axis, 0, 0, tiled=True
    )


def all_in_one(array, axis):
    leaves = jax.tree.leaves(array)
    order = sorted(range(len(leaves)), key=lambda k: -leaves[k].size)
    width = (1, *leaves[order[0]].shape)[-1]
    lines = [
        jnp.pad(leaves[k].reshape(-1), (0, -leaves[k].size % width)).reshape(-1, width)
        for k in order
    ]
    both, at, found = (from_everyone(jnp.concatenate(lines), axis), 0, {})
    for k, line in zip(order, lines):
        slab = both[:, at : at + len(line)].reshape(len(both), -1)
        found[k] = slab[:, : leaves[k].size].reshape(-1, *leaves[k].shape)
        at += len(line)
    numbers = iter(range(len(leaves)))
    return jax.tree.map(lambda _: found[next(numbers)], array)


def folded_in_pairs(pieces, combine):
    while len(jax.tree.leaves(pieces)[0]) > 1:
        pieces = jax.vmap(combine)(
            *(jax.tree.map(lambda part: part[side::2], pieces) for side in (0, 1))
        )
    return jax.tree.map(lambda part: part[0], pieces)


def carried_in(array, axis, combine, identity, reverse):
    devices, mine = (lax.axis_size(axis), lax.axis_index(axis))
    passed = jnp.arange(devices) > mine if reverse else jnp.arange(devices) < mine

    def kept(part, zero, own):
        part = jnp.where(
            passed.reshape(-1, *(1 for _ in own.shape)),
            part.astype(own.dtype),
            jnp.asarray(zero, own.dtype),
        )
        return part[::-1] if reverse else part

    pieces = all_in_one(
        jax.tree.map(lambda part, kind: part.astype(kind), array, (jnp.bfloat16, jnp.bfloat16)),
        axis,
    )
    return folded_in_pairs(jax.tree.map(kept, pieces, identity, array), combine)


def cut_along(array, dim, devices):
    before, after = (array.shape[:dim], array.shape[dim + 1 :])
    return jnp.moveaxis(array.reshape(*before, devices, -1, *after), dim, 0)


def sent_and_summed(array, axis, dim):
    blocks = cut_along(array, dim, lax.axis_size(axis))
    arrived = lax.all_to_all(blocks, axis, split_axis=0, concat_axis=0, tiled=True)
    return arrived.astype(jnp.float32).sum(axis=0)


def rms_scale(values):
    return lax.rsqrt(jnp.mean(values * values, axis=-1, keepdims=True) + epsilon)


def span_scan(queries, taken, values, kept_log):
    head_count, length, key_dim = queries.shape
    blocks = length // BLOCK

    def to_blocks(tensor):
        return tensor.reshape(head_count, blocks, BLOCK, tensor.shape[-1]).transpose(1, 0, 2, 3)

    lower_mask = jnp.tril(jnp.ones((BLOCK, BLOCK), dtype=bool))[:, :, None]

    def advance(state_stack, pieces):
        query_block, key_block, value_block, g_blk = pieces
        cumulative_log = jnp.cumsum(g_blk, axis=1)
        across_blocks = jnp.einsum(
            "bqy,byo->bqo", query_block * jnp.exp(cumulative_log), state_stack
        )
        spread = cumulative_log[:, :, None, :] - cumulative_log[:, None, :, :]
        decays = jnp.where(lower_mask, jnp.exp(jnp.where(lower_mask, spread, 0.0)), 0.0)
        scores = jnp.einsum("hik,hijk->hij", query_block, decays * key_block[:, None, :, :])
        inside = jnp.einsum("hij,hjv->hiv", scores, value_block)
        final_log_decay = cumulative_log[:, -1:, :]
        carried = jnp.exp(final_log_decay[:, 0, :])[..., None] * state_stack
        fresh_portion = jnp.einsum(
            "moc,moa->mca", key_block * jnp.exp(final_log_decay - cumulative_log), value_block
        )
        return (carried + fresh_portion, across_blocks + inside)

    start_state = jnp.zeros((head_count, key_dim, values.shape[-1]), jnp.float32)
    final_state, outputs = lax.scan(
        advance,
        start_state,
        (to_blocks(queries), to_blocks(taken), to_blocks(values), to_blocks(kept_log)),
    )
    return (
        outputs.transpose(1, 0, 2, 3).reshape(head_count, length, values.shape[-1]),
        final_state,
    )


def chain_join(early_part, later_part):
    return (early_part[0] * later_part[0], later_part[0][..., None] * early_part[1] + later_part[1])


def key_width(row_count):
    for candidate in range(min(row_count, 1024), 0, -1):
        if row_count % candidate == 0:
            return candidate
    return 1


def shards(
    inputs,
    norm_gain,
    hg_query_w,
    hg_fwd_w,
    hg_bwd_w,
    hg_value_w,
    floor_gap,
    hg_norm_gain,
    df_query_w,
    df_key_w,
    df_value_w,
    diff_lambda,
    df_norm_gain,
    out_hg_w,
    out_df_w,
    post_gain,
):
    tok_rows = inputs[0]
    length = tok_rows.shape[0]
    rows_float = tok_rows.astype(jnp.float32)
    normed = (rows_float * rms_scale(rows_float) * norm_gain).astype(jnp.bfloat16)
    pieces = in_one_piece(
        (hg_query_w, hg_fwd_w, hg_bwd_w, hg_value_w, df_query_w, df_key_w, df_value_w),
        ("sp", "fs"),
        0,
        1,
    )
    summed = tuple((jnp.dot(normed, piece, preferred_element_type=jnp.float32) for piece in pieces))
    hg_query, hg_fwd, hg_bwd, hg_value, df_query, df_key, df_value = [
        member.astype(jnp.bfloat16) for member in summed
    ]
    heads_hg = hg_query.shape[1] // HEAD

    def split_heads(tensor):
        return tensor.astype(jnp.float32).reshape(length, heads_hg, HEAD).transpose(1, 0, 2)

    queries = jax.nn.silu(split_heads(hg_query))
    values = split_heads(hg_value)

    def summarize(raw_gate, gap_row, flipped):
        taken = gap_row.reshape(heads_hg, 1, HEAD) * jax.nn.sigmoid(-split_heads(raw_gate))
        series = (queries, taken, values, jnp.log1p(-taken))
        if flipped:
            series = tuple((jnp.flip(tensor, axis=1) for tensor in series))
        local_out, final_state = span_scan(*series)
        cumulative_log = jnp.cumsum(series[3], axis=1)
        return (
            local_out,
            final_state,
            jnp.exp(cumulative_log[:, -1, :]),
            series[0] * jnp.exp(cumulative_log),
        )

    forward_output, fwd_state, fwd_decay, forward_reader = summarize(hg_fwd, floor_gap[0], False)
    backward_output, bwd_state, bwd_decay, backward_reader = summarize(hg_bwd, floor_gap[1], True)
    identity = (jnp.ones_like(fwd_decay), jnp.zeros_like(fwd_state))
    forward_carry = carried_in((fwd_decay, fwd_state), "sp", chain_join, identity, False)[1]
    backward_carry = carried_in((bwd_decay, bwd_state), "sp", chain_join, identity, True)[1]
    forward_sum = forward_output + jnp.einsum("bqy,byo->bqo", forward_reader, forward_carry)
    bwd_total = jnp.flip(
        backward_output + jnp.einsum("bqy,byo->bqo", backward_reader, backward_carry), axis=1
    )
    recurrent = forward_sum + bwd_total
    hg_out = (
        (recurrent * rms_scale(recurrent) * hg_norm_gain)
        .transpose(1, 0, 2)
        .reshape(length, heads_hg * HEAD)
        .astype(jnp.bfloat16)
    )
    heads_df = df_value.shape[1] // DFV
    df_queries = df_query.reshape(length, heads_df, 2, DQK)
    score_scale = DQK ** (-0.5)
    start_carry = (
        jnp.full((heads_df, 2, length), -1e30, jnp.float32),
        jnp.zeros((heads_df, 2, length), jnp.float32),
        jnp.zeros((heads_df, 2, length, DFV), jnp.float32),
    )
    carry = start_carry
    key_rows, value_rows = in_one_piece((df_key, df_value), "sp", 0, 1)
    row_count = key_rows.shape[0]
    block_rows = key_width(row_count)
    key_blocks = key_rows.reshape(row_count // block_rows, block_rows, heads_df, 2, DQK)
    value_blocks = value_rows.reshape(row_count // block_rows, block_rows, heads_df, DFV)

    def key_step(running, block_pair):
        tops, totals, accums = running
        key_blk, value_blk = block_pair
        scores = (
            jnp.einsum("qhmd,khmd->hmqk", df_queries, key_blk, preferred_element_type=jnp.float32)
            * score_scale
        )
        new_tops = jnp.maximum(tops, jnp.max(scores, axis=-1))
        factor = jnp.exp(tops - new_tops)
        weights_blk = jnp.exp(scores - new_tops[..., None])
        totals = totals * factor + jnp.sum(weights_blk, axis=-1)
        accums = accums * factor[..., None] + jnp.einsum(
            "hmqk,khd->hmqd",
            weights_blk.astype(jnp.bfloat16),
            value_blk,
            preferred_element_type=jnp.float32,
        )
        return ((new_tops, totals, accums), None)

    carry, unused = lax.scan(key_step, carry, (key_blocks, value_blocks))
    tops, totals, accums = carry
    maps = accums / totals[..., None]
    weighted = maps[:, 0] - diff_lambda[:, None, None] * maps[:, 1]
    df_out = (
        (weighted * rms_scale(weighted) * df_norm_gain * df_factor)
        .transpose(1, 0, 2)
        .reshape(length, heads_df * DFV)
        .astype(jnp.bfloat16)
    )
    mixture = sent_and_summed(
        (
            jnp.dot(hg_out, out_hg_w, preferred_element_type=jnp.float32)
            + jnp.dot(df_out, out_df_w, preferred_element_type=jnp.float32)
        ).astype(jnp.bfloat16),
        "tp",
        0,
    )
    return (mixture * rms_scale(mixture) * post_gain).astype(jnp.bfloat16)[None]


def solution(mesh):
    in_specs = (
        P("fs", "sp", None),
        P(),
        P(("sp", "fs"), "tp"),
        P(("sp", "fs"), "tp"),
        P(("sp", "fs"), "tp"),
        P(("sp", "fs"), "tp"),
        P(None, "tp"),
        P(),
        P(("sp", "fs"), "tp"),
        P(("sp", "fs"), "tp"),
        P(("sp", "fs"), "tp"),
        P("tp"),
        P(),
        P("tp", None),
        P("tp", None),
        P(),
    )
    out_specs = P("fs", ("sp", "tp"), None)
    return jax.shard_map(shards, mesh=mesh, in_specs=in_specs, out_specs=out_specs, check_vma=False)
```

profile of v0, /device:TPU:1, one launch (start us, length us, event | category | flops | bytes accessed | tf_op | source)
XLA Modules:
  0.0 296.0 jit_solution(6876685553226303031)
XLA Ops:
  6.5 1.6 concatenate.12
  8.8 0.8 slice_reduce_fusion.1
  9.8 1.2 fusion.80
  11.0 139.0 %all-gather.2.cloned.1.call-done = bf16[2048,704]{1,0:T(8,128)(2,1)} async-done(((bf16[32,704]{1,0:T(8,128)(2,1)}), bf16[2048,704]{1,0:T(8,128)(2,1)}) %all-gather.2.cloned.1.call-update) | async-done | bytes 2883600 | tf_op jit(solution)/shard_map/all_gather | solution.py:22
  150.0 1.6 convolution_convert_fusion.2
  151.7 0.1 reshape.352
  151.9 1.6 fusion.75
  154.1 1.5 fusion.79
  155.9 0.1 reshape.358
  156.0 1.4 convolution_convert_fusion.1
  157.8 0.5 copy-done.5
  158.4 0.2 reduce_window_sum.35
  158.7 0.5 copy-done.1
  159.2 6.6 %while.45 = (s32[]{:T(128)}, f32[2,64,64]{2,1,0:T(8,128)S(1)}, f32[2,2,64,64]{3,2,1,0:T(8,128)S(1)}, f32[2,2,64,64]{2,0,3,1:T(2,128)S(1)}, f32[2,2,64,64]{2,0,3,...) while((s32[]{:T(128)}, f32[2,64,64]{2,1,0:T(8,128)S(1)}, ...), condition=%wide.region_7.8_spmd.clone.clone, body=%wide.region_5.7_spmd.clone.clone.sunk | while | flops 6877187 | bytes 1158284 | solution.py:118
  159.6 0.1 fusion.194
  159.9 2.2 fusion.196
  162.2 0.2 convolution_add_fusion.10
  162.9 0.1 fusion.194
  163.2 2.2 fusion.196
  165.5 0.2 convolution_add_fusion.10
  166.0 0.5 copy-done.7
  166.5 6.6 %while.44 = (s32[]{:T(128)}, f32[2,64,64]{2,1,0:T(8,128)S(1)}, f32[2,2,64,64]{3,2,1,0:T(8,128)S(1)}, f32[2,2,64,64]{2,0,3,1:T(2,128)S(1)}, f32[2,2,64,64]{2,0,3,...) while((s32[]{:T(128)}, f32[2,64,64]{2,1,0:T(8,128)S(1)}, ...), condition=%wide.region_3.4_spmd.clone.clone, body=%wide.region_1.3_spmd.clone.clone.sunk | while | flops 6877187 | bytes 1158284 | solution.py:118
  166.8 0.1 fusion.183
  167.0 0.1 constant_dynamic-slice_fusion.14
  167.2 2.2 fusion.185
  169.4 0.2 convolution_add_fusion.9
  170.2 0.1 fusion.183
  170.5 2.2 fusion.185
  172.8 0.2 convolution_add_fusion.9
  173.2 0.9 broadcast_in_dim.137
  174.0 6.6 %all-to-all-start.1 = ((bf16[16,130,64]{1,2,0:T(8,128)(2,1)}), bf16[16,130,64]{1,2,0:T(8,128)(2,1)S(1)}, u32[]{:S(2)}, u32[]{:S(2)}) async-start(bf16[16,130,64]{1,2,0:T(8,128)(2,1)} %broadcast_in_dim.137), calls=%async_computation.1 | async-start | bytes 1048576 | tf_op jit(solution)/shard_map/all_to_all | solution.py:27
  180.6 1.5 convolution_convert_fusion.5
  182.1 1.7 convolution_convert_fusion.6
  183.8 38.9 %all_gather.7 = bf16[2048,128]{0,1:T(8,128)(2,1)S(1)} all-gather(bf16[128,128]{0,1:T(8,128)(2,1)S(1)} %pad_maximum_fusion.2), channel_id=1, replica_groups=mesh['sp'=16,'fs'=4,'tp'=8] {'sp'}, dimensions={0}, use_global_device_ids=true | all-gather | bytes 557056 | tf_op jit(solution)/shard_map/all_gather | solution.py:22
  222.8 0.2 reshape.365
  223.0 0.2 reshape.363
  223.3 1.4 convolution_convert_fusion.4
  224.7 1.8 while.43
  224.7 0.4 fusion.172
  225.1 0.2 fusion.174
  225.3 0.3 fusion.175
  225.6 0.4 fusion.172
  226.0 0.2 fusion.174
  226.2 0.3 fusion.175
  226.6 0.2 reduce_window_sum.34
  227.0 0.8 reshape.361
  227.9 0.8 reshape.355
  228.9 0.8 broadcast_in_dim.132
  229.7 10.6 %all-to-all-start = ((bf16[16,130,64]{1,2,0:T(8,128)(2,1)}), bf16[16,130,64]{1,2,0:T(8,128)(2,1)S(1)}, u32[]{:S(2)}, u32[]{:S(2)}) async-start(bf16[16,130,64]{1,2,0:T(8,128)(2,1)} %broadcast_in_dim.132), calls=%async_computation | async-start | bytes 1048576 | tf_op jit(solution)/shard_map/all_to_all | solution.py:27
  240.5 0.7 slice_multiply_fusion.1
  241.2 0.7 fusion.129
  241.9 0.6 reshape.373
  242.6 0.2 copy_select_fusion
  243.4 0.2 copy-done.2
  243.7 0.2 convolution_add_fusion.5
  243.9 13.3 %all-to-all-done = bf16[16,130,64]{1,2,0:T(8,128)(2,1)S(1)} async-done(((bf16[16,130,64]{1,2,0:T(8,128)(2,1)}), bf16[16,130,64]{1,2,0:T(8,128)(2,1)S(1)}, u32[]{:S(2)}, u32[]{:S(2)}) %all-to-all-start) | async-done | bytes 266272 | tf_op jit(solution)/shard_map/all_to_all | solution.py:27
  257.7 0.1 copy.70
  257.9 0.6 reshape.372
  258.5 0.2 copy_select_fusion.1
  258.9 0.2 multiply_reduce_fusion.1
  259.3 0.3 fusion.130
  259.7 0.4 fusion.70
  260.1 28.1 %all_to_all.15 = bf16[8,16,2048]{2,1,0:T(8,128)(2,1)S(1)} all-to-all(bf16[8,16,2048]{2,1,0:T(8,128)(2,1)S(1)} %bitcast.287), channel_id=1, replica_groups=mesh['sp'=16,'fs'=4,'tp'=8] {'tp'}, dimensions={0} | all-to-all | bytes 1048576 | tf_op jit(solution)/shard_map/all_to_all | solution.py:83
  288.4 0.7 fusion.91
  (170 shorter events, 7.0 us)
Async XLA Ops:
  6.5 252.8 %copy-start = (bf16[128,2048]{1,0:T(8,128)(2,1)S(1)}, bf16[128,2048]{1,0:T(8,128)(2,1)}, u32[]{:S(2)}) copy-start(bf16[128,2048]{1,0:T(8,128)(2,1)} %param.35) | copy-start | bytes 1572868
  6.5 147.6 %copy-start.3 = (bf16[1,128,2048]{2,1,0:T(8,128)(2,1)S(1)}, bf16[1,128,2048]{2,1,0:T(8,128)(2,1)}, u32[]{:S(2)}) copy-start(bf16[1,128,2048]{2,1,0:T(8,128)(2,1)} %param.22) | copy-start | bytes 1572868
  6.5 147.6 %copy-start.22 = (f32[2048]{0:T(1024)S(1)}, f32[2048]{0:T(1024)}, u32[]{:S(2)}) copy-start(f32[2048]{0:T(1024)} %param.23) | copy-start | bytes 24580
  6.5 143.5 %all-gather.2.cloned.1.call-start = ((), (), s32[]{:S(2)}) async-start(), calls=%async_computation.3 | async-start | bytes 3194880 | tf_op jit(solution)/shard_map/all_gather | solution.py:22
  157.6 0.7 copy-start.5
  158.6 0.7 copy-start.1
  165.9 0.7 copy-start.7
  174.0 54.8 %all-to-all-start.1 = ((bf16[16,130,64]{1,2,0:T(8,128)(2,1)}), bf16[16,130,64]{1,2,0:T(8,128)(2,1)S(1)}, u32[]{:S(2)}, u32[]{:S(2)}) async-start(bf16[16,130,64]{1,2,0:T(8,128)(2,1)} %broadcast_in_dim.137), calls=%async_computation.1 | async-start | bytes 1048576 | tf_op jit(solution)/shard_map/all_to_all | solution.py:27
  180.6 42.7 %copy-start.4 = (bf16[1,128,2048]{2,1,0:T(8,128)(2,1)S(1)}, bf16[1,128,2048]{2,1,0:T(8,128)(2,1)}, u32[]{:S(2)}) copy-start(bf16[1,128,2048]{2,1,0:T(8,128)(2,1)} %param.22) | copy-start | bytes 1572868
  224.7 2.2 copy-start.8
  226.8 2.9 copy-start.16
  228.8 0.9 copy-start.10
  229.7 27.5 %all-to-all-start = ((bf16[16,130,64]{1,2,0:T(8,128)(2,1)}), bf16[16,130,64]{1,2,0:T(8,128)(2,1)S(1)}, u32[]{:S(2)}, u32[]{:S(2)}) async-start(bf16[16,130,64]{1,2,0:T(8,128)(2,1)} %broadcast_in_dim.132), calls=%async_computation | async-start | bytes 1048576 | tf_op jit(solution)/shard_map/all_to_all | solution.py:27
  241.9 0.9 copy-start.12
  241.9 0.9 copy-start.15
  241.9 1.2 copy-start.9
  242.7 0.9 copy-start.2
  242.7 0.9 copy-start.13
  257.9 1.0 copy-start.6
  257.9 1.0 copy-start.17
  257.9 1.0 copy-start.18
  258.5 0.7 copy-start.20
  258.7 0.9 copy-start.11
  258.7 1.0 copy-start.14
  258.7 1.0 copy-start.21
  258.9 29.5 %copy-start.19 = (f32[2048]{0:T(1024)S(1)}, f32[2048]{0:T(1024)}, u32[]{:S(2)}) copy-start(f32[2048]{0:T(1024)} %param.37) | copy-start | bytes 24580
Sparse Core Ops, SparseCore 0:
  10.3 139.7 all-gather.1
where the time goes:
time: 297 us; the launch traced here: 296 us
  waiting for transfers between devices  152 us (51%)
  blocking collectives  67 us (23%)
  matrix products  24.1 us (8%)
  starting transfers between devices  17.2 us (6%)
  between operations  14.9 us (5%)
  local copies, waits for them, and re-layouts  14.7 us (5%)
  other arithmetic  5.48 us (2%)
    all_gather x1, waiting for transfers between devices, in_one_piece(): lax.all_gather(both, axis, axis=dim, tiled=True)  139 us
    all_gather x1, blocking collectives, in_one_piece(): lax.all_gather(both, axis, axis=dim, tiled=True)  38.9 us
    all_to_all x1, blocking collectives, sent_and_summed(): lax.all_to_all(blocks, axis, split_axis=0, concat_axis=0, tiled=True)  28.1 us
    all_to_all x2, starting transfers between devices, from_everyone(): lax.all_to_all(jnp.broadcast_to(array[None], (devices, *array.shape)), ax...  17.2 us
    all_to_all x2, waiting for transfers between devices, from_everyone(): lax.all_to_all(jnp.broadcast_to(array[None], (devices, *array.shape)), ax...  13.3 us
    dot_general x7, matrix products, shards(): jnp.dot(normed, piece, preferred_element_type=jnp.float32)  10.7 us
    dot_general x4, matrix products, advance(): jnp.einsum('hik,hijk->hij', query_block, decays * key_block[:, None, :, :])  8.96 us
  transfers between devices with their start and end apart: 3, of which 2 were waited for; matrix products, arithmetic and copies ran while one was open for 5% of the time, Pallas kernels for 0%

commit v1 on v0

v1 whole, which is shorter than its diff:
```python
import functools

import jax
import jax.numpy as jnp
from jax import lax
from jax.experimental import pallas as pl
from jax.experimental.pallas import tpu as pltpu
from jax.sharding import PartitionSpec as P

HEAD = 64
DQK = 32
LANES = 128
STATE_ROWS = 80

epsilon = 1e-06
df_factor = 0.8
f32 = jnp.float32
bf16 = jnp.bfloat16

SMEM_SPEC = pl.BlockSpec(memory_space=pltpu.SMEM)


def dot(a, b, dims, precision=None):
    return lax.dot_general(a, b, (dims, ((), ())), precision=precision, preferred_element_type=f32)


def pack_kernel(q, f, b, v, dq, dk, dv, out):
    copies, _, rows, _ = out.shape
    depth = q.shape[0]
    half = depth // 2
    for j, (wide, narrow) in enumerate(((q, dq), (f, dk), (b, dv), (v, dq))):
        folded = jnp.concatenate([narrow[:half, :], narrow[half:, :]], axis=1)
        block = jnp.concatenate([wide[...], folded], axis=0)
        for c in range(copies):
            out[c, j] = block


def norm_kernel(x, gain, out):
    rows = x[0].astype(f32)
    scale = lax.rsqrt(jnp.mean(rows * rows, axis=-1, keepdims=True) + epsilon)
    out[...] = (rows * scale * gain[...]).astype(bf16)


def project_kernel(places, own, before, after, far_top, far_low, weights, out, rhs):
    blocks, packed, _ = weights.shape
    depth = packed * 2 // 3
    half = depth // 2
    wide = weights[:, :depth, :]
    narrow = weights[:, depth:, :].astype(f32)
    first, second = narrow[:, :, :HEAD], narrow[:, :, HEAD:]
    narrow = jnp.concatenate(
        [
            jnp.concatenate([first, first], axis=2),
            jnp.concatenate([second, second], axis=2),
        ],
        axis=1,
    ).astype(bf16)
    rhs[:, :LANES] = wide.reshape(blocks * depth, LANES)
    rhs[:, LANES:] = narrow.reshape(blocks * depth, LANES)
    top = far_top.shape[0]
    for k, rows in enumerate((own, before, after)):
        out[places[k]] = dot(rows[...], rhs[...], ((1,), (0,))).astype(bf16)
    out[places[3], :top] = dot(far_top[...], rhs[...], ((1,), (0,))).astype(bf16)
    out[places[3], top:] = dot(far_low[...], rhs[...], ((1,), (0,))).astype(bf16)


def local_kernel(place, got, gaps, message, local, read_fwd, read_bwd):
    length = got.shape[1]
    devices = message.shape[0]
    me = place[0]
    row = lax.broadcasted_iota(jnp.int32, (length, length), 0)
    col = lax.broadcasted_iota(jnp.int32, (length, length), 1)
    lane = lax.broadcasted_iota(jnp.int32, (length, LANES), 1)
    lane_head = lax.broadcasted_iota(jnp.int32, (HEAD, LANES), 1)
    lower, upper = row >= col, row <= col
    queries = got[0, :, :LANES].astype(f32)
    queries = queries * jax.nn.sigmoid(queries)
    values = got[3, :, :LANES]
    pieces = []
    for j, mask in ((1, lower), (2, upper)):
        gate = got[j, :, :LANES].astype(f32)
        taken = gaps[j - 1 : j, :] * jax.nn.sigmoid(-gate)
        kept = jnp.log1p(-taken)
        gone = dot(mask.astype(f32), kept, ((1,), (0,)), lax.Precision.HIGHEST)
        total = gone[length - 1 : length] if j == 1 else gone[0:1]
        middle = gone[length // 2 : length // 2 + 1]
        decay = jnp.exp(total)
        state = dot(
            values, (taken * jnp.exp(total - gone)).astype(bf16), ((0,), (0,))
        )
        state = jnp.where(lane_head < HEAD, state[:HEAD], state[HEAD:])
        reader = read_fwd if j == 1 else read_bwd
        reader[...] = (queries * jnp.exp(gone)).astype(bf16)
        high = decay.astype(bf16)
        low = (decay - high.astype(f32)).astype(bf16)
        pieces.append((state.astype(bf16), high, low))
        query_part = queries * jnp.exp(gone - middle)
        key_part = (taken * jnp.exp(middle - gone)).astype(bf16)
        for h in range(2):
            inside = (lane >= h * HEAD) & (lane < (h + 1) * HEAD)
            score = dot(
                jnp.where(inside, query_part, 0.0).astype(bf16), key_part, ((1,), (1,))
            )
            pieces.append(jnp.where(mask, score, 0.0))
    (fwd, fwd_0, fwd_1, bwd, bwd_0, bwd_1) = pieces
    out_0 = dot((fwd_0 + bwd_0).astype(bf16), values, ((1,), (0,)))
    out_1 = dot((fwd_1 + bwd_1).astype(bf16), values, ((1,), (0,)))
    local[...] = jnp.where(lane < HEAD, out_0, out_1)
    keys_values = jnp.where(lane < HEAD, got[1, :, LANES:], got[2, :, LANES:])
    spare = STATE_ROWS - HEAD
    row_spare = lax.broadcasted_iota(jnp.int32, (spare, LANES), 0)

    def tail(piece):
        high = jnp.broadcast_to(piece[1].astype(f32), (spare, LANES))
        low = jnp.broadcast_to(piece[2].astype(f32), (spare, LANES))
        return jnp.where(row_spare == 0, high, low).astype(bf16)

    tails = tail(fwd), tail(bwd)
    for d in range(devices):
        message[d, :length] = keys_values

        @pl.when(d > me)
        def _():
            message[d, length : length + HEAD] = fwd[0]
            message[d, length + HEAD :] = tails[0]

        @pl.when(d <= me)
        def _():
            message[d, length : length + HEAD] = bwd[0]
            message[d, length + HEAD :] = tails[1]


def finish_kernel(
    place, lam, got, df_query, local, read_fwd, read_bwd, hg_gain, df_gain, hg_w, df_w, out, mixed
):
    devices = got.shape[0]
    length = local.shape[0]
    me = place[0]
    lane = lax.broadcasted_iota(jnp.int32, (length, LANES), 1)

    def folded(order, passed):
        state = jnp.zeros((HEAD, LANES), f32)
        for w in order:
            fresh = got[w, length : length + HEAD].astype(f32)
            tail = got[w, length + HEAD :].astype(f32)
            decay = tail[0:1] + tail[1:2]
            state = jnp.where(passed(w), decay * state + fresh, state)
        return state.astype(bf16)

    fwd = folded(range(devices), lambda w: w < me)
    bwd = folded(range(devices - 1, -1, -1), lambda w: w > me)
    recurrent = local[...]
    parts = []
    for h in range(2):
        inside = (lane >= h * HEAD) & (lane < (h + 1) * HEAD)
        zero = jnp.zeros((length, LANES), bf16)
        parts.append(
            dot(jnp.where(inside, read_fwd[...], zero), fwd, ((1,), (1,)))
            + dot(jnp.where(inside, read_bwd[...], zero), bwd, ((1,), (1,)))
        )
    recurrent = recurrent + jnp.concatenate(parts, axis=1)
    squares = recurrent * recurrent
    first = jnp.sum(jnp.where(lane < HEAD, squares, 0.0), axis=1, keepdims=True)
    second = jnp.sum(jnp.where(lane < HEAD, 0.0, squares), axis=1, keepdims=True)
    mean = jnp.where(lane < HEAD, first, second) * (1.0 / HEAD)
    mixed[:, :LANES] = (recurrent * lax.rsqrt(mean + epsilon) * hg_gain[...]).astype(bf16)

    step = 64
    keys_values = got[:, :length, :].reshape(devices * length, LANES)
    lane_step = lax.broadcasted_iota(jnp.int32, (step, LANES), 1)
    lam_value = lam[0]

    def attend(i, carry):
        rows = pl.ds(pl.multiple_of(i * step, step), step)
        query = df_query[rows, :]
        maps = []
        for m in range(2):
            inside = (lane_step >= m * DQK) & (lane_step < (m + 1) * DQK)
            only = jnp.where(inside, query, jnp.zeros_like(query))
            scores = dot(only, keys_values, ((1,), (1,))) * (DQK ** (-0.5))
            shifted = jnp.exp(scores - jnp.max(scores, axis=-1, keepdims=True))
            totals = jnp.sum(shifted, axis=-1, keepdims=True)
            maps.append(dot(shifted.astype(bf16), keys_values, ((1,), (0,))) / totals)
        weighted = (maps[0] - lam_value * maps[1])[:, HEAD:]
        mean = jnp.mean(weighted * weighted, axis=-1, keepdims=True)
        normed = (weighted * lax.rsqrt(mean + epsilon) * df_gain[...] * df_factor).astype(bf16)
        mixed[rows, LANES : LANES + HEAD] = normed
        return carry

    lax.fori_loop(0, length // step, attend, 0)
    out[...] = (
        dot(mixed[:, :LANES], hg_w[...], ((1,), (0,)))
        + dot(mixed[:, LANES : LANES + HEAD], df_w[...], ((1,), (0,)))
    ).astype(bf16)


def close_kernel(parts, gain, out):
    mixture = parts[0].astype(f32)
    for k in range(1, parts.shape[0]):
        mixture = mixture + parts[k].astype(f32)
    scale = lax.rsqrt(jnp.mean(mixture * mixture, axis=-1, keepdims=True) + epsilon)
    out[0] = (mixture * scale * gain[...]).astype(bf16)


def shards(
    inputs,
    norm_gain,
    hg_query_w,
    hg_fwd_w,
    hg_bwd_w,
    hg_value_w,
    floor_gap,
    hg_norm_gain,
    df_query_w,
    df_key_w,
    df_value_w,
    diff_lambda,
    df_norm_gain,
    out_hg_w,
    out_df_w,
    post_gain,
):
    sp, fs, tp = (lax.axis_size(a) for a in ("sp", "fs", "tp"))
    z, y = lax.axis_index("sp"), lax.axis_index("fs")
    _, length, width = inputs.shape
    depth = hg_query_w.shape[0]
    packed = depth + depth // 2

    sent = pl.pallas_call(
        pack_kernel,
        out_shape=jax.ShapeDtypeStruct((sp, fs, packed, LANES), bf16),
        name="pack",
    )(hg_query_w, hg_fwd_w, hg_bwd_w, hg_value_w, df_query_w, df_key_w, df_value_w)
    weights = lax.all_to_all(
        sent.reshape(sp * fs, packed, LANES), ("sp", "fs"), 0, 0, tiled=True
    )

    normed = pl.pallas_call(
        norm_kernel,
        out_shape=jax.ShapeDtypeStruct((length, width), bf16),
        name="norm",
    )(inputs, norm_gain[None])

    def shifted(array, by):
        return lax.ppermute(array, "fs", [(i, (i + by) % fs) for i in range(fs)])

    before = shifted(normed, 1)
    after = shifted(normed, -1)
    far_top = shifted(before[: length // 2], 1)
    far_low = shifted(after[length // 2 :], -1)
    places = jnp.stack([y, (y + fs - 1) % fs, (y + 1) % fs, (y + 2) % fs]).astype(jnp.int32)
    vmem = pl.BlockSpec(memory_space=pltpu.VMEM)
    projected = pl.pallas_call(
        project_kernel,
        in_specs=[SMEM_SPEC] + [vmem] * 6,
        out_specs=vmem,
        out_shape=jax.ShapeDtypeStruct((fs, length, 2 * LANES), bf16),
        scratch_shapes=[pltpu.VMEM((width, 2 * LANES), bf16)],
        name="project",
    )(places, normed, before, after, far_top, far_low, weights)
    got = lax.all_to_all(projected, "fs", 0, 0, tiled=True)

    place = z.astype(jnp.int32)[None]
    message, local, read_fwd, read_bwd = pl.pallas_call(
        local_kernel,
        in_specs=[SMEM_SPEC] + [vmem] * 2,
        out_specs=[vmem] * 4,
        out_shape=[
            jax.ShapeDtypeStruct((sp, length + STATE_ROWS, LANES), bf16),
            jax.ShapeDtypeStruct((length, LANES), f32),
            jax.ShapeDtypeStruct((length, LANES), bf16),
            jax.ShapeDtypeStruct((length, LANES), bf16),
        ],
        name="local",
    )(place, got, floor_gap)
    arrived = lax.all_to_all(message, "sp", 0, 0, tiled=True)
    partial = pl.pallas_call(
        finish_kernel,
        in_specs=[SMEM_SPEC] * 2 + [vmem] * 9,
        out_specs=vmem,
        out_shape=jax.ShapeDtypeStruct((length, width), bf16),
        scratch_shapes=[pltpu.VMEM((length, 2 * LANES), bf16)],
        name="finish",
    )(
        place,
        diff_lambda,
        arrived,
        got[0, :, LANES:],
        local,
        read_fwd,
        read_bwd,
        jnp.concatenate([hg_norm_gain, hg_norm_gain])[None],
        df_norm_gain[None],
        out_hg_w,
        out_df_w,
    )
    parts = lax.all_to_all(
        partial.reshape(tp, length // tp, width), "tp", 0, 0, tiled=True
    )
    return pl.pallas_call(
        close_kernel,
        out_shape=jax.ShapeDtypeStruct((1, length // tp, width), bf16),
        name="close",
    )(parts, post_gain[None])


def solution(mesh):
    rows = P(("sp", "fs"), "tp")
    in_specs = (
        P("fs", "sp", None),
        P(),
        rows,
        rows,
        rows,
        rows,
        P(None, "tp"),
        P(),
        rows,
        rows,
        rows,
        P("tp"),
        P(),
        P("tp", None),
        P("tp", None),
        P(),
    )
    out_specs = P("fs", ("sp", "tp"), None)
    return jax.shard_map(shards, mesh=mesh, in_specs=in_specs, out_specs=out_specs, check_vma=False)
```

time: 297 us -> 151 us (0.51)
  waiting for transfers between devices: 152 us -> 63.1 us
  blocking collectives: 67 us -> 20.2 us
  starting transfers between devices: 17.2 us -> 42.2 us
  matrix products: 24.1 us -> 0 us
  Pallas kernels: 0 us -> 18.2 us
  between operations: 14.9 us -> 0.81 us
  local copies, waits for them, and re-layouts: 14.7 us -> 3.94 us
  other arithmetic: 5.48 us -> 1.32 us
    all_gather x1 -> x0, waiting for transfers between devices: 139 us -> none  [in_one_piece(): lax.all_gather(both, axis, axis=dim, tiled=True)]
    all_gather x1 -> x0, blocking collectives: 38.9 us -> none  [in_one_piece(): lax.all_gather(both, axis, axis=dim, tiled=True)]
    all_to_all x2 -> x3, waiting for transfers between devices: 13.3 us -> 44.6 us  [the longest x1 32.6 us: shards(): arrived = lax.all_to_all(message, 'sp', 0, 0, tiled=True)]
    dot_general x31 -> x0, matrix products: 24.1 us -> none  [the longest x7 10.7 us: shards(): jnp.dot(normed, piece, preferred_element_type=jnp.float32)]
    ppermute x0 -> x4, waiting for transfers between devices: none -> 18.5 us  [shifted(): return lax.ppermute(array, 'fs', [(i, (i + by) % fs) for i in range(fs)])]
    pallas_call x0 -> x6, Pallas kernels: none -> 18.2 us  [the longest x1 5.89 us: shards(): pl.pallas_call(finish_kernel, in_specs=[SMEM_SPEC] * 2 + [vmem] * 9, out_...]
    ppermute x0 -> x4, starting transfers between devices: none -> 13 us  [shifted(): return lax.ppermute(array, 'fs', [(i, (i + by) % fs) for i in range(fs)])]
    all_to_all x2 -> x3, starting transfers between devices: 17.2 us -> 29.2 us  [the longest x1 19.3 us: shards(): lax.all_to_all(sent.reshape(sp * fs, packed, LANES), ('sp', 'fs'), 0, 0,...]
  transfers between devices with their start and end apart: 3 -> 7, of which waited for: 2 -> 5; matrix products, arithmetic and copies ran while one was open for 5% -> 2% of each run, Pallas kernels for 0% -> 1%
where the time goes in v1:
time: 151 us; the launch traced here: 150 us
  waiting for transfers between devices  63.1 us (42%)
  starting transfers between devices  42.2 us (28%)
  blocking collectives  20.2 us (13%)
  Pallas kernels  18.2 us (12%)
  local copies, waits for them, and re-layouts  3.94 us (3%)
    all_to_all x1, waiting for transfers between devices, shards(): arrived = lax.all_to_all(message, 'sp', 0, 0, tiled=True)  32.6 us
    all_to_all x1, blocking collectives, shards(): lax.all_to_all(partial.reshape(tp, length // tp, width), 'tp', 0, 0, tile...  20.2 us
    all_to_all x1, starting transfers between devices, shards(): lax.all_to_all(sent.reshape(sp * fs, packed, LANES), ('sp', 'fs'), 0, 0,...  19.3 us
    ppermute x4, waiting for transfers between devices, shifted(): return lax.ppermute(array, 'fs', [(i, (i + by) % fs) for i in range(fs)])  18.5 us
    ppermute x4, starting transfers between devices, shifted(): return lax.ppermute(array, 'fs', [(i, (i + by) % fs) for i in range(fs)])  13 us
    all_to_all x1, waiting for transfers between devices, shards(): lax.all_to_all(sent.reshape(sp * fs, packed, LANES), ('sp', 'fs'), 0, 0,...  6.45 us
    pallas_call x1, Pallas kernels, shards(): pl.pallas_call(finish_kernel, in_specs=[SMEM_SPEC] * 2 + [vmem] * 9, out_...  5.89 us
    all_to_all x1, starting transfers between devices, shards(): got = lax.all_to_all(projected, 'fs', 0, 0, tiled=True)  5.59 us
  transfers between devices with their start and end apart: 7, of which 5 were waited for; matrix products, arithmetic and copies ran while one was open for 2% of the time, Pallas kernels for 1%

profile of v1, /device:TPU:1, one launch (start us, length us, event | category | flops | bytes accessed | tf_op | source)
XLA Modules:
  0.0 149.7 jit_solution(12635507828039840292)
XLA Ops:
  0.0 1.8 %pack.1 = bf16[16,4,48,128]{3,2,1,0:T(8,128)(2,1)} custom-call(bf16[32,128]{1,0:T(8,128)(2,1)} %q.1, bf16[32,128]{1,0:T(8,128)(2,1)} %f.1, bf16[32,128]{1,0:T(8,128)(2,1)} %b.1, bf16[32,128]{1,0:T(8,128)(2,1)} %v.1, bf16[32,64]{1,0:T(8,128)(2,1)} %dq.1, bf16[32,64]{1,0:T(8,128)(2,1)} %dk.1, bf16[32,64]{1,0:T(8,128)(2,1)} %dv.1), custom_call_target="tpu_custom_call" | custom-call | tf_op jit(solution)/shard_map/pack/pallas_call | solution.py:229
  1.8 19.3 %all-to-all-start = ((bf16[64,48,128]{2,1,0:T(8,128)(2,1)}), bf16[64,48,128]{2,1,0:T(8,128)(2,1)S(1)}, u32[]{:S(2)}, u32[]{:S(2)}) async-start(bf16[64,48,128]{2,1,0:T(8,128)(2,1)} %bitcast.14), calls=%async_computation | async-start | bytes 1572864 | tf_op jit(solution)/shard_map/all_to_all | solution.py:234
  21.1 2.1 %norm.1.own = bf16[128,2048]{1,0:T(8,128)(2,1)} custom-call(bf16[1,128,2048]{2,1,0:T(8,128)(2,1)} %x.1, f32[1,2048]{1,0:T(1,128)} %bitcast.16), custom_call_target="tpu_custom_call" | custom-call | tf_op jit(solution)/shard_map/norm/pallas_call | solution.py:238
  23.1 2.9 %collective-permute-start = (bf16[128,2048]{1,0:T(8,128)(2,1)}, bf16[128,2048]{1,0:T(8,128)(2,1)S(1)}, u32[]{:S(2)}, u32[]{:S(2)}) collective-permute-start(bf16[128,2048]{1,0:T(8,128)(2,1)} %norm.1.own), channel_id=1, source_target_pairs={{0,8},{8,16},{16,24},{24,0},{1,9},{9,17},{17,25},{25,1},{2,10},{10... | collective-permute-start | bytes 1572872 | tf_op jit(solution)/shard_map/ppermute | solution.py:245
  26.1 3.6 %collective-permute-start.1 = (bf16[128,2048]{1,0:T(8,128)(2,1)}, bf16[128,2048]{1,0:T(8,128)(2,1)S(1)}, u32[]{:S(2)}, u32[]{:S(2)}) collective-permute-start(bf16[128,2048]{1,0:T(8,128)(2,1)} %norm.1.own), channel_id=1, source_target_pairs={{0,24},{8,0},{16,8},{24,16},{1,25},{9,1},{17,9},{25,17},{2,26},{10... | collective-permute-start | bytes 1572872 | tf_op jit(solution)/shard_map/ppermute | solution.py:245
  29.6 13.7 %collective-permute-done.before = bf16[128,2048]{1,0:T(8,128)(2,1)S(1)} collective-permute-done((bf16[128,2048]{1,0:T(8,128)(2,1)}, bf16[128,2048]{1,0:T(8,128)(2,1)S(1)}, u32[]{:S(2)}, u32[]{:S(2)}) %collective-permute-start) | collective-permute-done | bytes 524320 | tf_op jit(solution)/shard_map/ppermute | solution.py:245
  43.3 0.0 copy-start.3
  43.4 1.9 %collective-permute-start.2 = (bf16[64,2048]{1,0:T(8,128)(2,1)S(1)}, bf16[64,2048]{1,0:T(8,128)(2,1)S(1)}, u32[]{:S(2)}, u32[]{:S(2)}) collective-permute-start(bf16[64,2048]{1,0:T(8,128)(2,1)S(1)} %slice.12), channel_id=1, source_target_pairs={{0,8},{8,16},{16,24},{24,0},{1,9},{9,17},{17,25},{25,1},{2,10},{10... | collective-permute-start | bytes 786440 | tf_op jit(solution)/shard_map/ppermute | solution.py:245
  45.3 0.0 collective-permute-done.1.after
  45.3 0.0 copy-start.4
  45.3 0.0 copy-done.3
  45.3 4.6 %collective-permute-start.3 = (bf16[64,2048]{1,0:T(8,128)(2,1)S(1)}, bf16[64,2048]{1,0:T(8,128)(2,1)S(1)}, u32[]{:S(2)}, u32[]{:S(2)}) collective-permute-start(bf16[64,2048]{1,0:T(8,128)(2,1)S(1)} %slice.13), channel_id=1, source_target_pairs={{0,24},{8,0},{16,8},{24,16},{1,25},{9,1},{17,9},{25,17},{2,26},{10... | collective-permute-start | bytes 786440 | tf_op jit(solution)/shard_map/ppermute | solution.py:245
  50.0 0.7 pad_add_fusion.places
  50.6 4.8 %collective-permute-done.2.far_top = bf16[64,2048]{1,0:T(8,128)(2,1)S(1)} collective-permute-done((bf16[64,2048]{1,0:T(8,128)(2,1)S(1)}, bf16[64,2048]{1,0:T(8,128)(2,1)S(1)}, u32[]{:S(2)}, u32[]{:S(2)}) %collective-permute-start.2) | collective-permute-done | bytes 262176 | tf_op jit(solution)/shard_map/ppermute | solution.py:245
  55.4 0.0 copy-start.5
  55.4 0.0 collective-permute-done.3.far_low
  55.4 0.0 copy-start.6
  55.4 6.5 %all-to-all-done.weights = bf16[64,48,128]{2,1,0:T(8,128)(2,1)S(1)} async-done(((bf16[64,48,128]{2,1,0:T(8,128)(2,1)}), bf16[64,48,128]{2,1,0:T(8,128)(2,1)S(1)}, u32[]{:S(2)}, u32[]{:S(2)}) %all-to-all-start) | async-done | bytes 786464 | tf_op jit(solution)/shard_map/all_to_all | solution.py:234
  61.9 0.0 copy-done.4
  61.9 0.0 copy-done.5
  61.9 0.0 copy-done.6
  61.9 0.0 copy-start.1
  61.9 0.9 copy-done.1
  62.8 3.5 %project.1 = bf16[4,128,256]{2,1,0:T(8,128)(2,1)} custom-call(s32[4]{0:T(128)} %pad_add_fusion.places, bf16[128,2048]{1,0:T(8,128)(2,1)} %norm.1.own, bf16[128,2048]{1,0:T(8,128)(2,1)} %copy-done.3, bf16[128,2048]{1,0:T(8,128)(2,1)} %copy-done.4, bf16[64,2048]{1,0:T(8,128)(2,1)} %copy-done.5, bf16[64,2048]{1,0:T(8,128)(2,1)} %copy-done.6, ...), custom_call_target="tpu_custom_call" | custom-call | tf_op jit(solution)/shard_map/project/pallas_call | solution.py:253
  66.3 5.6 %all-to-all-start.1 = ((bf16[4,128,256]{2,1,0:T(8,128)(2,1)}), bf16[4,128,256]{2,1,0:T(8,128)(2,1)S(1)}, u32[]{:S(2)}, u32[]{:S(2)}) async-start(bf16[4,128,256]{2,1,0:T(8,128)(2,1)} %project.1), calls=%async_computation.1 | async-start | bytes 524288 | tf_op jit(solution)/shard_map/all_to_all | solution.py:261
  71.9 5.5 %all-to-all-done.1.got = bf16[4,128,256]{2,1,0:T(8,128)(2,1)S(1)} async-done(((bf16[4,128,256]{2,1,0:T(8,128)(2,1)}), bf16[4,128,256]{2,1,0:T(8,128)(2,1)S(1)}, u32[]{:S(2)}, u32[]{:S(2)}) %all-to-all-start.1) | async-done | bytes 262176 | tf_op jit(solution)/shard_map/all_to_all | solution.py:261
  77.4 0.0 copy-start.2
  77.4 0.7 copy-done.2
  78.1 3.1 %local.1 = (bf16[16,208,128]{2,1,0:T(8,128)(2,1)}, f32[128,128]{1,0:T(8,128)}, bf16[128,128]{1,0:T(8,128)(2,1)}, bf16[128,128]{1,0:T(8,128)(2,1)}) custom-call(s32[1]{0:T(128)} %bitcast.place, bf16[4,128,256]{2,1,0:T(8,128)(2,1)} %copy-done.2, f32[2,128]{1,0:T(2,128)} %gaps.1), custom_call_target="tpu_custom_call" | custom-call | tf_op jit(solution)/shard_map/local/pallas_call | solution.py:264
  81.2 4.3 %all-to-all-start.2 = ((bf16[16,208,128]{2,1,0:T(8,128)(2,1)}), bf16[16,208,128]{2,1,0:T(8,128)(2,1)S(1)}, u32[]{:S(2)}, u32[]{:S(2)}) async-start(bf16[16,208,128]{2,1,0:T(8,128)(2,1)} %get-tuple-element.9), calls=%async_computation.2 | async-start | bytes 1703936 | tf_op jit(solution)/shard_map/all_to_all | solution.py:276
  85.5 0.0 copy-start.7
  86.2 0.0 copy-done.7
  86.2 0.7 maximum_bitcast_fusion.hg_gain
  86.9 1.4 slice_bitcast_fusion.df_query
  88.2 32.6 %all-to-all-done.2.got = bf16[16,208,128]{2,1,0:T(8,128)(2,1)S(1)} async-done(((bf16[16,208,128]{2,1,0:T(8,128)(2,1)}), bf16[16,208,128]{2,1,0:T(8,128)(2,1)S(1)}, u32[]{:S(2)}, u32[]{:S(2)}) %all-to-all-start.2) | async-done | bytes 852000 | tf_op jit(solution)/shard_map/all_to_all | solution.py:276
  120.9 0.0 copy-start
  120.9 0.9 copy-done
  121.8 5.9 %finish.1 = bf16[128,2048]{1,0:T(8,128)(2,1)} custom-call(s32[1]{0:T(128)} %bitcast.place, f32[1]{0:T(128)S(6)} %copy.17.lam, bf16[16,208,128]{2,1,0:T(8,128)(2,1)} %copy-done, bf16[128,128]{1,0:T(8,128)(2,1)} %slice_bitcast_fusion.df_query, f32[128,128]{1,0:T(8,128)} %get-tuple-element.10.local, bf16[128,128]{1,0:T(8,128)(2,1)} %get-tuple-element.11.read_fwd, ...), custom_call_target="tpu_custom_call" | custom-call | tf_op jit(solution)/shard_map/finish/pallas_call | solution.py:277
  127.7 20.2 %all_to_all.20.parts = bf16[8,16,2048]{2,1,0:T(8,128)(2,1)} all-to-all(bf16[8,16,2048]{2,1,0:T(8,128)(2,1)} %bitcast.15), channel_id=1, replica_groups=mesh['sp'=16,'fs'=4,'tp'=8] {'tp'}, dimensions={0} | all-to-all | bytes 1048576 | tf_op jit(solution)/shard_map/all_to_all | solution.py:297
  147.9 1.8 %close.1 = bf16[1,16,2048]{2,1,0:T(8,128)(2,1)} custom-call(bf16[8,16,2048]{2,1,0:T(8,128)(2,1)} %all_to_all.20.parts, f32[1,2048]{1,0:T(1,128)} %bitcast.17), custom_call_target="tpu_custom_call" | custom-call | tf_op jit(solution)/shard_map/close/pallas_call | solution.py:300
  (2 shorter events, 0.0 us)
Async XLA Ops:
  1.8 60.1 %all-to-all-start = ((bf16[64,48,128]{2,1,0:T(8,128)(2,1)}), bf16[64,48,128]{2,1,0:T(8,128)(2,1)S(1)}, u32[]{:S(2)}, u32[]{:S(2)}) async-start(bf16[64,48,128]{2,1,0:T(8,128)(2,1)} %bitcast.14), calls=%async_computation | async-start | bytes 1572864 | tf_op jit(solution)/shard_map/all_to_all | solution.py:234
  23.1 20.2 %collective-permute-start = (bf16[128,2048]{1,0:T(8,128)(2,1)}, bf16[128,2048]{1,0:T(8,128)(2,1)S(1)}, u32[]{:S(2)}, u32[]{:S(2)}) collective-permute-start(bf16[128,2048]{1,0:T(8,128)(2,1)} %norm.1.own), channel_id=1, source_target_pairs={{0,8},{8,16},{16,24},{24,0},{1,9},{9,17},{17,25},{25,1},{2,10},{10... | collective-permute-start | bytes 1572872 | tf_op jit(solution)/shard_map/ppermute | solution.py:245
  26.1 19.2 %collective-permute-start.1 = (bf16[128,2048]{1,0:T(8,128)(2,1)}, bf16[128,2048]{1,0:T(8,128)(2,1)S(1)}, u32[]{:S(2)}, u32[]{:S(2)}) collective-permute-start(bf16[128,2048]{1,0:T(8,128)(2,1)} %norm.1.own), channel_id=1, source_target_pairs={{0,24},{8,0},{16,8},{24,16},{1,25},{9,1},{17,9},{25,17},{2,26},{10... | collective-permute-start | bytes 1572872 | tf_op jit(solution)/shard_map/ppermute | solution.py:245
  43.3 2.0 %copy-start.3 = (bf16[128,2048]{1,0:T(8,128)(2,1)}, bf16[128,2048]{1,0:T(8,128)(2,1)S(1)}, u32[]{:S(2)}) copy-start(bf16[128,2048]{1,0:T(8,128)(2,1)S(1)} %collective-permute-done.before) | copy-start | bytes 1572868
  43.4 12.1 %collective-permute-start.2 = (bf16[64,2048]{1,0:T(8,128)(2,1)S(1)}, bf16[64,2048]{1,0:T(8,128)(2,1)S(1)}, u32[]{:S(2)}, u32[]{:S(2)}) collective-permute-start(bf16[64,2048]{1,0:T(8,128)(2,1)S(1)} %slice.12), channel_id=1, source_target_pairs={{0,8},{8,16},{16,24},{24,0},{1,9},{9,17},{17,25},{25,1},{2,10},{10... | collective-permute-start | bytes 786440 | tf_op jit(solution)/shard_map/ppermute | solution.py:245
  45.3 16.6 %copy-start.4 = (bf16[128,2048]{1,0:T(8,128)(2,1)}, bf16[128,2048]{1,0:T(8,128)(2,1)S(1)}, u32[]{:S(2)}) copy-start(bf16[128,2048]{1,0:T(8,128)(2,1)S(1)} %collective-permute-done.1.after) | copy-start | bytes 1572868
  45.3 10.1 %collective-permute-start.3 = (bf16[64,2048]{1,0:T(8,128)(2,1)S(1)}, bf16[64,2048]{1,0:T(8,128)(2,1)S(1)}, u32[]{:S(2)}, u32[]{:S(2)}) collective-permute-start(bf16[64,2048]{1,0:T(8,128)(2,1)S(1)} %slice.13), channel_id=1, source_target_pairs={{0,24},{8,0},{16,8},{24,16},{1,25},{9,1},{17,9},{25,17},{2,26},{10... | collective-permute-start | bytes 786440 | tf_op jit(solution)/shard_map/ppermute | solution.py:245
  55.4 6.5 %copy-start.5 = (bf16[64,2048]{1,0:T(8,128)(2,1)}, bf16[64,2048]{1,0:T(8,128)(2,1)S(1)}, u32[]{:S(2)}) copy-start(bf16[64,2048]{1,0:T(8,128)(2,1)S(1)} %collective-permute-done.2.far_top) | copy-start | bytes 786436
  55.4 6.5 %copy-start.6 = (bf16[64,2048]{1,0:T(8,128)(2,1)}, bf16[64,2048]{1,0:T(8,128)(2,1)S(1)}, u32[]{:S(2)}) copy-start(bf16[64,2048]{1,0:T(8,128)(2,1)S(1)} %collective-permute-done.3.far_low) | copy-start | bytes 786436
  61.9 0.9 copy-start.1
  66.3 11.1 %all-to-all-start.1 = ((bf16[4,128,256]{2,1,0:T(8,128)(2,1)}), bf16[4,128,256]{2,1,0:T(8,128)(2,1)S(1)}, u32[]{:S(2)}, u32[]{:S(2)}) async-start(bf16[4,128,256]{2,1,0:T(8,128)(2,1)} %project.1), calls=%async_computation.1 | async-start | bytes 524288 | tf_op jit(solution)/shard_map/all_to_all | solution.py:261
  77.4 0.7 copy-start.2
  81.2 39.7 %all-to-all-start.2 = ((bf16[16,208,128]{2,1,0:T(8,128)(2,1)}), bf16[16,208,128]{2,1,0:T(8,128)(2,1)S(1)}, u32[]{:S(2)}, u32[]{:S(2)}) async-start(bf16[16,208,128]{2,1,0:T(8,128)(2,1)} %get-tuple-element.9), calls=%async_computation.2 | async-start | bytes 1703936 | tf_op jit(solution)/shard_map/all_to_all | solution.py:276
  85.5 0.7 copy-start.7
  120.9 0.9 copy-start

commit v2 on v1

--- a/solution.py
+++ b/solution.py
@@ -1,5 +1,3 @@
-import functools
-
 import jax
 import jax.numpy as jnp
 from jax import lax
@@ -10,7 +8,7 @@
 HEAD = 64
 DQK = 32
 LANES = 128
-STATE_ROWS = 80
+STATE_ROWS = 72
 
 epsilon = 1e-06
 df_factor = 0.8
@@ -18,33 +16,55 @@
 bf16 = jnp.bfloat16
 
 SMEM_SPEC = pl.BlockSpec(memory_space=pltpu.SMEM)
+VMEM_SPEC = pl.BlockSpec(memory_space=pltpu.VMEM)
+LIMIT = pltpu.CompilerParams(vmem_limit_bytes=24 * 2**20)
+
+
+FAR_SPEC = pl.BlockSpec(memory_space=pltpu.HBM)
+
+
+def there(array):
+    return pltpu.with_memory_space_constraint(array, pltpu.HBM)
+
+
+def here(array):
+    return pltpu.with_memory_space_constraint(array, pltpu.VMEM)
 
 
 def dot(a, b, dims, precision=None):
     return lax.dot_general(a, b, (dims, ((), ())), precision=precision, preferred_element_type=f32)
 
 
-def pack_kernel(q, f, b, v, dq, dk, dv, out):
-    copies, _, rows, _ = out.shape
-    depth = q.shape[0]
-    half = depth // 2
-    for j, (wide, narrow) in enumerate(((q, dq), (f, dk), (b, dv), (v, dq))):
-        folded = jnp.concatenate([narrow[:half, :], narrow[half:, :]], axis=1)
-        block = jnp.concatenate([wide[...], folded], axis=0)
-        for c in range(copies):
-            out[c, j] = block
+def pack_kernel(q, f, b, v, dq, dk, dv, out, wide, narrow, sems):
+    copies = [
+        pltpu.make_async_copy(source, wide.at[j], sems.at[j])
+        for j, source in enumerate((q, f, b, v))
+    ] + [
+        pltpu.make_async_copy(source, narrow.at[j], sems.at[4 + j])
+        for j, source in enumerate((dq, dk, dv))
+    ]
+    for copy in copies:
+        copy.start()
+    for copy in copies:
+        copy.wait()
+    half = q.shape[0] // 2
+    for j in range(4):
+        k = j % 3
+        folded = jnp.concatenate([narrow[k, :half, :], narrow[k, half:, :]], axis=1)
+        out[j] = jnp.concatenate([wide[j], folded], axis=0)
 
 
 def norm_kernel(x, gain, out):
     rows = x[0].astype(f32)
     scale = lax.rsqrt(jnp.mean(rows * rows, axis=-1, keepdims=True) + epsilon)
-    out[...] = (rows * scale * gain[...]).astype(bf16)
-
-
-def project_kernel(places, own, before, after, far_top, far_low, weights, out, rhs):
+    done = (rows * scale * gain[...]).astype(bf16)
+    for k in range(out.shape[0]):
+        out[k] = done
+
+
+def project_kernel(rows, weights, out, rhs):
     blocks, packed, _ = weights.shape
     depth = packed * 2 // 3
-    half = depth // 2
     wide = weights[:, :depth, :]
     narrow = weights[:, depth:, :].astype(f32)
     first, second = narrow[:, :, :HEAD], narrow[:, :, HEAD:]
@@ -57,14 +77,12 @@
     ).astype(bf16)
     rhs[:, :LANES] = wide.reshape(blocks * depth, LANES)
     rhs[:, LANES:] = narrow.reshape(blocks * depth, LANES)
-    top = far_top.shape[0]
-    for k, rows in enumerate((own, before, after)):
-        out[places[k]] = dot(rows[...], rhs[...], ((1,), (0,))).astype(bf16)
-    out[places[3], :top] = dot(far_top[...], rhs[...], ((1,), (0,))).astype(bf16)
-    out[places[3], top:] = dot(far_low[...], rhs[...], ((1,), (0,))).astype(bf16)
-
-
-def local_kernel(place, got, gaps, message, local, read_fwd, read_bwd):
+    for k in range(rows.shape[0]):
+        out[k] = dot(rows[k], rhs[...], ((1,), (0,))).astype(bf16)
+
+
+def local_kernel(place, got, gaps, gains_in, message, local, read_fwd, read_bwd, gains):
+    gains[...] = gains_in[...]
     length = got.shape[1]
     devices = message.shape[0]
     me = place[0]
@@ -131,7 +149,7 @@
 
 
 def finish_kernel(
-    place, lam, got, df_query, local, read_fwd, read_bwd, hg_gain, df_gain, hg_w, df_w, out, mixed
+    place, lam, got, df_query, local, read_fwd, read_bwd, gains, hg_w, df_w, out, mixed
 ):
     devices = got.shape[0]
     length = local.shape[0]
@@ -163,7 +181,7 @@
     first = jnp.sum(jnp.where(lane < HEAD, squares, 0.0), axis=1, keepdims=True)
     second = jnp.sum(jnp.where(lane < HEAD, 0.0, squares), axis=1, keepdims=True)
     mean = jnp.where(lane < HEAD, first, second) * (1.0 / HEAD)
-    mixed[:, :LANES] = (recurrent * lax.rsqrt(mean + epsilon) * hg_gain[...]).astype(bf16)
+    mixed[:, :LANES] = (recurrent * lax.rsqrt(mean + epsilon) * gains[0:1]).astype(bf16)
 
     step = 64
     keys_values = got[:, :length, :].reshape(devices * length, LANES)
@@ -172,7 +190,7 @@
 
     def attend(i, carry):
         rows = pl.ds(pl.multiple_of(i * step, step), step)
-        query = df_query[rows, :]
+        query = df_query[0, rows, LANES:]
         maps = []
         for m in range(2):
             inside = (lane_step >= m * DQK) & (lane_step < (m + 1) * DQK)
@@ -183,7 +201,7 @@
             maps.append(dot(shifted.astype(bf16), keys_values, ((1,), (0,))) / totals)
         weighted = (maps[0] - lam_value * maps[1])[:, HEAD:]
         mean = jnp.mean(weighted * weighted, axis=-1, keepdims=True)
-        normed = (weighted * lax.rsqrt(mean + epsilon) * df_gain[...] * df_factor).astype(bf16)
+        normed = (weighted * lax.rsqrt(mean + epsilon) * gains[1:2, :HEAD] * df_factor).astype(bf16)
         mixed[rows, LANES : LANES + HEAD] = normed
         return carry
 
@@ -221,78 +239,84 @@
     post_gain,
 ):
     sp, fs, tp = (lax.axis_size(a) for a in ("sp", "fs", "tp"))
-    z, y = lax.axis_index("sp"), lax.axis_index("fs")
+    z = lax.axis_index("sp")
     _, length, width = inputs.shape
     depth = hg_query_w.shape[0]
     packed = depth + depth // 2
 
+    vmem = VMEM_SPEC
+    normed = pl.pallas_call(
+        norm_kernel,
+        out_shape=pltpu.VMEM((fs, length, width), bf16),
+        compiler_params=LIMIT,
+        name="norm",
+    )(inputs, norm_gain[None])
+
+    rows = lax.all_to_all(normed, "fs", 0, 0, tiled=True)
+    sources = (hg_query_w, hg_fwd_w, hg_bwd_w, hg_value_w, df_query_w, df_key_w, df_value_w)
     sent = pl.pallas_call(
         pack_kernel,
-        out_shape=jax.ShapeDtypeStruct((sp, fs, packed, LANES), bf16),
+        in_specs=[FAR_SPEC] * 7,
+        out_specs=vmem,
+        out_shape=pltpu.VMEM((fs, packed, LANES), bf16),
+        scratch_shapes=[
+            pltpu.VMEM((4, depth, LANES), bf16),
+            pltpu.VMEM((3, depth, LANES // 2), bf16),
+            pltpu.SemaphoreType.DMA((7,)),
+        ],
+        compiler_params=LIMIT,
         name="pack",
-    )(hg_query_w, hg_fwd_w, hg_bwd_w, hg_value_w, df_query_w, df_key_w, df_value_w)
-    weights = lax.all_to_all(
-        sent.reshape(sp * fs, packed, LANES), ("sp", "fs"), 0, 0, tiled=True
-    )
-
-    normed = pl.pallas_call(
-        norm_kernel,
-        out_shape=jax.ShapeDtypeStruct((length, width), bf16),
-        name="norm",
-    )(inputs, norm_gain[None])
-
-    def shifted(array, by):
-        return lax.ppermute(array, "fs", [(i, (i + by) % fs) for i in range(fs)])
-
-    before = shifted(normed, 1)
-    after = shifted(normed, -1)
-    far_top = shifted(before[: length // 2], 1)
-    far_low = shifted(after[length // 2 :], -1)
-    places = jnp.stack([y, (y + fs - 1) % fs, (y + 1) % fs, (y + 2) % fs]).astype(jnp.int32)
-    vmem = pl.BlockSpec(memory_space=pltpu.VMEM)
+    )(*map(there, sources))
+    mine = lax.all_to_all(sent, "fs", 0, 0, tiled=True)
+    weights = lax.all_gather(mine[None], "sp", axis=0, tiled=True)
+    weights = weights.reshape(sp * fs, packed, LANES)
     projected = pl.pallas_call(
         project_kernel,
-        in_specs=[SMEM_SPEC] + [vmem] * 6,
+        in_specs=[vmem] * 2,
         out_specs=vmem,
-        out_shape=jax.ShapeDtypeStruct((fs, length, 2 * LANES), bf16),
+        out_shape=pltpu.VMEM((fs, length, 2 * LANES), bf16),
         scratch_shapes=[pltpu.VMEM((width, 2 * LANES), bf16)],
+        compiler_params=LIMIT,
         name="project",
-    )(places, normed, before, after, far_top, far_low, weights)
+    )(here(rows), here(weights))
     got = lax.all_to_all(projected, "fs", 0, 0, tiled=True)
 
     place = z.astype(jnp.int32)[None]
-    message, local, read_fwd, read_bwd = pl.pallas_call(
+    gains = jnp.concatenate([hg_norm_gain, hg_norm_gain, df_norm_gain, df_norm_gain])
+    message, local, read_fwd, read_bwd, gains = pl.pallas_call(
         local_kernel,
-        in_specs=[SMEM_SPEC] + [vmem] * 2,
-        out_specs=[vmem] * 4,
+        in_specs=[SMEM_SPEC] + [vmem] * 3,
+        out_specs=[vmem] * 5,
         out_shape=[
-            jax.ShapeDtypeStruct((sp, length + STATE_ROWS, LANES), bf16),
-            jax.ShapeDtypeStruct((length, LANES), f32),
-            jax.ShapeDtypeStruct((length, LANES), bf16),
-            jax.ShapeDtypeStruct((length, LANES), bf16),
+            pltpu.VMEM((sp, length + STATE_ROWS, LANES), bf16),
+            pltpu.VMEM((length, LANES), f32),
+            pltpu.VMEM((length, LANES), bf16),
+            pltpu.VMEM((length, LANES), bf16),
+            pltpu.VMEM((2, LANES), f32),
         ],
+        compiler_params=LIMIT,
         name="local",
-    )(place, got, floor_gap)
+    )(place, here(got), here(floor_gap), here(gains.reshape(2, LANES)))
     arrived = lax.all_to_all(message, "sp", 0, 0, tiled=True)
     partial = pl.pallas_call(
         finish_kernel,
-        in_specs=[SMEM_SPEC] * 2 + [vmem] * 9,
+        in_specs=[SMEM_SPEC] * 2 + [vmem] * 8,
         out_specs=vmem,
-        out_shape=jax.ShapeDtypeStruct((length, width), bf16),
+        out_shape=pltpu.VMEM((length, width), bf16),
         scratch_shapes=[pltpu.VMEM((length, 2 * LANES), bf16)],
+        compiler_params=LIMIT,
         name="finish",
     )(
         place,
         diff_lambda,
-        arrived,
-        got[0, :, LANES:],
-        local,
-        read_fwd,
-        read_bwd,
-        jnp.concatenate([hg_norm_gain, hg_norm_gain])[None],
-        df_norm_gain[None],
-        out_hg_w,
-        out_df_w,
+        here(arrived),
+        here(got),
+        here(local),
+        here(read_fwd),
+        here(read_bwd),
+        here(gains),
+        here(out_hg_w),
+        here(out_df_w),
     )
     parts = lax.all_to_all(
         partial.reshape(tp, length // tp, width), "tp", 0, 0, tiled=True
@@ -300,8 +324,9 @@
     return pl.pallas_call(
         close_kernel,
         out_shape=jax.ShapeDtypeStruct((1, length // tp, width), bf16),
+        compiler_params=LIMIT,
         name="close",
-    )(parts, post_gain[None])
+    )(here(parts), post_gain[None])
 
 
 def solution(mesh):
@@ -325,4 +350,6 @@
         P(),
     )
     out_specs = P("fs", ("sp", "tp"), None)
-    return jax.shard_map(shards, mesh=mesh, in_specs=in_specs, out_specs=out_specs, check_vma=False)
+    return jax.shard_map(
+        shards, mesh=mesh, in_specs=in_specs, out_specs=out_specs, check_vma=False
+    )

time: 151 us -> 130 us (0.86)
  blocking collectives: 20.2 us -> 60.3 us
  waiting for transfers between devices: 63.1 us -> 35.7 us
  starting transfers between devices: 42.2 us -> 19.3 us
  Pallas kernels: 18.2 us -> 11.2 us
  local copies, waits for them, and re-layouts: 3.94 us -> 1.77 us
    all_gather x0 -> x1, blocking collectives: none -> 34.9 us  [shards(): weights = lax.all_gather(mine[None], 'sp', axis=0, tiled=True)]
    ppermute x4 -> x0, waiting for transfers between devices: 18.5 us -> none  [shifted(): return lax.ppermute(array, 'fs', [(i, (i + by) % fs) for i in range(fs)])]
    ppermute x4 -> x0, starting transfers between devices: 13 us -> none  [shifted(): return lax.ppermute(array, 'fs', [(i, (i + by) % fs) for i in range(fs)])]
    all_to_all x1 -> x2, starting transfers between devices: 19.3 us -> 8.62 us  [the longest x1 5.01 us: shards(): mine = lax.all_to_all(sent, 'fs', 0, 0, tiled=True)]
    pallas_call x5, Pallas kernels: 16.3 us -> 10.4 us  [the longest x1 3.57 us: shards(): pl.pallas_call(finish_kernel, in_specs=[SMEM_SPEC] * 2 + [vmem] * 8, out_...]
    all_to_all x1 -> x2, waiting for transfers between devices: 6.45 us -> 1.01 us  [the longest x1 1.01 us: shards(): mine = lax.all_to_all(sent, 'fs', 0, 0, tiled=True)]
    all_to_all x1, blocking collectives: 20.2 us -> 25.3 us  [shards(): lax.all_to_all(partial.reshape(tp, length // tp, width), 'tp', 0, 0, tile...]
    all_to_all x1, waiting for transfers between devices: 32.6 us -> 29.2 us  [shards(): arrived = lax.all_to_all(message, 'sp', 0, 0, tiled=True)]
  transfers between devices with their start and end apart: 7 -> 4, of which waited for: 5 -> 3; matrix products, arithmetic and copies ran while one was open for 2% -> 0% of each run, Pallas kernels for 1% -> 1%
where the time goes in v2:
time: 130 us; the launch traced here: 129 us
  blocking collectives  60.3 us (46%)
  waiting for transfers between devices  35.7 us (27%)
  starting transfers between devices  19.3 us (15%)
  Pallas kernels  11.2 us (9%)
  local copies, waits for them, and re-layouts  1.77 us (1%)
    all_gather x1, blocking collectives, shards(): weights = lax.all_gather(mine[None], 'sp', axis=0, tiled=True)  34.9 us
    all_to_all x1, waiting for transfers between devices, shards(): arrived = lax.all_to_all(message, 'sp', 0, 0, tiled=True)  29.2 us
    all_to_all x1, blocking collectives, shards(): lax.all_to_all(partial.reshape(tp, length // tp, width), 'tp', 0, 0, tile...  25.3 us
    all_to_all x1, starting transfers between devices, shards(): arrived = lax.all_to_all(message, 'sp', 0, 0, tiled=True)  6.83 us
    all_to_all x1, waiting for transfers between devices, shards(): got = lax.all_to_all(projected, 'fs', 0, 0, tiled=True)  5.45 us
    all_to_all x1, starting transfers between devices, shards(): mine = lax.all_to_all(sent, 'fs', 0, 0, tiled=True)  5.01 us
    all_to_all x1, starting transfers between devices, shards(): got = lax.all_to_all(projected, 'fs', 0, 0, tiled=True)  3.82 us
    all_to_all x1, starting transfers between devices, shards(): rows = lax.all_to_all(normed, 'fs', 0, 0, tiled=True)  3.61 us
  transfers between devices with their start and end apart: 4, of which 3 were waited for; matrix products, arithmetic and copies ran while one was open for 0% of the time, Pallas kernels for 1%

profile of v2, /device:TPU:1, one launch (start us, length us, event | category | flops | bytes accessed | tf_op | source)
XLA Modules:
  0.0 129.0 jit_solution(2481364664891729625)
XLA Ops:
  0.0 1.5 %pack.1 = bf16[4,48,128]{2,1,0:T(8,128)(2,1)} custom-call(bf16[32,128]{1,0:T(8,128)(2,1)} %q.1, bf16[32,128]{1,0:T(8,128)(2,1)} %f.1, bf16[32,128]{1,0:T(8,128)(2,1)} %b.1, bf16[32,128]{1,0:T(8,128)(2,1)} %v.1, bf16[32,64]{1,0:T(8,128)(2,1)} %dq.1, bf16[32,64]{1,0:T(8,128)(2,1)} %dk.1, bf16[32,64]{1,0:T(8,128)(2,1)} %dv.1), custom_call_target="tpu_custom_call" | custom-call | tf_op jit(solution)/shard_map/pack/pallas_call | solution.py:257
  1.6 5.0 %all-to-all-start.1 = ((bf16[4,48,128]{2,1,0:T(8,128)(2,1)}), bf16[4,48,128]{2,1,0:T(8,128)(2,1)S(1)}, u32[]{:S(2)}, u32[]{:S(2)}) async-start(bf16[4,48,128]{2,1,0:T(8,128)(2,1)} %pack.1), calls=%async_computation.1 | async-start | bytes 98304 | tf_op jit(solution)/shard_map/all_to_all | solution.py:270
  6.6 0.0 copy-start
  6.6 1.0 copy-done
  7.6 0.0 copy-start.3
  7.6 0.7 copy-done.3
  8.3 1.6 %norm.1 = bf16[4,128,2048]{2,1,0:T(8,128)(2,1)} custom-call(bf16[1,128,2048]{2,1,0:T(8,128)(2,1)S(1)} %copy-done, f32[1,2048]{1,0:T(1,128)S(1)} %bitcast.7), custom_call_target="tpu_custom_call" | custom-call | tf_op jit(solution)/shard_map/norm/pallas_call | solution.py:248
  9.9 1.0 all-to-all-done.1
  11.0 3.6 %all-to-all-start = ((bf16[4,128,2048]{2,1,0:T(8,128)(2,1)}), bf16[4,128,2048]{2,1,0:T(8,128)(2,1)S(1)}, u32[]{:S(2)}, u32[]{:S(2)}) async-start(bf16[4,128,2048]{2,1,0:T(8,128)(2,1)} %norm.1), calls=%async_computation | async-start | bytes 4194304 | tf_op jit(solution)/shard_map/all_to_all | solution.py:255
  14.6 0.0 copy-start.6
  14.6 0.0 copy-start.7
  14.6 0.0 copy-start.5
  14.6 34.9 %all-gather.weights = bf16[64,48,128]{2,1,0:T(8,128)(2,1)S(1)} all-gather(bf16[4,48,128]{2,1,0:T(8,128)(2,1)S(1)} %all-to-all-done.1), channel_id=2, replica_groups=mesh['sp'=16,'fs'=4,'tp'=8] {'sp'}, dimensions={0}, use_global_device_ids=true | all-gather | bytes 835584 | tf_op jit(solution)/shard_map/all_gather | solution.py:271
  49.5 0.0 copy-start.1
  49.6 0.0 all-to-all-done.rows
  49.6 1.5 %project.1 = bf16[4,128,256]{2,1,0:T(8,128)(2,1)} custom-call(bf16[4,128,2048]{2,1,0:T(8,128)(2,1)S(1)} %all-to-all-done.rows, bf16[64,48,128]{2,1,0:T(8,128)(2,1)S(1)} %all-gather.weights), custom_call_target="tpu_custom_call" | custom-call | tf_op jit(solution)/shard_map/project/pallas_call | solution.py:273
  51.1 0.0 copy-start.2
  51.1 3.8 %all-to-all-start.2 = ((bf16[4,128,256]{2,1,0:T(8,128)(2,1)}), bf16[4,128,256]{2,1,0:T(8,128)(2,1)S(1)}, u32[]{:S(2)}, u32[]{:S(2)}) async-start(bf16[4,128,256]{2,1,0:T(8,128)(2,1)} %project.1), calls=%async_computation.2 | async-start | bytes 524288 | tf_op jit(solution)/shard_map/all_to_all | solution.py:282
  54.9 0.0 copy-done.6
  54.9 0.0 copy-done.7
  54.9 0.1 maximum_bitcast_fusion.gains_in
  55.0 5.4 %all-to-all-done.2.got.df_query = bf16[4,128,256]{2,1,0:T(8,128)(2,1)S(1)} async-done(((bf16[4,128,256]{2,1,0:T(8,128)(2,1)}), bf16[4,128,256]{2,1,0:T(8,128)(2,1)S(1)}, u32[]{:S(2)}, u32[]{:S(2)}) %all-to-all-start.2) | async-done | bytes 262176 | tf_op jit(solution)/shard_map/all_to_all | solution.py:282
  60.4 0.0 copy-done.5
  60.4 2.1 %local.1 = (bf16[16,200,128]{2,1,0:T(8,128)(2,1)}, f32[128,128]{1,0:T(8,128)S(1)}, bf16[128,128]{1,0:T(8,128)(2,1)S(1)}, bf16[128,128]{1,0:T(8,128)(2,1)S(1)}, f32[2,128]{1,0:T(2,128)S(1)}) custom-call(s32[1]{0:T(128)} %bitcast.place, bf16[4,128,256]{2,1,0:T(8,128)(2,1)S(1)} %all-to-all-done.2.got.df_query, f32[2,128]{1,0:T(2,128)S(1)} %copy-done.5, ...), custom_call_target="tpu_custom_call" | custom-call | tf_op jit(solution)/shard_map/local/pallas_call | solution.py:286
  62.5 6.8 %all-to-all-start.3 = ((bf16[16,200,128]{2,1,0:T(8,128)(2,1)}), bf16[16,200,128]{2,1,0:T(8,128)(2,1)S(1)}, u32[]{:S(2)}, u32[]{:S(2)}) async-start(bf16[16,200,128]{2,1,0:T(8,128)(2,1)} %get-tuple-element.10), calls=%async_computation.3 | async-start | bytes 1638400 | tf_op jit(solution)/shard_map/all_to_all | solution.py:300
  69.3 0.0 copy-start.4
  70.0 29.2 %all-to-all-done.3.got = bf16[16,200,128]{2,1,0:T(8,128)(2,1)S(1)} async-done(((bf16[16,200,128]{2,1,0:T(8,128)(2,1)}), bf16[16,200,128]{2,1,0:T(8,128)(2,1)S(1)}, u32[]{:S(2)}, u32[]{:S(2)}) %all-to-all-start.3) | async-done | bytes 819232 | tf_op jit(solution)/shard_map/all_to_all | solution.py:300
  99.2 0.0 copy-done.1
  99.2 0.0 copy-done.2
  99.2 3.6 %finish.1 = bf16[128,2048]{1,0:T(8,128)(2,1)S(1)} custom-call(s32[1]{0:T(128)} %bitcast.place, f32[1]{0:T(128)S(6)} %copy.17.lam, bf16[16,200,128]{2,1,0:T(8,128)(2,1)S(1)} %all-to-all-done.3.got, bf16[4,128,256]{2,1,0:T(8,128)(2,1)S(1)} %all-to-all-done.2.got.df_query, f32[128,128]{1,0:T(8,128)S(1)} %get-tuple-element.11.local, ...), custom_call_target="tpu_custom_call" | custom-call | tf_op jit(solution)/shard_map/finish/pallas_call | solution.py:301
  102.8 25.3 %all_to_all.25.parts = bf16[8,16,2048]{2,1,0:T(8,128)(2,1)S(1)} all-to-all(bf16[8,16,2048]{2,1,0:T(8,128)(2,1)S(1)} %bitcast.6), channel_id=1, replica_groups=mesh['sp'=16,'fs'=4,'tp'=8] {'tp'}, dimensions={0} | all-to-all | bytes 1048576 | tf_op jit(solution)/shard_map/all_to_all | solution.py:321
  128.2 0.0 copy-done.4
  128.2 0.8 close.1
Async XLA Ops:
  1.6 9.4 %all-to-all-start.1 = ((bf16[4,48,128]{2,1,0:T(8,128)(2,1)}), bf16[4,48,128]{2,1,0:T(8,128)(2,1)S(1)}, u32[]{:S(2)}, u32[]{:S(2)}) async-start(bf16[4,48,128]{2,1,0:T(8,128)(2,1)} %pack.1), calls=%async_computation.1 | async-start | bytes 98304 | tf_op jit(solution)/shard_map/all_to_all | solution.py:270
  6.6 1.0 copy-start
  7.6 0.7 copy-start.3
  11.0 38.6 %all-to-all-start = ((bf16[4,128,2048]{2,1,0:T(8,128)(2,1)}), bf16[4,128,2048]{2,1,0:T(8,128)(2,1)S(1)}, u32[]{:S(2)}, u32[]{:S(2)}) async-start(bf16[4,128,2048]{2,1,0:T(8,128)(2,1)} %norm.1), calls=%async_computation | async-start | bytes 4194304 | tf_op jit(solution)/shard_map/all_to_all | solution.py:255
  14.6 40.3 %copy-start.6 = (f32[64]{0:T(128)S(1)}, f32[64]{0:T(128)}, u32[]{:S(2)}) copy-start(f32[64]{0:T(128)} %param.28) | copy-start | bytes 772
  14.6 40.3 %copy-start.7 = (f32[64]{0:T(128)S(1)}, f32[64]{0:T(128)}, u32[]{:S(2)}) copy-start(f32[64]{0:T(128)} %param.23) | copy-start | bytes 772
  14.6 45.8 %copy-start.5 = (f32[2,128]{1,0:T(2,128)S(1)}, f32[2,128]{1,0:T(2,128)}, u32[]{:S(2)}) copy-start(f32[2,128]{1,0:T(2,128)} %gaps.1) | copy-start | bytes 3076
  49.5 49.7 %copy-start.1 = (bf16[128,2048]{1,0:T(8,128)(2,1)S(1)}, bf16[128,2048]{1,0:T(8,128)(2,1)}, u32[]{:S(2)}) copy-start(bf16[128,2048]{1,0:T(8,128)(2,1)} %hg_w.1) | copy-start | bytes 1572868
  51.1 48.2 %copy-start.2 = (bf16[64,2048]{1,0:T(8,128)(2,1)S(1)}, bf16[64,2048]{1,0:T(8,128)(2,1)}, u32[]{:S(2)}) copy-start(bf16[64,2048]{1,0:T(8,128)(2,1)} %df_w.1) | copy-start | bytes 786436
  51.1 9.3 %all-to-all-start.2 = ((bf16[4,128,256]{2,1,0:T(8,128)(2,1)}), bf16[4,128,256]{2,1,0:T(8,128)(2,1)S(1)}, u32[]{:S(2)}, u32[]{:S(2)}) async-start(bf16[4,128,256]{2,1,0:T(8,128)(2,1)} %project.1), calls=%async_computation.2 | async-start | bytes 524288 | tf_op jit(solution)/shard_map/all_to_all | solution.py:282
  62.5 36.7 %all-to-all-start.3 = ((bf16[16,200,128]{2,1,0:T(8,128)(2,1)}), bf16[16,200,128]{2,1,0:T(8,128)(2,1)S(1)}, u32[]{:S(2)}, u32[]{:S(2)}) async-start(bf16[16,200,128]{2,1,0:T(8,128)(2,1)} %get-tuple-element.10), calls=%async_computation.3 | async-start | bytes 1638400 | tf_op jit(solution)/shard_map/all_to_all | solution.py:300
  69.3 58.8 %copy-start.4 = (f32[2048]{0:T(1024)S(1)}, f32[2048]{0:T(1024)}, u32[]{:S(2)}) copy-start(f32[2048]{0:T(1024)} %param.31) | copy-start | bytes 24580

commit v3 on v2

--- a/solution.py
+++ b/solution.py
@@ -8,7 +8,8 @@
 HEAD = 64
 DQK = 32
 LANES = 128
-STATE_ROWS = 72
+EXTRA = 16
+TAIL = 8
 
 epsilon = 1e-06
 df_factor = 0.8
@@ -81,11 +82,9 @@
         out[k] = dot(rows[k], rhs[...], ((1,), (0,))).astype(bf16)
 
 
-def local_kernel(place, got, gaps, gains_in, message, local, read_fwd, read_bwd, gains):
+def local_kernel(got, gaps, gains_in, held, states, local, read_fwd, read_bwd, gains):
     gains[...] = gains_in[...]
     length = got.shape[1]
-    devices = message.shape[0]
-    me = place[0]
     row = lax.broadcasted_iota(jnp.int32, (length, length), 0)
     col = lax.broadcasted_iota(jnp.int32, (length, length), 1)
     lane = lax.broadcasted_iota(jnp.int32, (length, LANES), 1)
@@ -111,7 +110,7 @@
         reader[...] = (queries * jnp.exp(gone)).astype(bf16)
         high = decay.astype(bf16)
         low = (decay - high.astype(f32)).astype(bf16)
-        pieces.append((state.astype(bf16), high, low))
+        pieces.append((state, high, low))
         query_part = queries * jnp.exp(gone - middle)
         key_part = (taken * jnp.exp(middle - gone)).astype(bf16)
         for h in range(2):
@@ -124,49 +123,87 @@
     out_0 = dot((fwd_0 + bwd_0).astype(bf16), values, ((1,), (0,)))
     out_1 = dot((fwd_1 + bwd_1).astype(bf16), values, ((1,), (0,)))
     local[...] = jnp.where(lane < HEAD, out_0, out_1)
-    keys_values = jnp.where(lane < HEAD, got[1, :, LANES:], got[2, :, LANES:])
-    spare = STATE_ROWS - HEAD
-    row_spare = lax.broadcasted_iota(jnp.int32, (spare, LANES), 0)
-
-    def tail(piece):
-        high = jnp.broadcast_to(piece[1].astype(f32), (spare, LANES))
-        low = jnp.broadcast_to(piece[2].astype(f32), (spare, LANES))
-        return jnp.where(row_spare == 0, high, low).astype(bf16)
-
-    tails = tail(fwd), tail(bwd)
-    for d in range(devices):
-        message[d, :length] = keys_values
-
-        @pl.when(d > me)
-        def _():
-            message[d, length : length + HEAD] = fwd[0]
-            message[d, length + HEAD :] = tails[0]
-
-        @pl.when(d <= me)
-        def _():
-            message[d, length : length + HEAD] = bwd[0]
-            message[d, length + HEAD :] = tails[1]
+    held[...] = jnp.where(lane < HEAD, got[1, :, LANES:], got[2, :, LANES:])
+    states[: 2 * HEAD] = jnp.concatenate([fwd[0], bwd[0]], axis=0).astype(bf16)
+    states[2 * HEAD :] = stacked(EXTRA, (fwd[1], fwd[2], bwd[1], bwd[2]))
+
+
+def stacked(count, lines):
+    row = lax.broadcasted_iota(jnp.int32, (count, LANES), 0)
+    block = jnp.zeros((count, LANES), f32)
+    for k, line in enumerate(lines):
+        block = jnp.where(row == k, jnp.broadcast_to(line.astype(f32), (count, LANES)), block)
+    return block.astype(bf16)
+
+
+def halves(value):
+    high = value.astype(bf16)
+    return high, (value - high.astype(f32)).astype(bf16)
+
+
+def pair_kernel(place, held, mine, other, out):
+    length = held.shape[0]
+    odd = lax.rem(place[0], 2) == 1
+    mine_all = mine[: 2 * HEAD].astype(f32)
+    other_all = other[: 2 * HEAD].astype(f32)
+    low = jnp.where(odd, other_all, mine_all)
+    high = jnp.where(odd, mine_all, other_all)
+    mine_tail = mine[2 * HEAD :].astype(f32)
+    other_tail = other[2 * HEAD :].astype(f32)
+    low_tail = jnp.where(odd, other_tail, mine_tail)
+    high_tail = jnp.where(odd, mine_tail, other_tail)
+    low_fwd, low_bwd = low_tail[0:1] + low_tail[1:2], low_tail[2:3] + low_tail[3:4]
+    high_fwd, high_bwd = high_tail[0:1] + high_tail[1:2], high_tail[2:3] + high_tail[3:4]
+    fwd = high_fwd * low[:HEAD] + high[:HEAD]
+    bwd = low_bwd * high[HEAD:] + low[HEAD:]
+    half = HEAD // 2
+    part = jnp.concatenate(
+        [
+            jnp.where(odd, fwd[half:], fwd[:half]),
+            jnp.where(odd, bwd[half:], bwd[:half]),
+        ],
+        axis=0,
+    )
+    out[:length] = held[...]
+    out[length : length + HEAD] = part.astype(bf16)
+    lines = (*halves(low_fwd * high_fwd), *halves(low_bwd * high_bwd))
+    out[length + HEAD :] = stacked(TAIL, lines)
 
 
 def finish_kernel(
-    place, lam, got, df_query, local, read_fwd, read_bwd, gains, hg_w, df_w, out, mixed
+    place, lam, got, other, df_query, local, read_fwd, read_bwd, gains, hg_w, df_w, out,
+    mixed, rows_w, sems
 ):
     devices = got.shape[0]
     length = local.shape[0]
     me = place[0]
+    copies = [
+        pltpu.make_async_copy(hg_w, rows_w.at[:LANES], sems.at[0]),
+        pltpu.make_async_copy(df_w, rows_w.at[LANES:], sems.at[1]),
+    ]
+    for copy in copies:
+        copy.start()
     lane = lax.broadcasted_iota(jnp.int32, (length, LANES), 1)
 
-    def folded(order, passed):
+    half = HEAD // 2
+    pair, odd = me // 2, lax.rem(me, 2) == 1
+    partner = other[: 2 * HEAD].astype(f32)
+    partner_tail = other[2 * HEAD :].astype(f32)
+
+    def folded(order, passed, k):
         state = jnp.zeros((HEAD, LANES), f32)
+        rows = slice(length + k * half, length + (k + 1) * half)
         for w in order:
-            fresh = got[w, length : length + HEAD].astype(f32)
-            tail = got[w, length + HEAD :].astype(f32)
-            decay = tail[0:1] + tail[1:2]
+            fresh = jnp.concatenate([got[2 * w, rows], got[2 * w + 1, rows]], axis=0).astype(f32)
+            tail = got[2 * w, length + HEAD :].astype(f32)
+            decay = tail[2 * k : 2 * k + 1] + tail[2 * k + 1 : 2 * k + 2]
             state = jnp.where(passed(w), decay * state + fresh, state)
-        return state.astype(bf16)
-
-    fwd = folded(range(devices), lambda w: w < me)
-    bwd = folded(range(devices - 1, -1, -1), lambda w: w > me)
+        decay = partner_tail[2 * k : 2 * k + 1] + partner_tail[2 * k + 1 : 2 * k + 2]
+        joined = decay * state + partner[k * HEAD : (k + 1) * HEAD]
+        return jnp.where(odd if k == 0 else jnp.logical_not(odd), joined, state).astype(bf16)
+
+    fwd = folded(range(devices // 2), lambda w: w < pair, 0)
+    bwd = folded(range(devices // 2 - 1, -1, -1), lambda w: w > pair, 1)
     recurrent = local[...]
     parts = []
     for h in range(2):
@@ -183,33 +220,27 @@
     mean = jnp.where(lane < HEAD, first, second) * (1.0 / HEAD)
     mixed[:, :LANES] = (recurrent * lax.rsqrt(mean + epsilon) * gains[0:1]).astype(bf16)
 
-    step = 64
     keys_values = got[:, :length, :].reshape(devices * length, LANES)
-    lane_step = lax.broadcasted_iota(jnp.int32, (step, LANES), 1)
-    lam_value = lam[0]
-
-    def attend(i, carry):
-        rows = pl.ds(pl.multiple_of(i * step, step), step)
-        query = df_query[0, rows, LANES:]
-        maps = []
-        for m in range(2):
-            inside = (lane_step >= m * DQK) & (lane_step < (m + 1) * DQK)
-            only = jnp.where(inside, query, jnp.zeros_like(query))
-            scores = dot(only, keys_values, ((1,), (1,))) * (DQK ** (-0.5))
-            shifted = jnp.exp(scores - jnp.max(scores, axis=-1, keepdims=True))
-            totals = jnp.sum(shifted, axis=-1, keepdims=True)
-            maps.append(dot(shifted.astype(bf16), keys_values, ((1,), (0,))) / totals)
-        weighted = (maps[0] - lam_value * maps[1])[:, HEAD:]
-        mean = jnp.mean(weighted * weighted, axis=-1, keepdims=True)
-        normed = (weighted * lax.rsqrt(mean + epsilon) * gains[1:2, :HEAD] * df_factor).astype(bf16)
-        mixed[rows, LANES : LANES + HEAD] = normed
-        return carry
-
-    lax.fori_loop(0, length // step, attend, 0)
-    out[...] = (
-        dot(mixed[:, :LANES], hg_w[...], ((1,), (0,)))
-        + dot(mixed[:, LANES : LANES + HEAD], df_w[...], ((1,), (0,)))
+    query = df_query[0, :, LANES:]
+    only = jnp.concatenate(
+        [
+            jnp.where((lane >= m * DQK) & (lane < (m + 1) * DQK), query, jnp.zeros_like(query))
+            for m in range(2)
+        ],
+        axis=0,
+    )
+    scores = dot(only, keys_values, ((1,), (1,))) * (DQK ** (-0.5))
+    shifted = jnp.exp(scores - jnp.max(scores, axis=-1, keepdims=True))
+    totals = jnp.sum(shifted, axis=-1, keepdims=True)
+    maps = dot(shifted.astype(bf16), keys_values, ((1,), (0,))) / totals
+    weighted = (maps[:length] - lam[0] * maps[length:])[:, HEAD:]
+    mean = jnp.mean(weighted * weighted, axis=-1, keepdims=True)
+    mixed[:, LANES:] = (
+        weighted * lax.rsqrt(mean + epsilon) * gains[1:2, :HEAD] * df_factor
     ).astype(bf16)
+    for copy in copies:
+        copy.wait()
+    out[...] = dot(mixed[...], rows_w[...], ((1,), (0,))).astype(bf16)
 
 
 def close_kernel(parts, gain, out):
@@ -283,12 +314,13 @@
 
     place = z.astype(jnp.int32)[None]
     gains = jnp.concatenate([hg_norm_gain, hg_norm_gain, df_norm_gain, df_norm_gain])
-    message, local, read_fwd, read_bwd, gains = pl.pallas_call(
+    held, states, local, read_fwd, read_bwd, gains = pl.pallas_call(
         local_kernel,
-        in_specs=[SMEM_SPEC] + [vmem] * 3,
-        out_specs=[vmem] * 5,
+        in_specs=[vmem] * 3,
+        out_specs=[vmem] * 6,
         out_shape=[
-            pltpu.VMEM((sp, length + STATE_ROWS, LANES), bf16),
+            pltpu.VMEM((length, LANES), bf16),
+            pltpu.VMEM((2 * HEAD + EXTRA, LANES), bf16),
             pltpu.VMEM((length, LANES), f32),
             pltpu.VMEM((length, LANES), bf16),
             pltpu.VMEM((length, LANES), bf16),
@@ -296,27 +328,41 @@
         ],
         compiler_params=LIMIT,
         name="local",
-    )(place, here(got), here(floor_gap), here(gains.reshape(2, LANES)))
-    arrived = lax.all_to_all(message, "sp", 0, 0, tiled=True)
+    )(here(got), here(floor_gap), here(gains.reshape(2, LANES)))
+    other = lax.ppermute(states, "sp", [(i, i ^ 1) for i in range(sp)])
+    joined = pl.pallas_call(
+        pair_kernel,
+        in_specs=[SMEM_SPEC] + [vmem] * 3,
+        out_specs=vmem,
+        out_shape=pltpu.VMEM((length + HEAD + TAIL, LANES), bf16),
+        compiler_params=LIMIT,
+        name="pair",
+    )(place, here(held), here(states), here(other))
+    arrived = lax.all_gather(joined[None], "sp", axis=0, tiled=True)
     partial = pl.pallas_call(
         finish_kernel,
-        in_specs=[SMEM_SPEC] * 2 + [vmem] * 8,
+        in_specs=[SMEM_SPEC] * 2 + [vmem] * 7 + [FAR_SPEC] * 2,
         out_specs=vmem,
         out_shape=pltpu.VMEM((length, width), bf16),
-        scratch_shapes=[pltpu.VMEM((length, 2 * LANES), bf16)],
+        scratch_shapes=[
+            pltpu.VMEM((length, LANES + HEAD), bf16),
+            pltpu.VMEM((LANES + HEAD, width), bf16),
+            pltpu.SemaphoreType.DMA((2,)),
+        ],
         compiler_params=LIMIT,
         name="finish",
     )(
         place,
         diff_lambda,
         here(arrived),
+        here(other),
         here(got),
         here(local),
         here(read_fwd),
         here(read_bwd),
         here(gains),
-        here(out_hg_w),
-        here(out_df_w),
+        there(out_hg_w),
+        there(out_df_w),
     )
     parts = lax.all_to_all(
         partial.reshape(tp, length // tp, width), "tp", 0, 0, tiled=True

time: 130 us -> 125 us (0.962)
  blocking collectives: 60.3 us -> 90.1 us
  waiting for transfers between devices: 35.7 us -> 8.59 us
  starting transfers between devices: 19.3 us -> 14.2 us
  Pallas kernels: 11.2 us -> 9.37 us
    all_to_all x1 -> x0, waiting for transfers between devices: 29.2 us -> none  [shards(): arrived = lax.all_to_all(message, 'sp', 0, 0, tiled=True)]
    all_gather x0 -> x1, blocking collectives: none -> 24.2 us  [shards(): arrived = lax.all_gather(joined[None], 'sp', axis=0, tiled=True)]
    all_to_all x1 -> x0, starting transfers between devices: 6.83 us -> none  [shards(): arrived = lax.all_to_all(message, 'sp', 0, 0, tiled=True)]
    all_to_all x1, blocking collectives: 25.3 us -> 31 us  [shards(): lax.all_to_all(partial.reshape(tp, length // tp, width), 'tp', 0, 0, tile...]
    ppermute x0 -> x1, waiting for transfers between devices: none -> 2.12 us  [shards(): other = lax.ppermute(states, 'sp', [(i, i ^ 1) for i in range(sp)])]
    ppermute x0 -> x1, starting transfers between devices: none -> 1.92 us  [shards(): other = lax.ppermute(states, 'sp', [(i, i ^ 1) for i in range(sp)])]
    pallas_call x2 -> x3, Pallas kernels: 5.67 us -> 3.9 us  [the longest x1 2.88 us: shards(): pl.pallas_call(finish_kernel, in_specs=[SMEM_SPEC] * 2 + [vmem] * 7 + [FA...]
where the time goes in v3:
time: 125 us
  blocking collectives  90.1 us (72%)
  starting transfers between devices  14.2 us (11%)
  Pallas kernels  9.37 us (7%)
  waiting for transfers between devices  8.59 us (7%)
  local copies, waits for them, and re-layouts  1.76 us (1%)
    all_gather x1, blocking collectives, shards(): weights = lax.all_gather(mine[None], 'sp', axis=0, tiled=True)  34.9 us
    all_to_all x1, blocking collectives, shards(): lax.all_to_all(partial.reshape(tp, length // tp, width), 'tp', 0, 0, tile...  31 us
    all_gather x1, blocking collectives, shards(): arrived = lax.all_gather(joined[None], 'sp', axis=0, tiled=True)  24.2 us
    all_to_all x1, waiting for transfers between devices, shards(): got = lax.all_to_all(projected, 'fs', 0, 0, tiled=True)  5.45 us
    all_to_all x1, starting transfers between devices, shards(): mine = lax.all_to_all(sent, 'fs', 0, 0, tiled=True)  5.01 us
    all_to_all x1, starting transfers between devices, shards(): got = lax.all_to_all(projected, 'fs', 0, 0, tiled=True)  3.7 us
    all_to_all x1, starting transfers between devices, shards(): rows = lax.all_to_all(normed, 'fs', 0, 0, tiled=True)  3.61 us
    pallas_call x1, Pallas kernels, shards(): pl.pallas_call(finish_kernel, in_specs=[SMEM_SPEC] * 2 + [vmem] * 7 + [FA...  2.88 us
  transfers between devices with their start and end apart: 4, of which 3 were waited for; matrix products, arithmetic and copies ran while one was open for 0% of the time, Pallas kernels for 1%

profile of v3, /device:TPU:1, one launch (start us, length us, event | category | flops | bytes accessed | tf_op | source)
XLA Modules:
  0.0 124.9 jit_solution(13695595310513565174)
XLA Ops:
  0.0 1.5 %pack.1 = bf16[4,48,128]{2,1,0:T(8,128)(2,1)} custom-call(bf16[32,128]{1,0:T(8,128)(2,1)} %q.1, bf16[32,128]{1,0:T(8,128)(2,1)} %f.1, bf16[32,128]{1,0:T(8,128)(2,1)} %b.1, bf16[32,128]{1,0:T(8,128)(2,1)} %v.1, bf16[32,64]{1,0:T(8,128)(2,1)} %dq.1, bf16[32,64]{1,0:T(8,128)(2,1)} %dk.1, bf16[32,64]{1,0:T(8,128)(2,1)} %dv.1), custom_call_target="tpu_custom_call" | custom-call | tf_op jit(solution)/shard_map/pack/pallas_call | solution.py:288
  1.6 5.0 %all-to-all-start.1 = ((bf16[4,48,128]{2,1,0:T(8,128)(2,1)}), bf16[4,48,128]{2,1,0:T(8,128)(2,1)S(1)}, u32[]{:S(2)}, u32[]{:S(2)}) async-start(bf16[4,48,128]{2,1,0:T(8,128)(2,1)} %pack.1), calls=%async_computation.1 | async-start | bytes 98304 | tf_op jit(solution)/shard_map/all_to_all | solution.py:301
  6.6 0.0 copy-start
  6.6 1.0 copy-done
  7.6 0.0 copy-start.1
  7.6 0.7 copy-done.1
  8.3 1.6 %norm.1 = bf16[4,128,2048]{2,1,0:T(8,128)(2,1)} custom-call(bf16[1,128,2048]{2,1,0:T(8,128)(2,1)S(1)} %copy-done, f32[1,2048]{1,0:T(1,128)S(1)} %bitcast.9), custom_call_target="tpu_custom_call" | custom-call | tf_op jit(solution)/shard_map/norm/pallas_call | solution.py:279
  9.9 1.0 all-to-all-done.1
  11.0 3.6 %all-to-all-start = ((bf16[4,128,2048]{2,1,0:T(8,128)(2,1)}), bf16[4,128,2048]{2,1,0:T(8,128)(2,1)S(1)}, u32[]{:S(2)}, u32[]{:S(2)}) async-start(bf16[4,128,2048]{2,1,0:T(8,128)(2,1)} %norm.1), calls=%async_computation | async-start | bytes 4194304 | tf_op jit(solution)/shard_map/all_to_all | solution.py:286
  14.6 0.0 copy-start.4
  14.6 0.0 copy-start.5
  14.6 0.0 copy-start.3
  14.6 34.9 %all-gather.weights = bf16[64,48,128]{2,1,0:T(8,128)(2,1)S(1)} all-gather(bf16[4,48,128]{2,1,0:T(8,128)(2,1)S(1)} %all-to-all-done.1), channel_id=2, replica_groups=mesh['sp'=16,'fs'=4,'tp'=8] {'sp'}, dimensions={0}, use_global_device_ids=true | all-gather | bytes 835584 | tf_op jit(solution)/shard_map/all_gather | solution.py:302
  49.5 0.0 all-to-all-done.rows
  49.6 1.5 %project.1 = bf16[4,128,256]{2,1,0:T(8,128)(2,1)} custom-call(bf16[4,128,2048]{2,1,0:T(8,128)(2,1)S(1)} %all-to-all-done.rows, bf16[64,48,128]{2,1,0:T(8,128)(2,1)S(1)} %all-gather.weights), custom_call_target="tpu_custom_call" | custom-call | tf_op jit(solution)/shard_map/project/pallas_call | solution.py:304
  51.1 3.7 %all-to-all-start.2 = ((bf16[4,128,256]{2,1,0:T(8,128)(2,1)}), bf16[4,128,256]{2,1,0:T(8,128)(2,1)S(1)}, u32[]{:S(2)}, u32[]{:S(2)}) async-start(bf16[4,128,256]{2,1,0:T(8,128)(2,1)} %project.1), calls=%async_computation.2 | async-start | bytes 524288 | tf_op jit(solution)/shard_map/all_to_all | solution.py:313
  54.7 0.0 copy-done.4
  54.8 0.0 copy-done.5
  54.8 0.1 maximum_bitcast_fusion.gains_in
  54.8 5.4 %all-to-all-done.2.got.df_query = bf16[4,128,256]{2,1,0:T(8,128)(2,1)S(1)} async-done(((bf16[4,128,256]{2,1,0:T(8,128)(2,1)}), bf16[4,128,256]{2,1,0:T(8,128)(2,1)S(1)}, u32[]{:S(2)}, u32[]{:S(2)}) %all-to-all-start.2) | async-done | bytes 262176 | tf_op jit(solution)/shard_map/all_to_all | solution.py:313
  60.3 0.0 copy-done.3
  60.3 1.0 local.1
  61.3 1.9 %collective-permute-start = (bf16[144,128]{1,0:T(8,128)(2,1)S(1)}, bf16[144,128]{1,0:T(8,128)(2,1)S(1)}, u32[]{:S(2)}, u32[]{:S(2)}) collective-permute-start(bf16[144,128]{1,0:T(8,128)(2,1)S(1)} %get-tuple-element.12.mine), channel_id=1, source_target_pairs={{0,32},{32,0},{64,96},{96,64},{128,160},{160,128},{192,224},{224,1... | collective-permute-start | bytes 110600 | tf_op jit(solution)/shard_map/ppermute | solution.py:332
  63.9 2.1 %collective-permute-done.other = bf16[144,128]{1,0:T(8,128)(2,1)S(1)} collective-permute-done((bf16[144,128]{1,0:T(8,128)(2,1)S(1)}, bf16[144,128]{1,0:T(8,128)(2,1)S(1)}, u32[]{:S(2)}, u32[]{:S(2)}) %collective-permute-start) | collective-permute-done | bytes 36896 | tf_op jit(solution)/shard_map/ppermute | solution.py:332
  66.0 0.0 copy-start.2
  66.0 24.2 %all-gather.1 = bf16[3200,128]{1,0:T(8,128)(2,1)S(1)} all-gather(bf16[200,128]{1,0:T(8,128)(2,1)S(1)} %pair.1), channel_id=3, replica_groups=mesh['sp'=16,'fs'=4,'tp'=8] {'sp'}, dimensions={0}, use_global_device_ids=true | all-gather | bytes 870400 | tf_op jit(solution)/shard_map/all_gather | solution.py:341
  90.2 2.9 %finish.1 = bf16[128,2048]{1,0:T(8,128)(2,1)S(1)} custom-call(s32[1]{0:T(128)} %bitcast.place, f32[1]{0:T(128)S(6)} %copy.17.lam, bf16[16,200,128]{2,1,0:T(8,128)(2,1)S(1)} %bitcast.7, bf16[144,128]{1,0:T(8,128)(2,1)S(1)} %collective-permute-done.other, bf16[4,128,256]{2,1,0:T(8,128)(2,1)S(1)} %all-to-all-done.2.got.df_query, ...), custom_call_target="tpu_custom_call" | custom-call | tf_op jit(solution)/shard_map/finish/pallas_call | solution.py:342
  93.1 31.0 %all_to_all.20.parts = bf16[8,16,2048]{2,1,0:T(8,128)(2,1)S(1)} all-to-all(bf16[8,16,2048]{2,1,0:T(8,128)(2,1)S(1)} %bitcast.8), channel_id=1, replica_groups=mesh['sp'=16,'fs'=4,'tp'=8] {'tp'}, dimensions={0} | all-to-all | bytes 1048576 | tf_op jit(solution)/shard_map/all_to_all | solution.py:367
  124.1 0.0 copy-done.2
  124.1 0.8 close.1
  (1 shorter events, 0.0 us)
Async XLA Ops:
  1.6 9.4 %all-to-all-start.1 = ((bf16[4,48,128]{2,1,0:T(8,128)(2,1)}), bf16[4,48,128]{2,1,0:T(8,128)(2,1)S(1)}, u32[]{:S(2)}, u32[]{:S(2)}) async-start(bf16[4,48,128]{2,1,0:T(8,128)(2,1)} %pack.1), calls=%async_computation.1 | async-start | bytes 98304 | tf_op jit(solution)/shard_map/all_to_all | solution.py:301
  6.6 1.0 copy-start
  7.6 0.7 copy-start.1
  11.0 38.6 %all-to-all-start = ((bf16[4,128,2048]{2,1,0:T(8,128)(2,1)}), bf16[4,128,2048]{2,1,0:T(8,128)(2,1)S(1)}, u32[]{:S(2)}, u32[]{:S(2)}) async-start(bf16[4,128,2048]{2,1,0:T(8,128)(2,1)} %norm.1), calls=%async_computation | async-start | bytes 4194304 | tf_op jit(solution)/shard_map/all_to_all | solution.py:286
  14.6 40.2 %copy-start.4 = (f32[64]{0:T(128)S(1)}, f32[64]{0:T(128)}, u32[]{:S(2)}) copy-start(f32[64]{0:T(128)} %param.28) | copy-start | bytes 772
  14.6 40.2 %copy-start.5 = (f32[64]{0:T(128)S(1)}, f32[64]{0:T(128)}, u32[]{:S(2)}) copy-start(f32[64]{0:T(128)} %param.23) | copy-start | bytes 772
  14.6 45.7 %copy-start.3 = (f32[2,128]{1,0:T(2,128)S(1)}, f32[2,128]{1,0:T(2,128)}, u32[]{:S(2)}) copy-start(f32[2,128]{1,0:T(2,128)} %gaps.1) | copy-start | bytes 3076
  51.1 9.2 %all-to-all-start.2 = ((bf16[4,128,256]{2,1,0:T(8,128)(2,1)}), bf16[4,128,256]{2,1,0:T(8,128)(2,1)S(1)}, u32[]{:S(2)}, u32[]{:S(2)}) async-start(bf16[4,128,256]{2,1,0:T(8,128)(2,1)} %project.1), calls=%async_computation.2 | async-start | bytes 524288 | tf_op jit(solution)/shard_map/all_to_all | solution.py:313
  61.3 4.7 %collective-permute-start = (bf16[144,128]{1,0:T(8,128)(2,1)S(1)}, bf16[144,128]{1,0:T(8,128)(2,1)S(1)}, u32[]{:S(2)}, u32[]{:S(2)}) collective-permute-start(bf16[144,128]{1,0:T(8,128)(2,1)S(1)} %get-tuple-element.12.mine), channel_id=1, source_target_pairs={{0,32},{32,0},{64,96},{96,64},{128,160},{160,128},{192,224},{224,1... | collective-permute-start | bytes 110600 | tf_op jit(solution)/shard_map/ppermute | solution.py:332
  66.0 58.1 %copy-start.2 = (f32[2048]{0:T(1024)S(1)}, f32[2048]{0:T(1024)}, u32[]{:S(2)}) copy-start(f32[2048]{0:T(1024)} %param.31) | copy-start | bytes 24580

commit v4 on v3

--- a/solution.py
+++ b/solution.py
@@ -8,7 +8,6 @@
 HEAD = 64
 DQK = 32
 LANES = 128
-EXTRA = 16
 TAIL = 8
 
 epsilon = 1e-06
@@ -55,17 +54,26 @@
         out[j] = jnp.concatenate([wide[j], folded], axis=0)
 
 
-def norm_kernel(x, gain, out):
-    rows = x[0].astype(f32)
-    scale = lax.rsqrt(jnp.mean(rows * rows, axis=-1, keepdims=True) + epsilon)
-    done = (rows * scale * gain[...]).astype(bf16)
+def norm_kernel(x, gain_in, out, rows, gain, sems):
+    copies = (
+        pltpu.make_async_copy(x.at[0], rows, sems.at[0]),
+        pltpu.make_async_copy(gain_in, gain, sems.at[1]),
+    )
+    for copy in copies:
+        copy.start()
+    for copy in copies:
+        copy.wait()
+    part = rows[...].astype(f32)
+    scale = lax.rsqrt(jnp.mean(part * part, axis=-1, keepdims=True) + epsilon)
+    done = (part * scale * gain[...]).astype(bf16)
     for k in range(out.shape[0]):
         out[k] = done
 
 
-def project_kernel(rows, weights, out, rhs):
+def project_kernel(place, rows, weights, out, rhs):
     blocks, packed, _ = weights.shape
     depth = packed * 2 // 3
+    half = depth // 2
     wide = weights[:, :depth, :]
     narrow = weights[:, depth:, :].astype(f32)
     first, second = narrow[:, :, :HEAD], narrow[:, :, HEAD:]
@@ -78,54 +86,95 @@
     ).astype(bf16)
     rhs[:, :LANES] = wide.reshape(blocks * depth, LANES)
     rhs[:, LANES:] = narrow.reshape(blocks * depth, LANES)
-    for k in range(rows.shape[0]):
-        out[k] = dot(rows[k], rhs[...], ((1,), (0,))).astype(bf16)
-
-
-def local_kernel(got, gaps, gains_in, held, states, local, read_fwd, read_bwd, gains):
+    count, length, width = rows.shape
+    whole = dot(rows[...].reshape(count * length, width), rhs[...], ((1,), (0,))).astype(bf16)
+    half = length // 2
+    lane = lax.broadcasted_iota(jnp.int32, (half, LANES), 1)
+    turned = jnp.where(place[0] == 2, HEAD, 0)
+    early = lax.rem(lane + turned, LANES) < HEAD
+    for k in range(count):
+        part = whole[k * length : (k + 1) * length]
+        folded = jnp.where(early, part[:half, LANES:], part[half:, LANES:])
+        for a in range(2):
+            out[a, k, :length] = part[:, :LANES]
+            out[a, k, length:] = folded
+
+
+def swapped(block):
+    return jnp.concatenate([block[:, HEAD:], block[:, :HEAD]], axis=1)
+
+
+def local_kernel(
+    place, got, gaps, gains_in, out, other, query_out, local, read_fwd, read_bwd, gains
+):
     gains[...] = gains_in[...]
-    length = got.shape[1]
+    length = local.shape[0]
+    half = length // 2
+    odd = place[0] == 1
+    mine = place[0] * 4
     row = lax.broadcasted_iota(jnp.int32, (length, length), 0)
     col = lax.broadcasted_iota(jnp.int32, (length, length), 1)
     lane = lax.broadcasted_iota(jnp.int32, (length, LANES), 1)
     lane_head = lax.broadcasted_iota(jnp.int32, (HEAD, LANES), 1)
-    lower, upper = row >= col, row <= col
-    queries = got[0, :, :LANES].astype(f32)
+    masks = row >= col, row <= col
+    takens, gones, states, decays = ({}, {}, {}, {})
+    for slot in range(2):
+        values = got[4 * slot + 3, :length]
+        for d in range(2):
+            gate = got[4 * slot + 1 + d, :length].astype(f32)
+            taken = gaps[d : d + 1, :] * jax.nn.sigmoid(-gate)
+            kept = jnp.log1p(-taken)
+            gone = dot(masks[d].astype(f32), kept, ((1,), (0,)), lax.Precision.HIGHEST)
+            total = gone[length - 1 : length] if d == 0 else gone[0:1]
+            state = dot(values, (taken * jnp.exp(total - gone)).astype(bf16), ((0,), (0,)))
+            takens[slot, d], gones[slot, d] = taken, gone
+            states[slot, d] = jnp.where(lane_head < HEAD, state[:HEAD], state[HEAD:])
+            decays[slot, d] = jnp.exp(total)
+    fwd = decays[1, 0] * states[0, 0] + states[1, 0]
+    bwd = decays[0, 1] * states[1, 1] + states[0, 1]
+    quarter = HEAD // 2
+    part = jnp.concatenate(
+        [
+            jnp.where(odd, fwd[quarter:], fwd[:quarter]),
+            jnp.where(odd, bwd[quarter:], bwd[:quarter]),
+        ],
+        axis=0,
+    )
+    out[length : length + HEAD] = part.astype(bf16)
+    lines = (*halves(decays[0, 0] * decays[1, 0]), *halves(decays[0, 1] * decays[1, 1]))
+    out[length + HEAD :] = stacked(TAIL, lines)
+    other[:HEAD] = states[0, 0]
+    other[HEAD : 2 * HEAD] = states[1, 1]
+    row_tail = lax.broadcasted_iota(jnp.int32, (TAIL, LANES), 0)
+    other[2 * HEAD :] = jnp.where(row_tail == 0, decays[0, 0], decays[1, 1])
+
+    keys, worth = got[mine + 1, length:], got[mine + 2, length:]
+    lane_half = lane[:half]
+    out[:half] = jnp.where(lane_half < HEAD, keys, worth)
+    out[half:length] = swapped(jnp.where(lane_half < HEAD, worth, keys))
+    folded = got[mine, length:]
+    query_out[:half] = folded
+    query_out[half:] = swapped(folded)
+
+    queries = got[mine, :length].astype(f32)
     queries = queries * jax.nn.sigmoid(queries)
-    values = got[3, :, :LANES]
-    pieces = []
-    for j, mask in ((1, lower), (2, upper)):
-        gate = got[j, :, :LANES].astype(f32)
-        taken = gaps[j - 1 : j, :] * jax.nn.sigmoid(-gate)
-        kept = jnp.log1p(-taken)
-        gone = dot(mask.astype(f32), kept, ((1,), (0,)), lax.Precision.HIGHEST)
-        total = gone[length - 1 : length] if j == 1 else gone[0:1]
-        middle = gone[length // 2 : length // 2 + 1]
-        decay = jnp.exp(total)
-        state = dot(
-            values, (taken * jnp.exp(total - gone)).astype(bf16), ((0,), (0,))
-        )
-        state = jnp.where(lane_head < HEAD, state[:HEAD], state[HEAD:])
-        reader = read_fwd if j == 1 else read_bwd
+    values = got[mine + 3, :length]
+    weights = [0.0, 0.0]
+    for d in range(2):
+        gone = jnp.where(odd, gones[1, d], gones[0, d])
+        taken = jnp.where(odd, takens[1, d], takens[0, d])
+        reader = read_bwd if d else read_fwd
         reader[...] = (queries * jnp.exp(gone)).astype(bf16)
-        high = decay.astype(bf16)
-        low = (decay - high.astype(f32)).astype(bf16)
-        pieces.append((state, high, low))
+        middle = gone[half : half + 1]
         query_part = queries * jnp.exp(gone - middle)
         key_part = (taken * jnp.exp(middle - gone)).astype(bf16)
         for h in range(2):
             inside = (lane >= h * HEAD) & (lane < (h + 1) * HEAD)
-            score = dot(
-                jnp.where(inside, query_part, 0.0).astype(bf16), key_part, ((1,), (1,))
-            )
-            pieces.append(jnp.where(mask, score, 0.0))
-    (fwd, fwd_0, fwd_1, bwd, bwd_0, bwd_1) = pieces
-    out_0 = dot((fwd_0 + bwd_0).astype(bf16), values, ((1,), (0,)))
-    out_1 = dot((fwd_1 + bwd_1).astype(bf16), values, ((1,), (0,)))
+            score = dot(jnp.where(inside, query_part, 0.0).astype(bf16), key_part, ((1,), (1,)))
+            weights[h] = weights[h] + jnp.where(masks[d], score, 0.0)
+    out_0 = dot(weights[0].astype(bf16), values, ((1,), (0,)))
+    out_1 = dot(weights[1].astype(bf16), values, ((1,), (0,)))
     local[...] = jnp.where(lane < HEAD, out_0, out_1)
-    held[...] = jnp.where(lane < HEAD, got[1, :, LANES:], got[2, :, LANES:])
-    states[: 2 * HEAD] = jnp.concatenate([fwd[0], bwd[0]], axis=0).astype(bf16)
-    states[2 * HEAD :] = stacked(EXTRA, (fwd[1], fwd[2], bwd[1], bwd[2]))
 
 
 def stacked(count, lines):
@@ -139,35 +188,6 @@
 def halves(value):
     high = value.astype(bf16)
     return high, (value - high.astype(f32)).astype(bf16)
-
-
-def pair_kernel(place, held, mine, other, out):
-    length = held.shape[0]
-    odd = lax.rem(place[0], 2) == 1
-    mine_all = mine[: 2 * HEAD].astype(f32)
-    other_all = other[: 2 * HEAD].astype(f32)
-    low = jnp.where(odd, other_all, mine_all)
-    high = jnp.where(odd, mine_all, other_all)
-    mine_tail = mine[2 * HEAD :].astype(f32)
-    other_tail = other[2 * HEAD :].astype(f32)
-    low_tail = jnp.where(odd, other_tail, mine_tail)
-    high_tail = jnp.where(odd, mine_tail, other_tail)
-    low_fwd, low_bwd = low_tail[0:1] + low_tail[1:2], low_tail[2:3] + low_tail[3:4]
-    high_fwd, high_bwd = high_tail[0:1] + high_tail[1:2], high_tail[2:3] + high_tail[3:4]
-    fwd = high_fwd * low[:HEAD] + high[:HEAD]
-    bwd = low_bwd * high[HEAD:] + low[HEAD:]
-    half = HEAD // 2
-    part = jnp.concatenate(
-        [
-            jnp.where(odd, fwd[half:], fwd[:half]),
-            jnp.where(odd, bwd[half:], bwd[:half]),
-        ],
-        axis=0,
-    )
-    out[:length] = held[...]
-    out[length : length + HEAD] = part.astype(bf16)
-    lines = (*halves(low_fwd * high_fwd), *halves(low_bwd * high_bwd))
-    out[length + HEAD :] = stacked(TAIL, lines)
 
 
 def finish_kernel(
@@ -187,8 +207,6 @@
 
     half = HEAD // 2
     pair, odd = me // 2, lax.rem(me, 2) == 1
-    partner = other[: 2 * HEAD].astype(f32)
-    partner_tail = other[2 * HEAD :].astype(f32)
 
     def folded(order, passed, k):
         state = jnp.zeros((HEAD, LANES), f32)
@@ -198,8 +216,8 @@
             tail = got[2 * w, length + HEAD :].astype(f32)
             decay = tail[2 * k : 2 * k + 1] + tail[2 * k + 1 : 2 * k + 2]
             state = jnp.where(passed(w), decay * state + fresh, state)
-        decay = partner_tail[2 * k : 2 * k + 1] + partner_tail[2 * k + 1 : 2 * k + 2]
-        joined = decay * state + partner[k * HEAD : (k + 1) * HEAD]
+        decay = other[2 * HEAD + k : 2 * HEAD + k + 1]
+        joined = decay * state + other[k * HEAD : (k + 1) * HEAD]
         return jnp.where(odd if k == 0 else jnp.logical_not(odd), joined, state).astype(bf16)
 
     fwd = folded(range(devices // 2), lambda w: w < pair, 0)
@@ -221,7 +239,7 @@
     mixed[:, :LANES] = (recurrent * lax.rsqrt(mean + epsilon) * gains[0:1]).astype(bf16)
 
     keys_values = got[:, :length, :].reshape(devices * length, LANES)
-    query = df_query[0, :, LANES:]
+    query = df_query[...]
     only = jnp.concatenate(
         [
             jnp.where((lane >= m * DQK) & (lane < (m + 1) * DQK), query, jnp.zeros_like(query))
@@ -270,7 +288,7 @@
     post_gain,
 ):
     sp, fs, tp = (lax.axis_size(a) for a in ("sp", "fs", "tp"))
-    z = lax.axis_index("sp")
+    z, y = lax.axis_index("sp"), lax.axis_index("fs")
     _, length, width = inputs.shape
     depth = hg_query_w.shape[0]
     packed = depth + depth // 2
@@ -278,11 +296,17 @@
     vmem = VMEM_SPEC
     normed = pl.pallas_call(
         norm_kernel,
+        in_specs=[FAR_SPEC] * 2,
+        out_specs=vmem,
         out_shape=pltpu.VMEM((fs, length, width), bf16),
+        scratch_shapes=[
+            pltpu.VMEM((length, width), bf16),
+            pltpu.VMEM((1, width), f32),
+            pltpu.SemaphoreType.DMA((2,)),
+        ],
         compiler_params=LIMIT,
         name="norm",
-    )(inputs, norm_gain[None])
-
+    )(there(inputs), there(norm_gain[None]))
     rows = lax.all_to_all(normed, "fs", 0, 0, tiled=True)
     sources = (hg_query_w, hg_fwd_w, hg_bwd_w, hg_value_w, df_query_w, df_key_w, df_value_w)
     sent = pl.pallas_call(
@@ -303,24 +327,33 @@
     weights = weights.reshape(sp * fs, packed, LANES)
     projected = pl.pallas_call(
         project_kernel,
-        in_specs=[vmem] * 2,
+        in_specs=[SMEM_SPEC] + [vmem] * 2,
         out_specs=vmem,
-        out_shape=pltpu.VMEM((fs, length, 2 * LANES), bf16),
+        out_shape=pltpu.VMEM((2, fs, length + length // 2, LANES), bf16),
         scratch_shapes=[pltpu.VMEM((width, 2 * LANES), bf16)],
         compiler_params=LIMIT,
         name="project",
-    )(here(rows), here(weights))
-    got = lax.all_to_all(projected, "fs", 0, 0, tiled=True)
+    )(y.astype(jnp.int32)[None], here(rows), here(weights))
+    groups = [[2 * fs * i + k for k in range(2 * fs)] for i in range(sp // 2)]
+    got = lax.all_to_all(
+        projected.reshape(2 * fs, length + length // 2, LANES),
+        ("sp", "fs"),
+        0,
+        0,
+        axis_index_groups=groups,
+        tiled=True,
+    )
 
     place = z.astype(jnp.int32)[None]
     gains = jnp.concatenate([hg_norm_gain, hg_norm_gain, df_norm_gain, df_norm_gain])
-    held, states, local, read_fwd, read_bwd, gains = pl.pallas_call(
+    joined, other, query, local, read_fwd, read_bwd, gains = pl.pallas_call(
         local_kernel,
-        in_specs=[vmem] * 3,
-        out_specs=[vmem] * 6,
+        in_specs=[SMEM_SPEC] + [vmem] * 3,
+        out_specs=[vmem] * 7,
         out_shape=[
+            pltpu.VMEM((length + HEAD + TAIL, LANES), bf16),
+            pltpu.VMEM((2 * HEAD + TAIL, LANES), f32),
             pltpu.VMEM((length, LANES), bf16),
-            pltpu.VMEM((2 * HEAD + EXTRA, LANES), bf16),
             pltpu.VMEM((length, LANES), f32),
             pltpu.VMEM((length, LANES), bf16),
             pltpu.VMEM((length, LANES), bf16),
@@ -328,16 +361,7 @@
         ],
         compiler_params=LIMIT,
         name="local",
-    )(here(got), here(floor_gap), here(gains.reshape(2, LANES)))
-    other = lax.ppermute(states, "sp", [(i, i ^ 1) for i in range(sp)])
-    joined = pl.pallas_call(
-        pair_kernel,
-        in_specs=[SMEM_SPEC] + [vmem] * 3,
-        out_specs=vmem,
-        out_shape=pltpu.VMEM((length + HEAD + TAIL, LANES), bf16),
-        compiler_params=LIMIT,
-        name="pair",
-    )(place, here(held), here(states), here(other))
+    )(place % 2, here(got), here(floor_gap), here(gains.reshape(2, LANES)))
     arrived = lax.all_gather(joined[None], "sp", axis=0, tiled=True)
     partial = pl.pallas_call(
         finish_kernel,
@@ -356,7 +380,7 @@
         diff_lambda,
         here(arrived),
         here(other),
-        here(got),
+        here(query),
         here(local),
         here(read_fwd),
         here(read_bwd),
@@ -396,6 +420,4 @@
         P(),
     )
     out_specs = P("fs", ("sp", "tp"), None)
-    return jax.shard_map(
-        shards, mesh=mesh, in_specs=in_specs, out_specs=out_specs, check_vma=False
-    )
+    return jax.shard_map(shards, mesh=mesh, in_specs=in_specs, out_specs=out_specs, check_vma=False)

time: 125 us -> 121 us (0.968)
  starting transfers between devices: 14.2 us -> 12.3 us
  local copies, waits for them, and re-layouts: 1.76 us -> 0.02 us
  Pallas kernels: 9.37 us -> 10.9 us
    ppermute x1 -> x0, waiting for transfers between devices: 2.12 us -> none  [shards(): other = lax.ppermute(states, 'sp', [(i, i ^ 1) for i in range(sp)])]
    ppermute x1 -> x0, starting transfers between devices: 1.92 us -> none  [shards(): other = lax.ppermute(states, 'sp', [(i, i ^ 1) for i in range(sp)])]
    all_to_all x1, blocking collectives: 31 us -> 29.1 us  [shards(): lax.all_to_all(partial.reshape(tp, length // tp, width), 'tp', 0, 0, tile...]
    unnamed x12 -> x8, local copies, waits for them, and re-layouts: 1.76 us -> 0.02 us
    pallas_call x4 -> x3, Pallas kernels: 4.15 us -> 5.64 us  [the longest x1 2.64 us: shards(): pl.pallas_call(norm_kernel, in_specs=[FAR_SPEC] * 2, out_specs=vmem, out_...]
  transfers between devices with their start and end apart: 4 -> 3, of which waited for: 3 -> 2; matrix products, arithmetic and copies ran while one was open for 0% -> 0% of each run, Pallas kernels for 1% -> 2%
where the time goes in v4:
time: 121 us
  blocking collectives  89.3 us (74%)
  starting transfers between devices  12.3 us (10%)
  Pallas kernels  10.9 us (9%)
  waiting for transfers between devices  7.59 us (6%)
    all_gather x1, blocking collectives, shards(): weights = lax.all_gather(mine[None], 'sp', axis=0, tiled=True)  34.8 us
    all_to_all x1, blocking collectives, shards(): lax.all_to_all(partial.reshape(tp, length // tp, width), 'tp', 0, 0, tile...  29.1 us
    all_gather x1, blocking collectives, shards(): arrived = lax.all_gather(joined[None], 'sp', axis=0, tiled=True)  25.4 us
    all_to_all x1, waiting for transfers between devices, shards(): lax.all_to_all(projected.reshape(2 * fs, length + length // 2, LANES), ('...  5.85 us
    all_to_all x1, starting transfers between devices, shards(): mine = lax.all_to_all(sent, 'fs', 0, 0, tiled=True)  5.01 us
    all_to_all x1, starting transfers between devices, shards(): lax.all_to_all(projected.reshape(2 * fs, length + length // 2, LANES), ('...  3.69 us
    all_to_all x1, starting transfers between devices, shards(): rows = lax.all_to_all(normed, 'fs', 0, 0, tiled=True)  3.61 us
    pallas_call x1, Pallas kernels, shards(): pl.pallas_call(finish_kernel, in_specs=[SMEM_SPEC] * 2 + [vmem] * 7 + [FA...  2.89 us
  transfers between devices with their start and end apart: 3, of which 2 were waited for; matrix products, arithmetic and copies ran while one was open for 0% of the time, Pallas kernels for 2%

profile of v4, /device:TPU:1, one launch (start us, length us, event | category | flops | bytes accessed | tf_op | source)
XLA Modules:
  0.0 120.9 jit_solution(12889604993158541038)
XLA Ops:
  0.0 1.5 %pack.1 = bf16[4,48,128]{2,1,0:T(8,128)(2,1)} custom-call(bf16[32,128]{1,0:T(8,128)(2,1)} %q.1, bf16[32,128]{1,0:T(8,128)(2,1)} %f.1, bf16[32,128]{1,0:T(8,128)(2,1)} %b.1, bf16[32,128]{1,0:T(8,128)(2,1)} %v.1, bf16[32,64]{1,0:T(8,128)(2,1)} %dq.1, bf16[32,64]{1,0:T(8,128)(2,1)} %dk.1, bf16[32,64]{1,0:T(8,128)(2,1)} %dv.1), custom_call_target="tpu_custom_call" | custom-call | tf_op jit(solution)/shard_map/pack/pallas_call | solution.py:312
  1.6 5.0 %all-to-all-start.1 = ((bf16[4,48,128]{2,1,0:T(8,128)(2,1)}), bf16[4,48,128]{2,1,0:T(8,128)(2,1)S(1)}, u32[]{:S(2)}, u32[]{:S(2)}) async-start(bf16[4,48,128]{2,1,0:T(8,128)(2,1)} %pack.1), calls=%async_computation.1 | async-start | bytes 98304 | tf_op jit(solution)/shard_map/all_to_all | solution.py:325
  6.6 2.6 %norm.1 = bf16[4,128,2048]{2,1,0:T(8,128)(2,1)} custom-call(bf16[1,128,2048]{2,1,0:T(8,128)(2,1)} %x.1, f32[1,2048]{1,0:T(1,128)} %bitcast.12), custom_call_target="tpu_custom_call" | custom-call | tf_op jit(solution)/shard_map/norm/pallas_call | solution.py:297
  9.2 1.7 %all-to-all-done.1 = bf16[4,48,128]{2,1,0:T(8,128)(2,1)S(1)} async-done(((bf16[4,48,128]{2,1,0:T(8,128)(2,1)}), bf16[4,48,128]{2,1,0:T(8,128)(2,1)S(1)}, u32[]{:S(2)}, u32[]{:S(2)}) %all-to-all-start.1) | async-done | bytes 49184 | tf_op jit(solution)/shard_map/all_to_all | solution.py:325
  11.0 3.6 %all-to-all-start = ((bf16[4,128,2048]{2,1,0:T(8,128)(2,1)}), bf16[4,128,2048]{2,1,0:T(8,128)(2,1)S(1)}, u32[]{:S(2)}, u32[]{:S(2)}) async-start(bf16[4,128,2048]{2,1,0:T(8,128)(2,1)} %norm.1), calls=%async_computation | async-start | bytes 4194304 | tf_op jit(solution)/shard_map/all_to_all | solution.py:310
  14.6 34.8 %all-gather.weights = bf16[64,48,128]{2,1,0:T(8,128)(2,1)S(1)} all-gather(bf16[4,48,128]{2,1,0:T(8,128)(2,1)S(1)} %all-to-all-done.1), channel_id=2, replica_groups=mesh['sp'=16,'fs'=4,'tp'=8] {'sp'}, dimensions={0}, use_global_device_ids=true | all-gather | bytes 835584 | tf_op jit(solution)/shard_map/all_gather | solution.py:326
  49.4 0.0 copy-start.2
  49.4 0.0 copy-start.3
  49.4 0.0 copy-start.1
  49.4 0.0 all-to-all-done.rows
  49.4 1.6 %project.1 = bf16[2,4,192,128]{3,2,1,0:T(8,128)(2,1)} custom-call(s32[1]{0:T(128)} %bitcast.1.place, bf16[4,128,2048]{2,1,0:T(8,128)(2,1)S(1)} %all-to-all-done.rows, bf16[64,48,128]{2,1,0:T(8,128)(2,1)S(1)} %all-gather.weights), custom_call_target="tpu_custom_call" | custom-call | tf_op jit(solution)/shard_map/project/pallas_call | solution.py:328
  51.0 3.7 %all-to-all-start.2 = ((bf16[8,192,128]{2,1,0:T(8,128)(2,1)}), bf16[8,192,128]{2,1,0:T(8,128)(2,1)S(1)}, u32[]{:S(2)}, u32[]{:S(2)}) async-start(bf16[8,192,128]{2,1,0:T(8,128)(2,1)} %bitcast.3), calls=%async_computation.2 | async-start | bytes 786432 | tf_op jit(solution)/shard_map/all_to_all | solution.py:338
  55.4 0.0 copy-done.2
  55.4 0.0 copy-done.3
  55.4 0.1 maximum_bitcast_fusion.gains_in
  55.5 5.8 %all-to-all-done.2.got = bf16[8,192,128]{2,1,0:T(8,128)(2,1)S(1)} async-done(((bf16[8,192,128]{2,1,0:T(8,128)(2,1)}), bf16[8,192,128]{2,1,0:T(8,128)(2,1)S(1)}, u32[]{:S(2)}, u32[]{:S(2)}) %all-to-all-start.2) | async-done | bytes 393248 | tf_op jit(solution)/shard_map/all_to_all | solution.py:338
  61.3 0.0 copy-done.1
  61.3 1.4 %local.1 = (bf16[200,128]{1,0:T(8,128)(2,1)S(1)}, f32[136,128]{1,0:T(8,128)S(1)}, bf16[128,128]{1,0:T(8,128)(2,1)S(1)}, f32[128,128]{1,0:T(8,128)S(1)}, bf16[128...) custom-call(s32[1]{0:T(128)S(6)} %select_n.7.place, ...), custom_call_target="tpu_custom_call" | custom-call | tf_op jit(solution)/shard_map/local/pallas_call | solution.py:349
  62.7 0.0 copy-start
  62.7 25.4 %all-gather.1 = bf16[3200,128]{1,0:T(8,128)(2,1)S(1)} all-gather(bf16[200,128]{1,0:T(8,128)(2,1)S(1)} %get-tuple-element.12), channel_id=3, replica_groups=mesh['sp'=16,'fs'=4,'tp'=8] {'sp'}, dimensions={0}, use_global_device_ids=true | all-gather | bytes 870400 | tf_op jit(solution)/shard_map/all_gather | solution.py:365
  88.1 2.9 %finish.1 = bf16[128,2048]{1,0:T(8,128)(2,1)S(1)} custom-call(s32[1]{0:T(128)} %bitcast.place, f32[1]{0:T(128)S(6)} %copy.17.lam, bf16[16,200,128]{2,1,0:T(8,128)(2,1)S(1)} %bitcast.9, f32[136,128]{1,0:T(8,128)S(1)} %get-tuple-element.13.other, bf16[128,128]{1,0:T(8,128)(2,1)S(1)} %get-tuple-element.14.df_query, f32[128,128]{1,0:T(8,128)S(1)} %get-tuple-element.15.local, ...), custom_call_target="tpu_custom_call" | custom-call | tf_op jit(solution)/shard_map/finish/pallas_call | solution.py:366
  91.0 29.1 %all_to_all.20.parts = bf16[8,16,2048]{2,1,0:T(8,128)(2,1)S(1)} all-to-all(bf16[8,16,2048]{2,1,0:T(8,128)(2,1)S(1)} %bitcast.10), channel_id=1, replica_groups=mesh['sp'=16,'fs'=4,'tp'=8] {'tp'}, dimensions={0} | all-to-all | bytes 1048576 | tf_op jit(solution)/shard_map/all_to_all | solution.py:391
  120.1 0.0 copy-done
  120.1 0.8 close.1
Async XLA Ops:
  1.6 9.4 %all-to-all-start.1 = ((bf16[4,48,128]{2,1,0:T(8,128)(2,1)}), bf16[4,48,128]{2,1,0:T(8,128)(2,1)S(1)}, u32[]{:S(2)}, u32[]{:S(2)}) async-start(bf16[4,48,128]{2,1,0:T(8,128)(2,1)} %pack.1), calls=%async_computation.1 | async-start | bytes 98304 | tf_op jit(solution)/shard_map/all_to_all | solution.py:325
  11.0 38.5 %all-to-all-start = ((bf16[4,128,2048]{2,1,0:T(8,128)(2,1)}), bf16[4,128,2048]{2,1,0:T(8,128)(2,1)S(1)}, u32[]{:S(2)}, u32[]{:S(2)}) async-start(bf16[4,128,2048]{2,1,0:T(8,128)(2,1)} %norm.1), calls=%async_computation | async-start | bytes 4194304 | tf_op jit(solution)/shard_map/all_to_all | solution.py:310
  49.4 5.9 %copy-start.2 = (f32[64]{0:T(128)S(1)}, f32[64]{0:T(128)}, u32[]{:S(2)}) copy-start(f32[64]{0:T(128)} %param.28) | copy-start | bytes 772
  49.4 6.0 %copy-start.3 = (f32[64]{0:T(128)S(1)}, f32[64]{0:T(128)}, u32[]{:S(2)}) copy-start(f32[64]{0:T(128)} %param.23) | copy-start | bytes 772
  49.4 11.9 %copy-start.1 = (f32[2,128]{1,0:T(2,128)S(1)}, f32[2,128]{1,0:T(2,128)}, u32[]{:S(2)}) copy-start(f32[2,128]{1,0:T(2,128)} %gaps.1) | copy-start | bytes 3076
  51.0 10.3 %all-to-all-start.2 = ((bf16[8,192,128]{2,1,0:T(8,128)(2,1)}), bf16[8,192,128]{2,1,0:T(8,128)(2,1)S(1)}, u32[]{:S(2)}, u32[]{:S(2)}) async-start(bf16[8,192,128]{2,1,0:T(8,128)(2,1)} %bitcast.3), calls=%async_computation.2 | async-start | bytes 786432 | tf_op jit(solution)/shard_map/all_to_all | solution.py:338
  62.7 57.4 %copy-start = (f32[2048]{0:T(1024)S(1)}, f32[2048]{0:T(1024)}, u32[]{:S(2)}) copy-start(f32[2048]{0:T(1024)} %param.31) | copy-start | bytes 24580

commit v5 on v4

--- a/solution.py
+++ b/solution.py
@@ -9,6 +9,7 @@
 DQK = 32
 LANES = 128
 TAIL = 8
+EXTRA = 16
 
 epsilon = 1e-06
 df_factor = 0.8
@@ -35,23 +36,37 @@
     return lax.dot_general(a, b, (dims, ((), ())), precision=precision, preferred_element_type=f32)
 
 
-def pack_kernel(q, f, b, v, dq, dk, dv, out, wide, narrow, sems):
+def thirds(value):
+    pieces = []
+    for _ in range(3):
+        pieces.append(value.astype(bf16))
+        value = value - pieces[-1].astype(f32)
+    return pieces
+
+
+def pack_kernel(lam, q, f, b, v, dq, dk, dv, gaps_in, out, wide, narrow, gaps, sems):
     copies = [
         pltpu.make_async_copy(source, wide.at[j], sems.at[j])
         for j, source in enumerate((q, f, b, v))
     ] + [
         pltpu.make_async_copy(source, narrow.at[j], sems.at[4 + j])
         for j, source in enumerate((dq, dk, dv))
-    ]
+    ] + [pltpu.make_async_copy(gaps_in, gaps, sems.at[7])]
     for copy in copies:
         copy.start()
     for copy in copies:
         copy.wait()
     half = q.shape[0] // 2
+    extra = stacked(
+        EXTRA,
+        (*thirds(gaps[0:1]), *thirds(gaps[1:2]), *thirds(jnp.full((1, LANES), lam[0], f32))),
+    )
     for j in range(4):
         k = j % 3
         folded = jnp.concatenate([narrow[k, :half, :], narrow[k, half:, :]], axis=1)
-        out[j] = jnp.concatenate([wide[j], folded], axis=0)
+        block = jnp.concatenate([wide[j], folded, extra], axis=0)
+        for c in range(2):
+            out[c, j] = block
 
 
 def norm_kernel(x, gain_in, out, rows, gain, sems):
@@ -105,9 +120,12 @@
 
 
 def local_kernel(
-    place, got, gaps, gains_in, out, other, query_out, local, read_fwd, read_bwd, gains
+    place, got, extra_in, gains_in, out, other, query_out, local, read_fwd, read_bwd, gains
 ):
-    gains[...] = gains_in[...]
+    extra = extra_in[...].astype(f32)
+    gaps = [extra[3 * d : 3 * d + 1] + extra[3 * d + 1 : 3 * d + 2] + extra[3 * d + 2 : 3 * d + 3] for d in range(3)]
+    gains[:2] = gains_in[...]
+    gains[2:] = gaps[2]
     length = local.shape[0]
     half = length // 2
     odd = place[0] == 1
@@ -122,7 +140,7 @@
         values = got[4 * slot + 3, :length]
         for d in range(2):
             gate = got[4 * slot + 1 + d, :length].astype(f32)
-            taken = gaps[d : d + 1, :] * jax.nn.sigmoid(-gate)
+            taken = gaps[d] * jax.nn.sigmoid(-gate)
             kept = jnp.log1p(-taken)
             gone = dot(masks[d].astype(f32), kept, ((1,), (0,)), lax.Precision.HIGHEST)
             total = gone[length - 1 : length] if d == 0 else gone[0:1]
@@ -191,18 +209,11 @@
 
 
 def finish_kernel(
-    place, lam, got, other, df_query, local, read_fwd, read_bwd, gains, hg_w, df_w, out,
-    mixed, rows_w, sems
+    place, got, other, df_query, local, read_fwd, read_bwd, gains, hg_w, df_w, out, mixed
 ):
     devices = got.shape[0]
     length = local.shape[0]
     me = place[0]
-    copies = [
-        pltpu.make_async_copy(hg_w, rows_w.at[:LANES], sems.at[0]),
-        pltpu.make_async_copy(df_w, rows_w.at[LANES:], sems.at[1]),
-    ]
-    for copy in copies:
-        copy.start()
     lane = lax.broadcasted_iota(jnp.int32, (length, LANES), 1)
 
     half = HEAD // 2
@@ -251,14 +262,15 @@
     shifted = jnp.exp(scores - jnp.max(scores, axis=-1, keepdims=True))
     totals = jnp.sum(shifted, axis=-1, keepdims=True)
     maps = dot(shifted.astype(bf16), keys_values, ((1,), (0,))) / totals
-    weighted = (maps[:length] - lam[0] * maps[length:])[:, HEAD:]
+    weighted = (maps[:length] - gains[2:3] * maps[length:])[:, HEAD:]
     mean = jnp.mean(weighted * weighted, axis=-1, keepdims=True)
     mixed[:, LANES:] = (
         weighted * lax.rsqrt(mean + epsilon) * gains[1:2, :HEAD] * df_factor
     ).astype(bf16)
-    for copy in copies:
-        copy.wait()
-    out[...] = dot(mixed[...], rows_w[...], ((1,), (0,))).astype(bf16)
+    out[...] = (
+        dot(mixed[:, :LANES], hg_w[...], ((1,), (0,)))
+        + dot(mixed[:, LANES:], df_w[...], ((1,), (0,)))
+    ).astype(bf16)
 
 
 def close_kernel(parts, gain, out):
@@ -311,19 +323,35 @@
     sources = (hg_query_w, hg_fwd_w, hg_bwd_w, hg_value_w, df_query_w, df_key_w, df_value_w)
     sent = pl.pallas_call(
         pack_kernel,
-        in_specs=[FAR_SPEC] * 7,
+        in_specs=[SMEM_SPEC] + [FAR_SPEC] * 8,
         out_specs=vmem,
-        out_shape=pltpu.VMEM((fs, packed, LANES), bf16),
+        out_shape=pltpu.VMEM((2, fs, packed + EXTRA, LANES), bf16),
         scratch_shapes=[
             pltpu.VMEM((4, depth, LANES), bf16),
             pltpu.VMEM((3, depth, LANES // 2), bf16),
-            pltpu.SemaphoreType.DMA((7,)),
+            pltpu.VMEM((2, LANES), f32),
+            pltpu.SemaphoreType.DMA((8,)),
         ],
         compiler_params=LIMIT,
         name="pack",
-    )(*map(there, sources))
-    mine = lax.all_to_all(sent, "fs", 0, 0, tiled=True)
-    weights = lax.all_gather(mine[None], "sp", axis=0, tiled=True)
+    )(diff_lambda, *map(there, (*sources, floor_gap)))
+    share = (lax.axis_index("tp") + z) % 2
+    both = lax.all_to_all(
+        sent.reshape(2 * fs, packed + EXTRA, LANES),
+        ("fs", "tp"),
+        0,
+        0,
+        axis_index_groups=[
+            [k * tp + 2 * x + c for c in range(2) for k in range(fs)] for x in range(tp // 2)
+        ],
+        tiled=True,
+    )
+    mine = lax.dynamic_slice_in_dim(both, share * fs, fs, 0)
+    extra = mine[0, packed:]
+    rings = [[k * tp + (t ^ (k % 2)) for k in range(sp)] for t in range(tp)]
+    weights = lax.all_gather(
+        mine[None, :, :packed], ("sp", "tp"), axis=0, tiled=True, axis_index_groups=rings
+    )
     weights = weights.reshape(sp * fs, packed, LANES)
     projected = pl.pallas_call(
         project_kernel,
@@ -334,15 +362,22 @@
         compiler_params=LIMIT,
         name="project",
     )(y.astype(jnp.int32)[None], here(rows), here(weights))
-    groups = [[2 * fs * i + k for k in range(2 * fs)] for i in range(sp // 2)]
+    groups = [
+        [((2 * i + a) * fs + k) * tp + (t ^ a) for a in range(2) for k in range(fs)]
+        for i in range(sp // 2)
+        for t in range(tp)
+    ]
     got = lax.all_to_all(
         projected.reshape(2 * fs, length + length // 2, LANES),
-        ("sp", "fs"),
+        ("sp", "fs", "tp"),
         0,
         0,
         axis_index_groups=groups,
         tiled=True,
     )
+    swap = [(k * tp + t, k * tp + (t ^ (k % 2))) for k in range(sp) for t in range(tp)]
+    hg_rows = lax.ppermute(out_hg_w, ("sp", "tp"), swap)
+    df_rows = lax.ppermute(out_df_w, ("sp", "tp"), swap)
 
     place = z.astype(jnp.int32)[None]
     gains = jnp.concatenate([hg_norm_gain, hg_norm_gain, df_norm_gain, df_norm_gain])
@@ -357,27 +392,24 @@
             pltpu.VMEM((length, LANES), f32),
             pltpu.VMEM((length, LANES), bf16),
             pltpu.VMEM((length, LANES), bf16),
-            pltpu.VMEM((2, LANES), f32),
+            pltpu.VMEM((3, LANES), f32),
         ],
         compiler_params=LIMIT,
         name="local",
-    )(place % 2, here(got), here(floor_gap), here(gains.reshape(2, LANES)))
-    arrived = lax.all_gather(joined[None], "sp", axis=0, tiled=True)
+    )(place % 2, here(got), here(extra), here(gains.reshape(2, LANES)))
+    arrived = lax.all_gather(
+        joined[None], ("sp", "tp"), axis=0, tiled=True, axis_index_groups=rings
+    )
     partial = pl.pallas_call(
         finish_kernel,
-        in_specs=[SMEM_SPEC] * 2 + [vmem] * 7 + [FAR_SPEC] * 2,
+        in_specs=[SMEM_SPEC] + [vmem] * 9,
         out_specs=vmem,
         out_shape=pltpu.VMEM((length, width), bf16),
-        scratch_shapes=[
-            pltpu.VMEM((length, LANES + HEAD), bf16),
-            pltpu.VMEM((LANES + HEAD, width), bf16),
-            pltpu.SemaphoreType.DMA((2,)),
-        ],
+        scratch_shapes=[pltpu.VMEM((length, LANES + HEAD), bf16)],
         compiler_params=LIMIT,
         name="finish",
     )(
         place,
-        diff_lambda,
         here(arrived),
         here(other),
         here(query),
@@ -385,8 +417,8 @@
         here(read_fwd),
         here(read_bwd),
         here(gains),
-        there(out_hg_w),
-        there(out_df_w),
+        here(hg_rows),
+        here(df_rows),
     )
     parts = lax.all_to_all(
         partial.reshape(tp, length // tp, width), "tp", 0, 0, tiled=True

time: 121 us -> 118 us (0.975)
  blocking collectives: 89.3 us -> 78.2 us
  starting transfers between devices: 12.3 us -> 20.1 us
    all_to_all x1, blocking collectives: 29.1 us -> 13.5 us  [shards(): lax.all_to_all(partial.reshape(tp, length // tp, width), 'tp', 0, 0, tile...]
    all_to_all x1, starting transfers between devices: 5.01 us -> 10.1 us  [shards(): lax.all_to_all(sent.reshape(2 * fs, packed + EXTRA, LANES), ('fs', 'tp'),...]
    all_gather x2, blocking collectives: 60.2 us -> 64.7 us  [the longest x1 34.2 us: shards(): lax.all_gather(mine[None, :, :packed], ('sp', 'tp'), axis=0, tiled=True,...]
    ppermute x0 -> x2, starting transfers between devices: none -> 2.3 us  [the longest x1 1.61 us: shards(): df_rows = lax.ppermute(out_df_w, ('sp', 'tp'), swap)]
  transfers between devices with their start and end apart: 3 -> 5, of which waited for: 2 -> 2; matrix products, arithmetic and copies ran while one was open for 0% -> 0% of each run, Pallas kernels for 2% -> 3%
where the time goes in v5:
time: 118 us
  blocking collectives  78.2 us (66%)
  starting transfers between devices  20.1 us (17%)
  Pallas kernels  9.94 us (8%)
  waiting for transfers between devices  8.66 us (7%)
    all_gather x1, blocking collectives, shards(): lax.all_gather(mine[None, :, :packed], ('sp', 'tp'), axis=0, tiled=True,...  34.2 us
    all_gather x1, blocking collectives, shards(): lax.all_gather(joined[None], ('sp', 'tp'), axis=0, tiled=True, axis_index...  30.4 us
    all_to_all x1, blocking collectives, shards(): lax.all_to_all(partial.reshape(tp, length // tp, width), 'tp', 0, 0, tile...  13.5 us
    all_to_all x1, starting transfers between devices, shards(): lax.all_to_all(sent.reshape(2 * fs, packed + EXTRA, LANES), ('fs', 'tp'),...  10.1 us
    all_to_all x1, waiting for transfers between devices, shards(): lax.all_to_all(projected.reshape(2 * fs, length + length // 2, LANES), ('...  6.11 us
    all_to_all x1, starting transfers between devices, shards(): lax.all_to_all(projected.reshape(2 * fs, length + length // 2, LANES), ('...  4.05 us
    all_to_all x1, starting transfers between devices, shards(): rows = lax.all_to_all(normed, 'fs', 0, 0, tiled=True)  3.61 us
    pallas_call x1, Pallas kernels, shards(): pl.pallas_call(norm_kernel, in_specs=[FAR_SPEC] * 2, out_specs=vmem, out_...  2.64 us
  transfers between devices with their start and end apart: 5, of which 2 were waited for; matrix products, arithmetic and copies ran while one was open for 0% of the time, Pallas kernels for 3%

profile of v5, /device:TPU:1, one launch (start us, length us, event | category | flops | bytes accessed | tf_op | source)
XLA Modules:
  0.0 117.8 jit_solution(1914479210739536003)
XLA Ops:
  0.7 1.6 %pack.1 = bf16[2,4,64,128]{3,2,1,0:T(8,128)(2,1)} custom-call(f32[1]{0:T(128)S(6)} %copy.17.lam, bf16[32,128]{1,0:T(8,128)(2,1)} %q.1, bf16[32,128]{1,0:T(8,128)(2,1)} %f.1, bf16[32,128]{1,0:T(8,128)(2,1)} %b.1, bf16[32,128]{1,0:T(8,128)(2,1)} %v.1, bf16[32,64]{1,0:T(8,128)(2,1)} %dq.1, bf16[32,64]{1,0:T(8,128)(2,1)} %dk.1, bf16[32,64]{1,0:T(8,128)(2,1)} %dv.1, ...), custom_call_target="tpu_custom_call" | custom-call | tf_op jit(solution)/shard_map/pack/pallas_call | solution.py:324
  2.2 10.1 %all-to-all-start.1 = ((bf16[8,64,128]{2,1,0:T(8,128)(2,1)}), bf16[8,64,128]{2,1,0:T(8,128)(2,1)S(1)}, u32[]{:S(2)}, u32[]{:S(2)}) async-start(bf16[8,64,128]{2,1,0:T(8,128)(2,1)} %bitcast.3), calls=%async_computation.1 | async-start | bytes 262144 | tf_op jit(solution)/shard_map/all_to_all | solution.py:339
  12.4 2.6 %norm.1 = bf16[4,128,2048]{2,1,0:T(8,128)(2,1)} custom-call(bf16[1,128,2048]{2,1,0:T(8,128)(2,1)} %x.1, f32[1,2048]{1,0:T(1,128)} %bitcast.15), custom_call_target="tpu_custom_call" | custom-call | tf_op jit(solution)/shard_map/norm/pallas_call | solution.py:309
  15.0 2.6 %all-to-all-done.1 = bf16[8,64,128]{2,1,0:T(8,128)(2,1)S(1)} async-done(((bf16[8,64,128]{2,1,0:T(8,128)(2,1)}), bf16[8,64,128]{2,1,0:T(8,128)(2,1)S(1)}, u32[]{:S(2)}, u32[]{:S(2)}) %all-to-all-start.1) | async-done | bytes 131104 | tf_op jit(solution)/shard_map/all_to_all | solution.py:339
  17.6 3.6 %all-to-all-start = ((bf16[4,128,2048]{2,1,0:T(8,128)(2,1)}), bf16[4,128,2048]{2,1,0:T(8,128)(2,1)S(1)}, u32[]{:S(2)}, u32[]{:S(2)}) async-start(bf16[4,128,2048]{2,1,0:T(8,128)(2,1)} %norm.1), calls=%async_computation | async-start | bytes 4194304 | tf_op jit(solution)/shard_map/all_to_all | solution.py:322
  21.2 34.2 %all-gather.weights = bf16[64,48,128]{2,1,0:T(8,128)(2,1)S(1)} all-gather(bf16[4,48,128]{2,1,0:T(8,128)(2,1)S(1)} %constant_dynamic-slice_fusion), channel_id=2, replica_groups={{0,33,64,97,128,161,192,225,256,289,320,353,384,417,448,481},{1,32,65,9..., dimensions={0}, use_global_device_ids=true | all-gather | bytes 835584 | tf_op jit(solution)/shard_map/all_gather | solution.py:352
  55.4 0.0 copy-start.3
  55.4 0.0 copy-start.1
  55.4 0.0 copy-start.2
  55.5 0.0 all-to-all-done.rows
  55.5 1.6 %project.1 = bf16[2,4,192,128]{3,2,1,0:T(8,128)(2,1)} custom-call(s32[1]{0:T(128)} %bitcast.1.place, bf16[4,128,2048]{2,1,0:T(8,128)(2,1)S(1)} %all-to-all-done.rows, bf16[64,48,128]{2,1,0:T(8,128)(2,1)S(1)} %all-gather.weights), custom_call_target="tpu_custom_call" | custom-call | tf_op jit(solution)/shard_map/project/pallas_call | solution.py:356
  57.0 4.0 %all-to-all-start.2 = ((bf16[8,192,128]{2,1,0:T(8,128)(2,1)}), bf16[8,192,128]{2,1,0:T(8,128)(2,1)S(1)}, u32[]{:S(2)}, u32[]{:S(2)}) async-start(bf16[8,192,128]{2,1,0:T(8,128)(2,1)} %bitcast.4), calls=%async_computation.2 | async-start | bytes 786432 | tf_op jit(solution)/shard_map/all_to_all | solution.py:370
  61.1 0.0 copy-done.3
  61.1 0.7 collective-permute-start
  61.8 1.6 %collective-permute-start.1 = (bf16[64,2048]{1,0:T(8,128)(2,1)}, bf16[64,2048]{1,0:T(8,128)(2,1)S(1)}, u32[]{:S(2)}, u32[]{:S(2)}) collective-permute-start(bf16[64,2048]{1,0:T(8,128)(2,1)} %param.30), channel_id=1, source_target_pairs={{0,0},{1,1},{2,2},{3,3},{4,4},{5,5},{6,6},{7,7},{32,33},{33,32},{3... | collective-permute-start | bytes 786440 | tf_op jit(solution)/shard_map/ppermute | solution.py:380
  63.4 0.0 copy-done.1
  63.4 0.0 copy-done.2
  63.4 0.1 maximum_bitcast_fusion.gains_in
  63.5 6.1 %all-to-all-done.2.got = bf16[8,192,128]{2,1,0:T(8,128)(2,1)S(1)} async-done(((bf16[8,192,128]{2,1,0:T(8,128)(2,1)}), bf16[8,192,128]{2,1,0:T(8,128)(2,1)S(1)}, u32[]{:S(2)}, u32[]{:S(2)}) %all-to-all-start.2) | async-done | bytes 393248 | tf_op jit(solution)/shard_map/all_to_all | solution.py:370
  69.6 1.4 %local.1 = (bf16[200,128]{1,0:T(8,128)(2,1)S(1)}, f32[136,128]{1,0:T(8,128)S(1)}, bf16[128,128]{1,0:T(8,128)(2,1)S(1)}, f32[128,128]{1,0:T(8,128)S(1)}, bf16[128...) custom-call(s32[1]{0:T(128)S(6)} %select_n.16.place, ...), custom_call_target="tpu_custom_call" | custom-call | tf_op jit(solution)/shard_map/local/pallas_call | solution.py:384
  71.0 0.0 copy-start
  71.0 30.4 %all-gather.1 = bf16[3200,128]{1,0:T(8,128)(2,1)S(1)} all-gather(bf16[200,128]{1,0:T(8,128)(2,1)S(1)} %get-tuple-element.12), channel_id=3, replica_groups={{0,33,64,97,128,161,192,225,256,289,320,353,384,417,448,481},{1,32,65,9..., dimensions={0}, use_global_device_ids=true | all-gather | bytes 870400 | tf_op jit(solution)/shard_map/all_gather | solution.py:400
  101.5 0.0 collective-permute-done.1.df_w
  101.5 0.0 collective-permute-done.hg_w
  101.5 1.9 %finish.1 = bf16[128,2048]{1,0:T(8,128)(2,1)S(1)} custom-call(s32[1]{0:T(128)} %bitcast.place, bf16[16,200,128]{2,1,0:T(8,128)(2,1)S(1)} %bitcast.12, f32[136,128]{1,0:T(8,128)S(1)} %get-tuple-element.13.other, bf16[128,128]{1,0:T(8,128)(2,1)S(1)} %get-tuple-element.14.df_query, f32[128,128]{1,0:T(8,128)S(1)} %get-tuple-element.15.local, ...), custom_call_target="tpu_custom_call" | custom-call | tf_op jit(solution)/shard_map/finish/pallas_call | solution.py:403
  103.4 13.5 %all_to_all.20.parts = bf16[8,16,2048]{2,1,0:T(8,128)(2,1)S(1)} all-to-all(bf16[8,16,2048]{2,1,0:T(8,128)(2,1)S(1)} %bitcast.13), channel_id=1, replica_groups=mesh['sp'=16,'fs'=4,'tp'=8] {'tp'}, dimensions={0} | all-to-all | bytes 1048576 | tf_op jit(solution)/shard_map/all_to_all | solution.py:423
  116.9 0.0 copy-done
  117.0 0.8 close.1
  (2 shorter events, 0.0 us)
Async XLA Ops:
  2.2 15.3 %all-to-all-start.1 = ((bf16[8,64,128]{2,1,0:T(8,128)(2,1)}), bf16[8,64,128]{2,1,0:T(8,128)(2,1)S(1)}, u32[]{:S(2)}, u32[]{:S(2)}) async-start(bf16[8,64,128]{2,1,0:T(8,128)(2,1)} %bitcast.3), calls=%async_computation.1 | async-start | bytes 262144 | tf_op jit(solution)/shard_map/all_to_all | solution.py:339
  17.6 37.9 %all-to-all-start = ((bf16[4,128,2048]{2,1,0:T(8,128)(2,1)}), bf16[4,128,2048]{2,1,0:T(8,128)(2,1)S(1)}, u32[]{:S(2)}, u32[]{:S(2)}) async-start(bf16[4,128,2048]{2,1,0:T(8,128)(2,1)} %norm.1), calls=%async_computation | async-start | bytes 4194304 | tf_op jit(solution)/shard_map/all_to_all | solution.py:322
  55.4 5.6 %copy-start.3 = (bf16[128,2048]{1,0:T(8,128)(2,1)S(1)}, bf16[128,2048]{1,0:T(8,128)(2,1)}, u32[]{:S(2)}) copy-start(bf16[128,2048]{1,0:T(8,128)(2,1)} %param.29) | copy-start | bytes 1572868
  55.4 8.0 %copy-start.1 = (f32[64]{0:T(128)S(1)}, f32[64]{0:T(128)}, u32[]{:S(2)}) copy-start(f32[64]{0:T(128)} %param.28) | copy-start | bytes 772
  55.4 8.0 %copy-start.2 = (f32[64]{0:T(128)S(1)}, f32[64]{0:T(128)}, u32[]{:S(2)}) copy-start(f32[64]{0:T(128)} %param.23) | copy-start | bytes 772
  57.0 12.6 %all-to-all-start.2 = ((bf16[8,192,128]{2,1,0:T(8,128)(2,1)}), bf16[8,192,128]{2,1,0:T(8,128)(2,1)S(1)}, u32[]{:S(2)}, u32[]{:S(2)}) async-start(bf16[8,192,128]{2,1,0:T(8,128)(2,1)} %bitcast.4), calls=%async_computation.2 | async-start | bytes 786432 | tf_op jit(solution)/shard_map/all_to_all | solution.py:370
  61.1 40.4 %collective-permute-start = (bf16[128,2048]{1,0:T(8,128)(2,1)S(1)}, bf16[128,2048]{1,0:T(8,128)(2,1)S(1)}, u32[]{:S(2)}, u32[]{:S(2)}) collective-permute-start(bf16[128,2048]{1,0:T(8,128)(2,1)S(1)} %copy-done.3), channel_id=1, source_target_pairs={{0,0},{1,1},{2,2},{3,3},{4,4},{5,5},{6,6},{7,7},{32,33},{33,32},{3... | collective-permute-start | bytes 1572872 | tf_op jit(solution)/shard_map/ppermute | solution.py:379
  61.8 39.7 %collective-permute-start.1 = (bf16[64,2048]{1,0:T(8,128)(2,1)}, bf16[64,2048]{1,0:T(8,128)(2,1)S(1)}, u32[]{:S(2)}, u32[]{:S(2)}) collective-permute-start(bf16[64,2048]{1,0:T(8,128)(2,1)} %param.30), channel_id=1, source_target_pairs={{0,0},{1,1},{2,2},{3,3},{4,4},{5,5},{6,6},{7,7},{32,33},{33,32},{3... | collective-permute-start | bytes 786440 | tf_op jit(solution)/shard_map/ppermute | solution.py:380
  71.0 45.9 %copy-start = (f32[2048]{0:T(1024)S(1)}, f32[2048]{0:T(1024)}, u32[]{:S(2)}) copy-start(f32[2048]{0:T(1024)} %param.31) | copy-start | bytes 24580

commit v6 on v5

--- a/solution.py
+++ b/solution.py
@@ -44,7 +44,7 @@
     return pieces
 
 
-def pack_kernel(lam, q, f, b, v, dq, dk, dv, gaps_in, out, wide, narrow, gaps, sems):
+def pack_kernel(q, f, b, v, dq, dk, dv, gaps_in, out, wide, narrow, gaps, sems):
     copies = [
         pltpu.make_async_copy(source, wide.at[j], sems.at[j])
         for j, source in enumerate((q, f, b, v))
@@ -57,10 +57,7 @@
     for copy in copies:
         copy.wait()
     half = q.shape[0] // 2
-    extra = stacked(
-        EXTRA,
-        (*thirds(gaps[0:1]), *thirds(gaps[1:2]), *thirds(jnp.full((1, LANES), lam[0], f32))),
-    )
+    extra = stacked(EXTRA, (*thirds(gaps[0:1]), *thirds(gaps[1:2])))
     for j in range(4):
         k = j % 3
         folded = jnp.concatenate([narrow[k, :half, :], narrow[k, half:, :]], axis=1)
@@ -120,12 +117,11 @@
 
 
 def local_kernel(
-    place, got, extra_in, gains_in, out, other, query_out, local, read_fwd, read_bwd, gains
+    place, lam, got, extra_in, gains_in, out, other, query_out, local, read_fwd, read_bwd, gains
 ):
     extra = extra_in[...].astype(f32)
-    gaps = [extra[3 * d : 3 * d + 1] + extra[3 * d + 1 : 3 * d + 2] + extra[3 * d + 2 : 3 * d + 3] for d in range(3)]
-    gains[:2] = gains_in[...]
-    gains[2:] = gaps[2]
+    gaps = [extra[3 * d : 3 * d + 1] + extra[3 * d + 1 : 3 * d + 2] + extra[3 * d + 2 : 3 * d + 3] for d in range(2)]
+    gains[...] = gains_in[...]
     length = local.shape[0]
     half = length // 2
     odd = place[0] == 1
@@ -160,6 +156,7 @@
     )
     out[length : length + HEAD] = part.astype(bf16)
     lines = (*halves(decays[0, 0] * decays[1, 0]), *halves(decays[0, 1] * decays[1, 1]))
+    lines = (*lines, *thirds(jnp.full((1, LANES), lam[0], f32)))
     out[length + HEAD :] = stacked(TAIL, lines)
     other[:HEAD] = states[0, 0]
     other[HEAD : 2 * HEAD] = states[1, 1]
@@ -262,7 +259,9 @@
     shifted = jnp.exp(scores - jnp.max(scores, axis=-1, keepdims=True))
     totals = jnp.sum(shifted, axis=-1, keepdims=True)
     maps = dot(shifted.astype(bf16), keys_values, ((1,), (0,))) / totals
-    weighted = (maps[:length] - gains[2:3] * maps[length:])[:, HEAD:]
+    first = got[0, length + HEAD :].astype(f32)
+    lam = first[4:5] + first[5:6] + first[6:7]
+    weighted = (maps[:length] - lam * maps[length:])[:, HEAD:]
     mean = jnp.mean(weighted * weighted, axis=-1, keepdims=True)
     mixed[:, LANES:] = (
         weighted * lax.rsqrt(mean + epsilon) * gains[1:2, :HEAD] * df_factor
@@ -323,7 +322,7 @@
     sources = (hg_query_w, hg_fwd_w, hg_bwd_w, hg_value_w, df_query_w, df_key_w, df_value_w)
     sent = pl.pallas_call(
         pack_kernel,
-        in_specs=[SMEM_SPEC] + [FAR_SPEC] * 8,
+        in_specs=[FAR_SPEC] * 8,
         out_specs=vmem,
         out_shape=pltpu.VMEM((2, fs, packed + EXTRA, LANES), bf16),
         scratch_shapes=[
@@ -334,8 +333,8 @@
         ],
         compiler_params=LIMIT,
         name="pack",
-    )(diff_lambda, *map(there, (*sources, floor_gap)))
-    share = (lax.axis_index("tp") + z) % 2
+    )(*map(there, (*sources, floor_gap)))
+    share = (lax.axis_index("tp") + z // 2) % 2
     both = lax.all_to_all(
         sent.reshape(2 * fs, packed + EXTRA, LANES),
         ("fs", "tp"),
@@ -348,7 +347,7 @@
     )
     mine = lax.dynamic_slice_in_dim(both, share * fs, fs, 0)
     extra = mine[0, packed:]
-    rings = [[k * tp + (t ^ (k % 2)) for k in range(sp)] for t in range(tp)]
+    rings = [[k * tp + (t ^ (k // 2 % 2)) for k in range(sp)] for t in range(tp)]
     weights = lax.all_gather(
         mine[None, :, :packed], ("sp", "tp"), axis=0, tiled=True, axis_index_groups=rings
     )
@@ -363,7 +362,7 @@
         name="project",
     )(y.astype(jnp.int32)[None], here(rows), here(weights))
     groups = [
-        [((2 * i + a) * fs + k) * tp + (t ^ a) for a in range(2) for k in range(fs)]
+        [((2 * i + a) * fs + k) * tp + t for a in range(2) for k in range(fs)]
         for i in range(sp // 2)
         for t in range(tp)
     ]
@@ -375,7 +374,7 @@
         axis_index_groups=groups,
         tiled=True,
     )
-    swap = [(k * tp + t, k * tp + (t ^ (k % 2))) for k in range(sp) for t in range(tp)]
+    swap = [(k * tp + t, k * tp + (t ^ (k // 2 % 2))) for k in range(sp) for t in range(tp)]
     hg_rows = lax.ppermute(out_hg_w, ("sp", "tp"), swap)
     df_rows = lax.ppermute(out_df_w, ("sp", "tp"), swap)
 
@@ -383,7 +382,7 @@
     gains = jnp.concatenate([hg_norm_gain, hg_norm_gain, df_norm_gain, df_norm_gain])
     joined, other, query, local, read_fwd, read_bwd, gains = pl.pallas_call(
         local_kernel,
-        in_specs=[SMEM_SPEC] + [vmem] * 3,
+        in_specs=[SMEM_SPEC] * 2 + [vmem] * 3,
         out_specs=[vmem] * 7,
         out_shape=[
             pltpu.VMEM((length + HEAD + TAIL, LANES), bf16),
@@ -392,11 +391,11 @@
             pltpu.VMEM((length, LANES), f32),
             pltpu.VMEM((length, LANES), bf16),
             pltpu.VMEM((length, LANES), bf16),
-            pltpu.VMEM((3, LANES), f32),
+            pltpu.VMEM((2, LANES), f32),
         ],
         compiler_params=LIMIT,
         name="local",
-    )(place % 2, here(got), here(extra), here(gains.reshape(2, LANES)))
+    )(place % 2, diff_lambda, here(got), here(extra), here(gains.reshape(2, LANES)))
     arrived = lax.all_gather(
         joined[None], ("sp", "tp"), axis=0, tiled=True, axis_index_groups=rings
     )

time: 118 us -> 117 us (level)
  waiting for transfers between devices: 8.66 us -> 6.85 us
    all_to_all x1, waiting for transfers between devices: 6.11 us -> 4.29 us  [shards(): lax.all_to_all(projected.reshape(2 * fs, length + length // 2, LANES), ('...]
where the time goes in v6:
time: 117 us
  blocking collectives  79.1 us (68%)
  starting transfers between devices  20 us (17%)
  Pallas kernels  9.94 us (8%)
  waiting for transfers between devices  6.85 us (6%)
    all_gather x1, blocking collectives, shards(): lax.all_gather(mine[None, :, :packed], ('sp', 'tp'), axis=0, tiled=True,...  34.2 us
    all_gather x1, blocking collectives, shards(): lax.all_gather(joined[None], ('sp', 'tp'), axis=0, tiled=True, axis_index...  31.4 us
    all_to_all x1, blocking collectives, shards(): lax.all_to_all(partial.reshape(tp, length // tp, width), 'tp', 0, 0, tile...  13.6 us
    all_to_all x1, starting transfers between devices, shards(): lax.all_to_all(sent.reshape(2 * fs, packed + EXTRA, LANES), ('fs', 'tp'),...  10.1 us
    all_to_all x1, waiting for transfers between devices, shards(): lax.all_to_all(projected.reshape(2 * fs, length + length // 2, LANES), ('...  4.29 us
    all_to_all x1, starting transfers between devices, shards(): lax.all_to_all(projected.reshape(2 * fs, length + length // 2, LANES), ('...  3.91 us
    all_to_all x1, starting transfers between devices, shards(): rows = lax.all_to_all(normed, 'fs', 0, 0, tiled=True)  3.61 us
    pallas_call x1, Pallas kernels, shards(): pl.pallas_call(norm_kernel, in_specs=[FAR_SPEC] * 2, out_specs=vmem, out_...  2.64 us
  transfers between devices with their start and end apart: 5, of which 2 were waited for; matrix products, arithmetic and copies ran while one was open for 0% of the time, Pallas kernels for 3%

profile of v6, /device:TPU:1, one launch (start us, length us, event | category | flops | bytes accessed | tf_op | source)
XLA Modules:
  0.0 116.8 jit_solution(11836415415660124293)
XLA Ops:
  0.0 1.6 %pack.1 = bf16[2,4,64,128]{3,2,1,0:T(8,128)(2,1)} custom-call(bf16[32,128]{1,0:T(8,128)(2,1)} %q.1, bf16[32,128]{1,0:T(8,128)(2,1)} %f.1, bf16[32,128]{1,0:T(8,128)(2,1)} %b.1, bf16[32,128]{1,0:T(8,128)(2,1)} %v.1, bf16[32,64]{1,0:T(8,128)(2,1)} %dq.1, bf16[32,64]{1,0:T(8,128)(2,1)} %dk.1, bf16[32,64]{1,0:T(8,128)(2,1)} %dv.1, f32[2,128]{1,0:T(2,128)} %gaps_in.1), custom_call_target="tpu_custom_call" | custom-call | tf_op jit(solution)/shard_map/pack/pallas_call | solution.py:323
  1.6 10.1 %all-to-all-start.1 = ((bf16[8,64,128]{2,1,0:T(8,128)(2,1)}), bf16[8,64,128]{2,1,0:T(8,128)(2,1)S(1)}, u32[]{:S(2)}, u32[]{:S(2)}) async-start(bf16[8,64,128]{2,1,0:T(8,128)(2,1)} %bitcast.3), calls=%async_computation.1 | async-start | bytes 262144 | tf_op jit(solution)/shard_map/all_to_all | solution.py:338
  11.7 2.6 %norm.1 = bf16[4,128,2048]{2,1,0:T(8,128)(2,1)} custom-call(bf16[1,128,2048]{2,1,0:T(8,128)(2,1)} %x.1, f32[1,2048]{1,0:T(1,128)} %bitcast.15), custom_call_target="tpu_custom_call" | custom-call | tf_op jit(solution)/shard_map/norm/pallas_call | solution.py:308
  14.4 2.6 %all-to-all-done.1 = bf16[8,64,128]{2,1,0:T(8,128)(2,1)S(1)} async-done(((bf16[8,64,128]{2,1,0:T(8,128)(2,1)}), bf16[8,64,128]{2,1,0:T(8,128)(2,1)S(1)}, u32[]{:S(2)}, u32[]{:S(2)}) %all-to-all-start.1) | async-done | bytes 131104 | tf_op jit(solution)/shard_map/all_to_all | solution.py:338
  16.9 3.6 %all-to-all-start = ((bf16[4,128,2048]{2,1,0:T(8,128)(2,1)}), bf16[4,128,2048]{2,1,0:T(8,128)(2,1)S(1)}, u32[]{:S(2)}, u32[]{:S(2)}) async-start(bf16[4,128,2048]{2,1,0:T(8,128)(2,1)} %norm.1), calls=%async_computation | async-start | bytes 4194304 | tf_op jit(solution)/shard_map/all_to_all | solution.py:321
  20.6 34.2 %all-gather.weights = bf16[64,48,128]{2,1,0:T(8,128)(2,1)S(1)} all-gather(bf16[4,48,128]{2,1,0:T(8,128)(2,1)S(1)} %constant_dynamic-slice_fusion), channel_id=2, replica_groups={{0,32,65,97,128,160,193,225,256,288,321,353,384,416,449,481},{1,33,64,9..., dimensions={0}, use_global_device_ids=true | all-gather | bytes 835584 | tf_op jit(solution)/shard_map/all_gather | solution.py:351
  54.8 0.0 copy-start.3
  54.8 0.0 copy-start.1
  54.8 0.0 copy-start.2
  54.8 0.0 all-to-all-done.rows
  54.8 1.6 %project.1 = bf16[2,4,192,128]{3,2,1,0:T(8,128)(2,1)} custom-call(s32[1]{0:T(128)} %bitcast.1.place, bf16[4,128,2048]{2,1,0:T(8,128)(2,1)S(1)} %all-to-all-done.rows, bf16[64,48,128]{2,1,0:T(8,128)(2,1)S(1)} %all-gather.weights), custom_call_target="tpu_custom_call" | custom-call | tf_op jit(solution)/shard_map/project/pallas_call | solution.py:355
  56.4 3.9 %all-to-all-start.2 = ((bf16[8,192,128]{2,1,0:T(8,128)(2,1)}), bf16[8,192,128]{2,1,0:T(8,128)(2,1)S(1)}, u32[]{:S(2)}, u32[]{:S(2)}) async-start(bf16[8,192,128]{2,1,0:T(8,128)(2,1)} %bitcast.4), calls=%async_computation.2 | async-start | bytes 786432 | tf_op jit(solution)/shard_map/all_to_all | solution.py:369
  60.3 0.0 copy-done.3
  60.3 0.7 collective-permute-start
  61.0 1.6 %collective-permute-start.1 = (bf16[64,2048]{1,0:T(8,128)(2,1)}, bf16[64,2048]{1,0:T(8,128)(2,1)S(1)}, u32[]{:S(2)}, u32[]{:S(2)}) collective-permute-start(bf16[64,2048]{1,0:T(8,128)(2,1)} %param.30), channel_id=1, source_target_pairs={{0,0},{1,1},{2,2},{3,3},{4,4},{5,5},{6,6},{7,7},{32,32},{33,33},{3... | collective-permute-start | bytes 786440 | tf_op jit(solution)/shard_map/ppermute | solution.py:379
  62.6 0.0 copy-done.1
  62.6 0.0 copy-done.2
  62.6 0.1 maximum_bitcast_fusion.gains_in
  63.4 4.3 %all-to-all-done.2.got = bf16[8,192,128]{2,1,0:T(8,128)(2,1)S(1)} async-done(((bf16[8,192,128]{2,1,0:T(8,128)(2,1)}), bf16[8,192,128]{2,1,0:T(8,128)(2,1)S(1)}, u32[]{:S(2)}, u32[]{:S(2)}) %all-to-all-start.2) | async-done | bytes 393248 | tf_op jit(solution)/shard_map/all_to_all | solution.py:369
  67.7 1.4 %local.1 = (bf16[200,128]{1,0:T(8,128)(2,1)S(1)}, f32[136,128]{1,0:T(8,128)S(1)}, bf16[128,128]{1,0:T(8,128)(2,1)S(1)}, f32[128,128]{1,0:T(8,128)S(1)}, bf16[128...) custom-call(s32[1]{0:T(128)S(6)} %select_n.20.place, f32[1]{0:T(128)S(6)} %copy.17.lam, ...), custom_call_target="tpu_custom_call" | custom-call | tf_op jit(solution)/shard_map/local/pallas_call | solution.py:383
  69.1 0.0 copy-start
  69.1 31.4 %all-gather.1 = bf16[3200,128]{1,0:T(8,128)(2,1)S(1)} all-gather(bf16[200,128]{1,0:T(8,128)(2,1)S(1)} %get-tuple-element.12), channel_id=3, replica_groups={{0,32,65,97,128,160,193,225,256,288,321,353,384,416,449,481},{1,33,64,9..., dimensions={0}, use_global_device_ids=true | all-gather | bytes 870400 | tf_op jit(solution)/shard_map/all_gather | solution.py:399
  100.5 0.0 collective-permute-done.1.df_w
  100.5 0.0 collective-permute-done.hg_w
  100.5 1.9 %finish.1 = bf16[128,2048]{1,0:T(8,128)(2,1)S(1)} custom-call(s32[1]{0:T(128)} %bitcast.place, bf16[16,200,128]{2,1,0:T(8,128)(2,1)S(1)} %bitcast.12, f32[136,128]{1,0:T(8,128)S(1)} %get-tuple-element.13.other, bf16[128,128]{1,0:T(8,128)(2,1)S(1)} %get-tuple-element.14.df_query, f32[128,128]{1,0:T(8,128)S(1)} %get-tuple-element.15.local, ...), custom_call_target="tpu_custom_call" | custom-call | tf_op jit(solution)/shard_map/finish/pallas_call | solution.py:402
  102.4 13.6 %all_to_all.20.parts = bf16[8,16,2048]{2,1,0:T(8,128)(2,1)S(1)} all-to-all(bf16[8,16,2048]{2,1,0:T(8,128)(2,1)S(1)} %bitcast.13), channel_id=1, replica_groups=mesh['sp'=16,'fs'=4,'tp'=8] {'tp'}, dimensions={0} | all-to-all | bytes 1048576 | tf_op jit(solution)/shard_map/all_to_all | solution.py:422
  116.0 0.0 copy-done
  116.0 0.8 close.1
  (2 shorter events, 0.0 us)
Async XLA Ops:
  1.6 15.3 %all-to-all-start.1 = ((bf16[8,64,128]{2,1,0:T(8,128)(2,1)}), bf16[8,64,128]{2,1,0:T(8,128)(2,1)S(1)}, u32[]{:S(2)}, u32[]{:S(2)}) async-start(bf16[8,64,128]{2,1,0:T(8,128)(2,1)} %bitcast.3), calls=%async_computation.1 | async-start | bytes 262144 | tf_op jit(solution)/shard_map/all_to_all | solution.py:338
  16.9 37.9 %all-to-all-start = ((bf16[4,128,2048]{2,1,0:T(8,128)(2,1)}), bf16[4,128,2048]{2,1,0:T(8,128)(2,1)S(1)}, u32[]{:S(2)}, u32[]{:S(2)}) async-start(bf16[4,128,2048]{2,1,0:T(8,128)(2,1)} %norm.1), calls=%async_computation | async-start | bytes 4194304 | tf_op jit(solution)/shard_map/all_to_all | solution.py:321
  54.8 5.5 %copy-start.3 = (bf16[128,2048]{1,0:T(8,128)(2,1)S(1)}, bf16[128,2048]{1,0:T(8,128)(2,1)}, u32[]{:S(2)}) copy-start(bf16[128,2048]{1,0:T(8,128)(2,1)} %param.29) | copy-start | bytes 1572868
  54.8 7.8 %copy-start.1 = (f32[64]{0:T(128)S(1)}, f32[64]{0:T(128)}, u32[]{:S(2)}) copy-start(f32[64]{0:T(128)} %param.28) | copy-start | bytes 772
  54.8 7.8 %copy-start.2 = (f32[64]{0:T(128)S(1)}, f32[64]{0:T(128)}, u32[]{:S(2)}) copy-start(f32[64]{0:T(128)} %param.23) | copy-start | bytes 772
  56.4 11.3 %all-to-all-start.2 = ((bf16[8,192,128]{2,1,0:T(8,128)(2,1)}), bf16[8,192,128]{2,1,0:T(8,128)(2,1)S(1)}, u32[]{:S(2)}, u32[]{:S(2)}) async-start(bf16[8,192,128]{2,1,0:T(8,128)(2,1)} %bitcast.4), calls=%async_computation.2 | async-start | bytes 786432 | tf_op jit(solution)/shard_map/all_to_all | solution.py:369
  60.3 40.2 %collective-permute-start = (bf16[128,2048]{1,0:T(8,128)(2,1)S(1)}, bf16[128,2048]{1,0:T(8,128)(2,1)S(1)}, u32[]{:S(2)}, u32[]{:S(2)}) collective-permute-start(bf16[128,2048]{1,0:T(8,128)(2,1)S(1)} %copy-done.3), channel_id=1, source_target_pairs={{0,0},{1,1},{2,2},{3,3},{4,4},{5,5},{6,6},{7,7},{32,32},{33,33},{3... | collective-permute-start | bytes 1572872 | tf_op jit(solution)/shard_map/ppermute | solution.py:378
  61.0 39.5 %collective-permute-start.1 = (bf16[64,2048]{1,0:T(8,128)(2,1)}, bf16[64,2048]{1,0:T(8,128)(2,1)S(1)}, u32[]{:S(2)}, u32[]{:S(2)}) collective-permute-start(bf16[64,2048]{1,0:T(8,128)(2,1)} %param.30), channel_id=1, source_target_pairs={{0,0},{1,1},{2,2},{3,3},{4,4},{5,5},{6,6},{7,7},{32,32},{33,33},{3... | collective-permute-start | bytes 786440 | tf_op jit(solution)/shard_map/ppermute | solution.py:379
  69.1 46.9 %copy-start = (f32[2048]{0:T(1024)S(1)}, f32[2048]{0:T(1024)}, u32[]{:S(2)}) copy-start(f32[2048]{0:T(1024)} %param.31) | copy-start | bytes 24580

commit v7 on v6

--- a/solution.py
+++ b/solution.py
@@ -66,20 +66,27 @@
             out[c, j] = block
 
 
-def norm_kernel(x, gain_in, out, rows, gain, sems):
+def norm_kernel(x, gain_in, hg_w, df_w, out, outer, rows, gain, joined, sems):
     copies = (
         pltpu.make_async_copy(x.at[0], rows, sems.at[0]),
         pltpu.make_async_copy(gain_in, gain, sems.at[1]),
     )
-    for copy in copies:
+    late = (
+        pltpu.make_async_copy(hg_w, joined.at[:LANES], sems.at[2]),
+        pltpu.make_async_copy(df_w, joined.at[LANES:], sems.at[3]),
+    )
+    for copy in (*copies, *late):
         copy.start()
-    for copy in copies:
+    for copy in (*copies, *late):
         copy.wait()
+    store = pltpu.make_async_copy(joined, outer, sems.at[4])
+    store.start()
     part = rows[...].astype(f32)
     scale = lax.rsqrt(jnp.mean(part * part, axis=-1, keepdims=True) + epsilon)
     done = (part * scale * gain[...]).astype(bf16)
     for k in range(out.shape[0]):
         out[k] = done
+    store.wait()
 
 
 def project_kernel(place, rows, weights, out, rhs):
@@ -206,7 +213,7 @@
 
 
 def finish_kernel(
-    place, got, other, df_query, local, read_fwd, read_bwd, gains, hg_w, df_w, out, mixed
+    place, got, other, df_query, local, read_fwd, read_bwd, gains, outer, out, mixed
 ):
     devices = got.shape[0]
     length = local.shape[0]
@@ -266,10 +273,7 @@
     mixed[:, LANES:] = (
         weighted * lax.rsqrt(mean + epsilon) * gains[1:2, :HEAD] * df_factor
     ).astype(bf16)
-    out[...] = (
-        dot(mixed[:, :LANES], hg_w[...], ((1,), (0,)))
-        + dot(mixed[:, LANES:], df_w[...], ((1,), (0,)))
-    ).astype(bf16)
+    out[...] = dot(mixed[...], outer[...], ((1,), (0,))).astype(bf16)
 
 
 def close_kernel(parts, gain, out):
@@ -305,19 +309,23 @@
     packed = depth + depth // 2
 
     vmem = VMEM_SPEC
-    normed = pl.pallas_call(
+    normed, outer = pl.pallas_call(
         norm_kernel,
-        in_specs=[FAR_SPEC] * 2,
-        out_specs=vmem,
-        out_shape=pltpu.VMEM((fs, length, width), bf16),
+        in_specs=[FAR_SPEC] * 4,
+        out_specs=[pl.BlockSpec((fs, length, width), lambda: (0, 0, 0)), FAR_SPEC],
+        out_shape=[
+            pltpu.HBM((fs, length, width), bf16),
+            pltpu.HBM((LANES + HEAD, width), bf16),
+        ],
         scratch_shapes=[
             pltpu.VMEM((length, width), bf16),
             pltpu.VMEM((1, width), f32),
-            pltpu.SemaphoreType.DMA((2,)),
+            pltpu.VMEM((LANES + HEAD, width), bf16),
+            pltpu.SemaphoreType.DMA((5,)),
         ],
         compiler_params=LIMIT,
         name="norm",
-    )(there(inputs), there(norm_gain[None]))
+    )(*map(there, (inputs, norm_gain[None], out_hg_w, out_df_w)))
     rows = lax.all_to_all(normed, "fs", 0, 0, tiled=True)
     sources = (hg_query_w, hg_fwd_w, hg_bwd_w, hg_value_w, df_query_w, df_key_w, df_value_w)
     sent = pl.pallas_call(
@@ -375,8 +383,7 @@
         tiled=True,
     )
     swap = [(k * tp + t, k * tp + (t ^ (k // 2 % 2))) for k in range(sp) for t in range(tp)]
-    hg_rows = lax.ppermute(out_hg_w, ("sp", "tp"), swap)
-    df_rows = lax.ppermute(out_df_w, ("sp", "tp"), swap)
+    outer = lax.ppermute(outer, ("sp", "tp"), swap)
 
     place = z.astype(jnp.int32)[None]
     gains = jnp.concatenate([hg_norm_gain, hg_norm_gain, df_norm_gain, df_norm_gain])
@@ -401,7 +408,7 @@
     )
     partial = pl.pallas_call(
         finish_kernel,
-        in_specs=[SMEM_SPEC] + [vmem] * 9,
+        in_specs=[SMEM_SPEC] + [vmem] * 8,
         out_specs=vmem,
         out_shape=pltpu.VMEM((length, width), bf16),
         scratch_shapes=[pltpu.VMEM((length, LANES + HEAD), bf16)],
@@ -416,8 +423,7 @@
         here(read_fwd),
         here(read_bwd),
         here(gains),
-        here(hg_rows),
-        here(df_rows),
+        here(outer),
     )
     parts = lax.all_to_all(
         partial.reshape(tp, length // tp, width), "tp", 0, 0, tiled=True

time: 117 us -> 117 us (level)
  transfers between devices with their start and end apart: 5 -> 4, of which waited for: 2 -> 2; matrix products, arithmetic and copies ran while one was open for 0% -> 0% of each run, Pallas kernels for 3% -> 4%
where the time goes in v7:
time: 117 us
  blocking collectives  79.1 us (68%)
  starting transfers between devices  19.4 us (17%)
  Pallas kernels  10.7 us (9%)
  waiting for transfers between devices  6.5 us (6%)
    all_gather x1, blocking collectives, shards(): lax.all_gather(mine[None, :, :packed], ('sp', 'tp'), axis=0, tiled=True,...  34.2 us
    all_gather x1, blocking collectives, shards(): lax.all_gather(joined[None], ('sp', 'tp'), axis=0, tiled=True, axis_index...  31.3 us
    all_to_all x1, blocking collectives, shards(): lax.all_to_all(partial.reshape(tp, length // tp, width), 'tp', 0, 0, tile...  13.6 us
    all_to_all x1, starting transfers between devices, shards(): lax.all_to_all(sent.reshape(2 * fs, packed + EXTRA, LANES), ('fs', 'tp'),...  10.1 us
    all_to_all x1, waiting for transfers between devices, shards(): lax.all_to_all(projected.reshape(2 * fs, length + length // 2, LANES), ('...  4.84 us
    all_to_all x1, starting transfers between devices, shards(): lax.all_to_all(projected.reshape(2 * fs, length + length // 2, LANES), ('...  3.91 us
    all_to_all x1, starting transfers between devices, shards(): rows = lax.all_to_all(normed, 'fs', 0, 0, tiled=True)  3.61 us
    pallas_call x1, Pallas kernels, shards(): pl.pallas_call(norm_kernel, in_specs=[FAR_SPEC] * 4, out_specs=[pl.BlockS...  3.53 us
  transfers between devices with their start and end apart: 4, of which 2 were waited for; matrix products, arithmetic and copies ran while one was open for 0% of the time, Pallas kernels for 4%

profile of v7, /device:TPU:1, one launch (start us, length us, event | category | flops | bytes accessed | tf_op | source)
XLA Modules:
  0.0 116.6 jit_solution(5055210733064956011)
XLA Ops:
  0.0 1.6 %pack.1 = bf16[2,4,64,128]{3,2,1,0:T(8,128)(2,1)} custom-call(bf16[32,128]{1,0:T(8,128)(2,1)} %q.1, bf16[32,128]{1,0:T(8,128)(2,1)} %f.1, bf16[32,128]{1,0:T(8,128)(2,1)} %b.1, bf16[32,128]{1,0:T(8,128)(2,1)} %v.1, bf16[32,64]{1,0:T(8,128)(2,1)} %dq.1, bf16[32,64]{1,0:T(8,128)(2,1)} %dk.1, bf16[32,64]{1,0:T(8,128)(2,1)} %dv.1, f32[2,128]{1,0:T(2,128)} %gaps_in.1), custom_call_target="tpu_custom_call" | custom-call | tf_op jit(solution)/shard_map/pack/pallas_call | solution.py:331
  1.6 10.1 %all-to-all-start.1 = ((bf16[8,64,128]{2,1,0:T(8,128)(2,1)}), bf16[8,64,128]{2,1,0:T(8,128)(2,1)S(1)}, u32[]{:S(2)}, u32[]{:S(2)}) async-start(bf16[8,64,128]{2,1,0:T(8,128)(2,1)} %bitcast.3), calls=%async_computation.1 | async-start | bytes 262144 | tf_op jit(solution)/shard_map/all_to_all | solution.py:346
  11.7 3.5 %norm.1 = (bf16[4,128,2048]{2,1,0:T(8,128)(2,1)}, bf16[192,2048]{1,0:T(8,128)(2,1)}) custom-call(bf16[1,128,2048]{2,1,0:T(8,128)(2,1)} %x.1, f32[1,2048]{1,0:T(1,128)} %bitcast.15, bf16[128,2048]{1,0:T(8,128)(2,1)} %hg_w.1, bf16[64,2048]{1,0:T(8,128)(2,1)} %df_w.1), custom_call_target="tpu_custom_call" | custom-call | tf_op jit(solution)/shard_map/norm/pallas_call | solution.py:312
  15.3 1.7 %all-to-all-done.1 = bf16[8,64,128]{2,1,0:T(8,128)(2,1)S(1)} async-done(((bf16[8,64,128]{2,1,0:T(8,128)(2,1)}), bf16[8,64,128]{2,1,0:T(8,128)(2,1)S(1)}, u32[]{:S(2)}, u32[]{:S(2)}) %all-to-all-start.1) | async-done | bytes 131104 | tf_op jit(solution)/shard_map/all_to_all | solution.py:346
  16.9 3.6 %all-to-all-start = ((bf16[4,128,2048]{2,1,0:T(8,128)(2,1)}), bf16[4,128,2048]{2,1,0:T(8,128)(2,1)S(1)}, u32[]{:S(2)}, u32[]{:S(2)}) async-start(bf16[4,128,2048]{2,1,0:T(8,128)(2,1)} %get-tuple-element.14), calls=%async_computation | async-start | bytes 4194304 | tf_op jit(solution)/shard_map/all_to_all | solution.py:329
  20.6 34.2 %all-gather.weights = bf16[64,48,128]{2,1,0:T(8,128)(2,1)S(1)} all-gather(bf16[4,48,128]{2,1,0:T(8,128)(2,1)S(1)} %constant_dynamic-slice_fusion), channel_id=2, replica_groups={{0,32,65,97,128,160,193,225,256,288,321,353,384,416,449,481},{1,33,64,9..., dimensions={0}, use_global_device_ids=true | all-gather | bytes 835584 | tf_op jit(solution)/shard_map/all_gather | solution.py:359
  54.8 0.0 copy-start.1
  54.8 0.0 copy-start.2
  54.8 0.0 all-to-all-done.rows
  54.8 1.6 %project.1 = bf16[2,4,192,128]{3,2,1,0:T(8,128)(2,1)} custom-call(s32[1]{0:T(128)} %bitcast.1.place, bf16[4,128,2048]{2,1,0:T(8,128)(2,1)S(1)} %all-to-all-done.rows, bf16[64,48,128]{2,1,0:T(8,128)(2,1)S(1)} %all-gather.weights), custom_call_target="tpu_custom_call" | custom-call | tf_op jit(solution)/shard_map/project/pallas_call | solution.py:363
  56.4 3.9 %all-to-all-start.2 = ((bf16[8,192,128]{2,1,0:T(8,128)(2,1)}), bf16[8,192,128]{2,1,0:T(8,128)(2,1)S(1)}, u32[]{:S(2)}, u32[]{:S(2)}) async-start(bf16[8,192,128]{2,1,0:T(8,128)(2,1)} %bitcast.4), calls=%async_computation.2 | async-start | bytes 786432 | tf_op jit(solution)/shard_map/all_to_all | solution.py:377
  60.3 1.8 %collective-permute-start = (bf16[192,2048]{1,0:T(8,128)(2,1)}, bf16[192,2048]{1,0:T(8,128)(2,1)S(1)}, u32[]{:S(2)}, u32[]{:S(2)}) collective-permute-start(bf16[192,2048]{1,0:T(8,128)(2,1)} %get-tuple-element.22), channel_id=1, source_target_pairs={{0,0},{1,1},{2,2},{3,3},{4,4},{5,5},{6,6},{7,7},{32,32},{33,33},{3... | collective-permute-start | bytes 2359304 | tf_op jit(solution)/shard_map/ppermute | solution.py:386
  62.8 0.0 copy-done.1
  62.8 0.0 copy-done.2
  62.8 0.1 maximum_bitcast_fusion.gains_in
  62.9 4.8 %all-to-all-done.2.got = bf16[8,192,128]{2,1,0:T(8,128)(2,1)S(1)} async-done(((bf16[8,192,128]{2,1,0:T(8,128)(2,1)}), bf16[8,192,128]{2,1,0:T(8,128)(2,1)S(1)}, u32[]{:S(2)}, u32[]{:S(2)}) %all-to-all-start.2) | async-done | bytes 393248 | tf_op jit(solution)/shard_map/all_to_all | solution.py:377
  67.7 1.4 %local.1 = (bf16[200,128]{1,0:T(8,128)(2,1)S(1)}, f32[136,128]{1,0:T(8,128)S(1)}, bf16[128,128]{1,0:T(8,128)(2,1)S(1)}, f32[128,128]{1,0:T(8,128)S(1)}, bf16[128...) custom-call(s32[1]{0:T(128)S(6)} %select_n.20.place, f32[1]{0:T(128)S(6)} %copy.17.lam, ...), custom_call_target="tpu_custom_call" | custom-call | tf_op jit(solution)/shard_map/local/pallas_call | solution.py:390
  69.1 0.0 copy-start
  69.1 31.3 %all-gather.1 = bf16[3200,128]{1,0:T(8,128)(2,1)S(1)} all-gather(bf16[200,128]{1,0:T(8,128)(2,1)S(1)} %get-tuple-element.15), channel_id=3, replica_groups={{0,32,65,97,128,160,193,225,256,288,321,353,384,416,449,481},{1,33,64,9..., dimensions={0}, use_global_device_ids=true | all-gather | bytes 870400 | tf_op jit(solution)/shard_map/all_gather | solution.py:406
  100.5 0.0 collective-permute-done.outer
  100.5 1.8 %finish.1 = bf16[128,2048]{1,0:T(8,128)(2,1)S(1)} custom-call(s32[1]{0:T(128)} %bitcast.place, bf16[16,200,128]{2,1,0:T(8,128)(2,1)S(1)} %bitcast.12, f32[136,128]{1,0:T(8,128)S(1)} %get-tuple-element.16.other, bf16[128,128]{1,0:T(8,128)(2,1)S(1)} %get-tuple-element.17.df_query, f32[128,128]{1,0:T(8,128)S(1)} %get-tuple-element.18.local, ...), custom_call_target="tpu_custom_call" | custom-call | tf_op jit(solution)/shard_map/finish/pallas_call | solution.py:409
  102.3 13.6 %all_to_all.20.parts = bf16[8,16,2048]{2,1,0:T(8,128)(2,1)S(1)} all-to-all(bf16[8,16,2048]{2,1,0:T(8,128)(2,1)S(1)} %bitcast.13), channel_id=1, replica_groups=mesh['sp'=16,'fs'=4,'tp'=8] {'tp'}, dimensions={0} | all-to-all | bytes 1048576 | tf_op jit(solution)/shard_map/all_to_all | solution.py:428
  115.8 0.0 copy-done
  115.8 0.8 close.1
  (2 shorter events, 0.0 us)
Async XLA Ops:
  1.6 15.3 %all-to-all-start.1 = ((bf16[8,64,128]{2,1,0:T(8,128)(2,1)}), bf16[8,64,128]{2,1,0:T(8,128)(2,1)S(1)}, u32[]{:S(2)}, u32[]{:S(2)}) async-start(bf16[8,64,128]{2,1,0:T(8,128)(2,1)} %bitcast.3), calls=%async_computation.1 | async-start | bytes 262144 | tf_op jit(solution)/shard_map/all_to_all | solution.py:346
  16.9 37.9 %all-to-all-start = ((bf16[4,128,2048]{2,1,0:T(8,128)(2,1)}), bf16[4,128,2048]{2,1,0:T(8,128)(2,1)S(1)}, u32[]{:S(2)}, u32[]{:S(2)}) async-start(bf16[4,128,2048]{2,1,0:T(8,128)(2,1)} %get-tuple-element.14), calls=%async_computation | async-start | bytes 4194304 | tf_op jit(solution)/shard_map/all_to_all | solution.py:329
  54.8 7.9 %copy-start.1 = (f32[64]{0:T(128)S(1)}, f32[64]{0:T(128)}, u32[]{:S(2)}) copy-start(f32[64]{0:T(128)} %param.28) | copy-start | bytes 772
  54.8 7.9 %copy-start.2 = (f32[64]{0:T(128)S(1)}, f32[64]{0:T(128)}, u32[]{:S(2)}) copy-start(f32[64]{0:T(128)} %param.23) | copy-start | bytes 772
  56.4 11.3 %all-to-all-start.2 = ((bf16[8,192,128]{2,1,0:T(8,128)(2,1)}), bf16[8,192,128]{2,1,0:T(8,128)(2,1)S(1)}, u32[]{:S(2)}, u32[]{:S(2)}) async-start(bf16[8,192,128]{2,1,0:T(8,128)(2,1)} %bitcast.4), calls=%async_computation.2 | async-start | bytes 786432 | tf_op jit(solution)/shard_map/all_to_all | solution.py:377
  60.3 40.2 %collective-permute-start = (bf16[192,2048]{1,0:T(8,128)(2,1)}, bf16[192,2048]{1,0:T(8,128)(2,1)S(1)}, u32[]{:S(2)}, u32[]{:S(2)}) collective-permute-start(bf16[192,2048]{1,0:T(8,128)(2,1)} %get-tuple-element.22), channel_id=1, source_target_pairs={{0,0},{1,1},{2,2},{3,3},{4,4},{5,5},{6,6},{7,7},{32,32},{33,33},{3... | collective-permute-start | bytes 2359304 | tf_op jit(solution)/shard_map/ppermute | solution.py:386
  69.1 46.7 %copy-start = (f32[2048]{0:T(1024)S(1)}, f32[2048]{0:T(1024)}, u32[]{:S(2)}) copy-start(f32[2048]{0:T(1024)} %param.31) | copy-start | bytes 24580

commit v8 on v7

--- a/solution.py
+++ b/solution.py
@@ -66,7 +66,7 @@
             out[c, j] = block
 
 
-def norm_kernel(x, gain_in, hg_w, df_w, out, outer, rows, gain, joined, sems):
+def norm_kernel(x, gain_in, hg_w, df_w, out, outer, rows, gain, joined, done, sems, out_sems):
     copies = (
         pltpu.make_async_copy(x.at[0], rows, sems.at[0]),
         pltpu.make_async_copy(gain_in, gain, sems.at[1]),
@@ -81,12 +81,21 @@
         copy.wait()
     store = pltpu.make_async_copy(joined, outer, sems.at[4])
     store.start()
-    part = rows[...].astype(f32)
-    scale = lax.rsqrt(jnp.mean(part * part, axis=-1, keepdims=True) + epsilon)
-    done = (part * scale * gain[...]).astype(bf16)
-    for k in range(out.shape[0]):
-        out[k] = done
-    store.wait()
+    chunks, step, _ = done.shape
+    stores = [store]
+    for c in range(chunks):
+        part = rows[c * step : (c + 1) * step].astype(f32)
+        scale = lax.rsqrt(jnp.mean(part * part, axis=-1, keepdims=True) + epsilon)
+        done[c] = (part * scale * gain[...]).astype(bf16)
+        for k in range(out.shape[0]):
+            stores.append(
+                pltpu.make_async_copy(
+                    done.at[c], out.at[k, pl.ds(c * step, step)], out_sems.at[c, k]
+                )
+            )
+            stores[-1].start()
+    for store in stores:
+        store.wait()
 
 
 def project_kernel(place, rows, weights, out, rhs):
@@ -312,7 +321,7 @@
     normed, outer = pl.pallas_call(
         norm_kernel,
         in_specs=[FAR_SPEC] * 4,
-        out_specs=[pl.BlockSpec((fs, length, width), lambda: (0, 0, 0)), FAR_SPEC],
+        out_specs=[FAR_SPEC] * 2,
         out_shape=[
             pltpu.HBM((fs, length, width), bf16),
             pltpu.HBM((LANES + HEAD, width), bf16),
@@ -321,7 +330,9 @@
             pltpu.VMEM((length, width), bf16),
             pltpu.VMEM((1, width), f32),
             pltpu.VMEM((LANES + HEAD, width), bf16),
+            pltpu.VMEM((4, length // 4, width), bf16),
             pltpu.SemaphoreType.DMA((5,)),
+            pltpu.SemaphoreType.DMA((4, fs)),
         ],
         compiler_params=LIMIT,
         name="norm",

time: 117 us -> 117 us (level)
  no operation moved by 1% of the time
where the time goes in v8:
time: 117 us
  blocking collectives  79.1 us (68%)
  starting transfers between devices  19.4 us (17%)
  Pallas kernels  10.2 us (9%)
  waiting for transfers between devices  6.98 us (6%)
    all_gather x1, blocking collectives, shards(): lax.all_gather(mine[None, :, :packed], ('sp', 'tp'), axis=0, tiled=True,...  34.2 us
    all_gather x1, blocking collectives, shards(): lax.all_gather(joined[None], ('sp', 'tp'), axis=0, tiled=True, axis_index...  31.3 us
    all_to_all x1, blocking collectives, shards(): lax.all_to_all(partial.reshape(tp, length // tp, width), 'tp', 0, 0, tile...  13.6 us
    all_to_all x1, starting transfers between devices, shards(): lax.all_to_all(sent.reshape(2 * fs, packed + EXTRA, LANES), ('fs', 'tp'),...  10.1 us
    all_to_all x1, waiting for transfers between devices, shards(): lax.all_to_all(projected.reshape(2 * fs, length + length // 2, LANES), ('...  4.84 us
    all_to_all x1, starting transfers between devices, shards(): lax.all_to_all(projected.reshape(2 * fs, length + length // 2, LANES), ('...  3.91 us
    all_to_all x1, starting transfers between devices, shards(): rows = lax.all_to_all(normed, 'fs', 0, 0, tiled=True)  3.61 us
    pallas_call x1, Pallas kernels, shards(): pl.pallas_call(norm_kernel, in_specs=[FAR_SPEC] * 4, out_specs=[FAR_SPEC]...  3.05 us
  transfers between devices with their start and end apart: 4, of which 2 were waited for; matrix products, arithmetic and copies ran while one was open for 0% of the time, Pallas kernels for 4%

profile of v8, /device:TPU:1, one launch (start us, length us, event | category | flops | bytes accessed | tf_op | source)
XLA Modules:
  0.0 116.6 jit_solution(12919010290437728377)
XLA Ops:
  0.0 1.6 %pack.1 = bf16[2,4,64,128]{3,2,1,0:T(8,128)(2,1)} custom-call(bf16[32,128]{1,0:T(8,128)(2,1)} %q.1, bf16[32,128]{1,0:T(8,128)(2,1)} %f.1, bf16[32,128]{1,0:T(8,128)(2,1)} %b.1, bf16[32,128]{1,0:T(8,128)(2,1)} %v.1, bf16[32,64]{1,0:T(8,128)(2,1)} %dq.1, bf16[32,64]{1,0:T(8,128)(2,1)} %dk.1, bf16[32,64]{1,0:T(8,128)(2,1)} %dv.1, f32[2,128]{1,0:T(2,128)} %gaps_in.1), custom_call_target="tpu_custom_call" | custom-call | tf_op jit(solution)/shard_map/pack/pallas_call | solution.py:342
  1.6 10.1 %all-to-all-start.1 = ((bf16[8,64,128]{2,1,0:T(8,128)(2,1)}), bf16[8,64,128]{2,1,0:T(8,128)(2,1)S(1)}, u32[]{:S(2)}, u32[]{:S(2)}) async-start(bf16[8,64,128]{2,1,0:T(8,128)(2,1)} %bitcast.3), calls=%async_computation.1 | async-start | bytes 262144 | tf_op jit(solution)/shard_map/all_to_all | solution.py:357
  11.7 3.0 %norm.1 = (bf16[4,128,2048]{2,1,0:T(8,128)(2,1)}, bf16[192,2048]{1,0:T(8,128)(2,1)}) custom-call(bf16[1,128,2048]{2,1,0:T(8,128)(2,1)} %x.1, f32[1,2048]{1,0:T(1,128)} %bitcast.15, bf16[128,2048]{1,0:T(8,128)(2,1)} %hg_w.1, bf16[64,2048]{1,0:T(8,128)(2,1)} %df_w.1), custom_call_target="tpu_custom_call" | custom-call | tf_op jit(solution)/shard_map/norm/pallas_call | solution.py:321
  14.8 2.1 %all-to-all-done.1 = bf16[8,64,128]{2,1,0:T(8,128)(2,1)S(1)} async-done(((bf16[8,64,128]{2,1,0:T(8,128)(2,1)}), bf16[8,64,128]{2,1,0:T(8,128)(2,1)S(1)}, u32[]{:S(2)}, u32[]{:S(2)}) %all-to-all-start.1) | async-done | bytes 131104 | tf_op jit(solution)/shard_map/all_to_all | solution.py:357
  16.9 3.6 %all-to-all-start = ((bf16[4,128,2048]{2,1,0:T(8,128)(2,1)}), bf16[4,128,2048]{2,1,0:T(8,128)(2,1)S(1)}, u32[]{:S(2)}, u32[]{:S(2)}) async-start(bf16[4,128,2048]{2,1,0:T(8,128)(2,1)} %get-tuple-element.14), calls=%async_computation | async-start | bytes 4194304 | tf_op jit(solution)/shard_map/all_to_all | solution.py:340
  20.6 34.2 %all-gather.weights = bf16[64,48,128]{2,1,0:T(8,128)(2,1)S(1)} all-gather(bf16[4,48,128]{2,1,0:T(8,128)(2,1)S(1)} %constant_dynamic-slice_fusion), channel_id=2, replica_groups={{0,32,65,97,128,160,193,225,256,288,321,353,384,416,449,481},{1,33,64,9..., dimensions={0}, use_global_device_ids=true | all-gather | bytes 835584 | tf_op jit(solution)/shard_map/all_gather | solution.py:370
  54.8 0.0 copy-start.1
  54.8 0.0 copy-start.2
  54.8 0.0 all-to-all-done.rows
  54.8 1.6 %project.1 = bf16[2,4,192,128]{3,2,1,0:T(8,128)(2,1)} custom-call(s32[1]{0:T(128)} %bitcast.1.place, bf16[4,128,2048]{2,1,0:T(8,128)(2,1)S(1)} %all-to-all-done.rows, bf16[64,48,128]{2,1,0:T(8,128)(2,1)S(1)} %all-gather.weights), custom_call_target="tpu_custom_call" | custom-call | tf_op jit(solution)/shard_map/project/pallas_call | solution.py:374
  56.4 3.9 %all-to-all-start.2 = ((bf16[8,192,128]{2,1,0:T(8,128)(2,1)}), bf16[8,192,128]{2,1,0:T(8,128)(2,1)S(1)}, u32[]{:S(2)}, u32[]{:S(2)}) async-start(bf16[8,192,128]{2,1,0:T(8,128)(2,1)} %bitcast.4), calls=%async_computation.2 | async-start | bytes 786432 | tf_op jit(solution)/shard_map/all_to_all | solution.py:388
  60.3 1.8 %collective-permute-start = (bf16[192,2048]{1,0:T(8,128)(2,1)}, bf16[192,2048]{1,0:T(8,128)(2,1)S(1)}, u32[]{:S(2)}, u32[]{:S(2)}) collective-permute-start(bf16[192,2048]{1,0:T(8,128)(2,1)} %get-tuple-element.22), channel_id=1, source_target_pairs={{0,0},{1,1},{2,2},{3,3},{4,4},{5,5},{6,6},{7,7},{32,32},{33,33},{3... | collective-permute-start | bytes 2359304 | tf_op jit(solution)/shard_map/ppermute | solution.py:397
  62.8 0.0 copy-done.1
  62.8 0.0 copy-done.2
  62.8 0.1 maximum_bitcast_fusion.gains_in
  62.9 4.8 %all-to-all-done.2.got = bf16[8,192,128]{2,1,0:T(8,128)(2,1)S(1)} async-done(((bf16[8,192,128]{2,1,0:T(8,128)(2,1)}), bf16[8,192,128]{2,1,0:T(8,128)(2,1)S(1)}, u32[]{:S(2)}, u32[]{:S(2)}) %all-to-all-start.2) | async-done | bytes 393248 | tf_op jit(solution)/shard_map/all_to_all | solution.py:388
  67.7 1.4 %local.1 = (bf16[200,128]{1,0:T(8,128)(2,1)S(1)}, f32[136,128]{1,0:T(8,128)S(1)}, bf16[128,128]{1,0:T(8,128)(2,1)S(1)}, f32[128,128]{1,0:T(8,128)S(1)}, bf16[128...) custom-call(s32[1]{0:T(128)S(6)} %select_n.20.place, f32[1]{0:T(128)S(6)} %copy.17.lam, ...), custom_call_target="tpu_custom_call" | custom-call | tf_op jit(solution)/shard_map/local/pallas_call | solution.py:401
  69.1 0.0 copy-start
  69.1 31.3 %all-gather.1 = bf16[3200,128]{1,0:T(8,128)(2,1)S(1)} all-gather(bf16[200,128]{1,0:T(8,128)(2,1)S(1)} %get-tuple-element.15), channel_id=3, replica_groups={{0,32,65,97,128,160,193,225,256,288,321,353,384,416,449,481},{1,33,64,9..., dimensions={0}, use_global_device_ids=true | all-gather | bytes 870400 | tf_op jit(solution)/shard_map/all_gather | solution.py:417
  100.5 0.0 collective-permute-done.outer
  100.5 1.8 %finish.1 = bf16[128,2048]{1,0:T(8,128)(2,1)S(1)} custom-call(s32[1]{0:T(128)} %bitcast.place, bf16[16,200,128]{2,1,0:T(8,128)(2,1)S(1)} %bitcast.12, f32[136,128]{1,0:T(8,128)S(1)} %get-tuple-element.16.other, bf16[128,128]{1,0:T(8,128)(2,1)S(1)} %get-tuple-element.17.df_query, f32[128,128]{1,0:T(8,128)S(1)} %get-tuple-element.18.local, ...), custom_call_target="tpu_custom_call" | custom-call | tf_op jit(solution)/shard_map/finish/pallas_call | solution.py:420
  102.3 13.6 %all_to_all.20.parts = bf16[8,16,2048]{2,1,0:T(8,128)(2,1)S(1)} all-to-all(bf16[8,16,2048]{2,1,0:T(8,128)(2,1)S(1)} %bitcast.13), channel_id=1, replica_groups=mesh['sp'=16,'fs'=4,'tp'=8] {'tp'}, dimensions={0} | all-to-all | bytes 1048576 | tf_op jit(solution)/shard_map/all_to_all | solution.py:439
  115.8 0.0 copy-done
  115.8 0.8 close.1
  (2 shorter events, 0.0 us)
Async XLA Ops:
  1.6 15.3 %all-to-all-start.1 = ((bf16[8,64,128]{2,1,0:T(8,128)(2,1)}), bf16[8,64,128]{2,1,0:T(8,128)(2,1)S(1)}, u32[]{:S(2)}, u32[]{:S(2)}) async-start(bf16[8,64,128]{2,1,0:T(8,128)(2,1)} %bitcast.3), calls=%async_computation.1 | async-start | bytes 262144 | tf_op jit(solution)/shard_map/all_to_all | solution.py:357
  16.9 37.9 %all-to-all-start = ((bf16[4,128,2048]{2,1,0:T(8,128)(2,1)}), bf16[4,128,2048]{2,1,0:T(8,128)(2,1)S(1)}, u32[]{:S(2)}, u32[]{:S(2)}) async-start(bf16[4,128,2048]{2,1,0:T(8,128)(2,1)} %get-tuple-element.14), calls=%async_computation | async-start | bytes 4194304 | tf_op jit(solution)/shard_map/all_to_all | solution.py:340
  54.8 7.9 %copy-start.1 = (f32[64]{0:T(128)S(1)}, f32[64]{0:T(128)}, u32[]{:S(2)}) copy-start(f32[64]{0:T(128)} %param.28) | copy-start | bytes 772
  54.8 7.9 %copy-start.2 = (f32[64]{0:T(128)S(1)}, f32[64]{0:T(128)}, u32[]{:S(2)}) copy-start(f32[64]{0:T(128)} %param.23) | copy-start | bytes 772
  56.4 11.3 %all-to-all-start.2 = ((bf16[8,192,128]{2,1,0:T(8,128)(2,1)}), bf16[8,192,128]{2,1,0:T(8,128)(2,1)S(1)}, u32[]{:S(2)}, u32[]{:S(2)}) async-start(bf16[8,192,128]{2,1,0:T(8,128)(2,1)} %bitcast.4), calls=%async_computation.2 | async-start | bytes 786432 | tf_op jit(solution)/shard_map/all_to_all | solution.py:388
  60.3 40.2 %collective-permute-start = (bf16[192,2048]{1,0:T(8,128)(2,1)}, bf16[192,2048]{1,0:T(8,128)(2,1)S(1)}, u32[]{:S(2)}, u32[]{:S(2)}) collective-permute-start(bf16[192,2048]{1,0:T(8,128)(2,1)} %get-tuple-element.22), channel_id=1, source_target_pairs={{0,0},{1,1},{2,2},{3,3},{4,4},{5,5},{6,6},{7,7},{32,32},{33,33},{3... | collective-permute-start | bytes 2359304 | tf_op jit(solution)/shard_map/ppermute | solution.py:397
  69.1 46.7 %copy-start = (f32[2048]{0:T(1024)S(1)}, f32[2048]{0:T(1024)}, u32[]{:S(2)}) copy-start(f32[2048]{0:T(1024)} %param.31) | copy-start | bytes 24580
